TPU v7x, 32 devices: a whole 2x2x4 slice. The times are simulated.
32 devices in a mesh: ep: 8 (over z, x), tp: 4 (over y, core).
Axes of the slice: x: 2, y: 2, z: 4, core: 2. Of those that a mesh axis runs over, the one named last changes fastest.
Arguments:
- queries: bfloat16 [4096, 1024], P('ep', 'tp'), may hold values from -6 to 6
- key_input: bfloat16 [4096, 256], P('ep'), may hold values from -6 to 6
- value_input: bfloat16 [4096, 256], P('ep'), may hold values from -6 to 6
- query_gain: float32 [64], replicated, may hold values from 0.1 to 1.9
- key_gain: float32 [64], replicated, may hold values from 0.1 to 1.9
- mix_out_weight: bfloat16 [1024, 2048], P('tp'), may hold values from -0.1875 to 0.1875
- expert_input: bfloat16 [1280, 2048], P('ep'), may hold values from -6 to 6
- ffn_gain: float32 [2048], replicated, may hold values from 0.1 to 1.9
- routes: int32 [1280, 2], P('ep'), may hold values from 0 to 7, all different within a row; in each aligned block of 160 rows (0 to 159, 160 to 319, ...) at most 60 rows name the same one
- route_scores: float32 [1280, 2], P('ep'), may hold values from 0.1 to 1
- gate_weight: bfloat16 [8, 2048, 4096], P('ep', None, 'tp'), may hold values from -0.125 to 0.125
- up_weight: bfloat16 [8, 2048, 4096], P('ep', None, 'tp'), may hold values from -0.125 to 0.125
- down_weight: bfloat16 [8, 4096, 2048], P('ep', 'tp'), may hold values from -0.09375 to 0.09375
Outputs:
- mixed_rows: bfloat16 [4096, 2048], P(('ep', 'tp'))
- expert_out: bfloat16 [1280, 2048], P('ep', 'tp')
Inputs may be any that keep to these rules, and one draw needn't show every extreme that they name: `routes`: each row names 2 different experts. Within the rows of one index of ep (aligned blocks of 160 rows) no expert is named by more than 60 rows, and in every draw some expert is named by exactly 60 rows of some block.
All inputs are finite; a program needn't handle non-finite values.
Results may differ from a plain program's by a relative error of at most 0.019.
The roundings to bfloat16 on the way count: a program that leaves them out, or rounds other values in their place, can miss the bound.
Values may be sent and summed in bfloat16 or wider, within the bound.
No kernel may reach another device: no remote copies, remote signals or barrier semaphores. Data moves between devices by JAX's collectives and lax.ppermute only.
A program may use at most 64 MiB of HBM per device.

v0:
```python
import functools

import jax
import jax.numpy as jnp
import numpy as np
from jax import lax
from jax.experimental import pallas as pl
from jax.experimental.pallas import tpu as pltpu
from jax.sharding import PartitionSpec as P


HEADS = 16
KV_HEADS = 4
HD = 64
GRID_W = 64
EPSILON = 1e-06
ROPE_BASE = 10000.0
LOG2E = 1.4426950408889634
F32 = jnp.float32
BF16 = jnp.bfloat16
VMEM_LIMIT = 48 * 1024 * 1024
FLOPS_PER_MICRO = 500_000_000
CHUNKS = 1


def full(shape):
    return pl.BlockSpec(shape, lambda *_: (0,) * len(shape))


def hbm():
    return pl.BlockSpec(memory_space=pltpu.HBM)


def call(body, place, args, in_specs, outs, grid=(1,), scratch=(), out_specs=None, micros=1.0):
    return pl.pallas_call(
        body,
        grid_spec=pltpu.PrefetchScalarGridSpec(
            num_scalar_prefetch=1,
            grid=grid,
            in_specs=in_specs,
            out_specs=[full(o.shape) for o in outs] if out_specs is None else out_specs,
            scratch_shapes=list(scratch),
        ),
        out_shape=outs,
        cost_estimate=pl.CostEstimate(
            flops=int(micros * FLOPS_PER_MICRO), transcendentals=0, bytes_accessed=0
        ),
        compiler_params=pltpu.CompilerParams(
            dimension_semantics=("arbitrary",) * len(grid), vmem_limit_bytes=VMEM_LIMIT
        ),
    )(place, *args)


def mm(a, b, dims=((1,), (0,))):
    return lax.dot_general(a, b, (dims, ((), ())), preferred_element_type=F32)


def send(x, axis, flip):
    n = lax.axis_size(axis)
    return lax.ppermute(x, axis, [(i, i ^ flip) for i in range(n)])


def dispatch_body(place, routes_ref, x_hbm, *outs, experts, cap, chunks):
    out_refs, slot_ref, x_ref, sem = outs[:chunks], *outs[chunks:]
    tokens, feat = x_ref.shape
    cols = pl.ds(pl.multiple_of(place[0] * feat, feat), feat)
    fetch = pltpu.make_async_copy(x_hbm.at[:, cols], x_ref, sem)
    fetch.start()
    routes = routes_ref[...]
    rows = lax.broadcasted_iota(jnp.int32, (experts, tokens), 0)
    first = (rows == routes[0:1, :]).astype(F32)
    second = (rows == routes[1:2, :]).astype(F32)
    hits = first + second
    row = lax.broadcasted_iota(jnp.int32, (tokens, tokens), 0)
    col = lax.broadcasted_iota(jnp.int32, (tokens, tokens), 1)
    before = (row < col).astype(F32).astype(BF16)
    count = mm(hits.astype(BF16), before)
    slot = jnp.where(hits > 0.5, count, -1.0).astype(jnp.int32)
    part = cap // chunks

    def flat(choice, expert):
        at = jnp.sum(count * choice, axis=0, keepdims=True).astype(jnp.int32)
        piece = sum([(at >= c * part).astype(jnp.int32) for c in range(1, chunks)], jnp.zeros_like(at))
        return piece * (experts * part) + expert * part + at - piece * part

    slot_ref[0:1, :] = flat(first, routes[0:1, :])
    slot_ref[1:2, :] = flat(second, routes[1:2, :])
    fetch.wait()
    x = x_ref[...]
    for c in range(chunks):
        slots = lax.broadcasted_iota(jnp.int32, (part, tokens), 0) + c * part
        for e in range(experts):
            pick = (slots == slot[e : e + 1, :]).astype(F32).astype(BF16)
            out_refs[c][e * part : (e + 1) * part, :] = mm(pick, x).astype(BF16)


def dispatch(place, routes, expert_input, experts, cap, chunks, feat):
    tokens = routes.shape[1]
    outs = [jax.ShapeDtypeStruct((experts * cap // chunks, feat), BF16)] * chunks
    outs += [jax.ShapeDtypeStruct((2, tokens), jnp.int32)]
    return call(
        functools.partial(dispatch_body, experts=experts, cap=cap, chunks=chunks),
        place,
        (routes, expert_input),
        [full(routes.shape), hbm()],
        outs,
        scratch=[pltpu.VMEM((tokens, feat), BF16), pltpu.SemaphoreType.DMA],
        micros=1.5,
    )


def rope_tables(token_count, n_ep):
    quarter = HD // 4
    inverse = (np.float32(ROPE_BASE) ** (-np.arange(quarter, dtype=np.float32) / np.float32(quarter))).astype(
        np.float32
    )
    pos = np.arange(token_count * n_ep)

    def both(steps):
        angle = (inverse[:, None] * steps.astype(np.float32)[None, :]).astype(np.float32).astype(np.float64)
        return np.concatenate([np.cos(angle), np.sin(angle)], 0).astype(np.float32)

    return np.concatenate([both(pos // GRID_W), both(pos % GRID_W)], 0)


def turn(x, gain, table, low):
    quarter = HD // 4
    x = x.astype(F32)
    scale = lax.rsqrt(jnp.mean(x * x, axis=0, keepdims=True) + EPSILON)
    x = x * scale * gain
    u0, w0, u1, w1 = (x[i * quarter : (i + 1) * quarter] for i in range(4))
    cr, sr, cc, sc = (table[i * quarter : (i + 1) * quarter] for i in range(4))
    return jnp.concatenate(
        [u0 * cr - w0 * sr, w0 * cr + u0 * sr, u1 * cc - w1 * sc, w1 * cc + u1 * sc], axis=0
    ).astype(low)


def column(row):
    n = row.shape[1]
    same = lax.broadcasted_iota(jnp.int32, (n, n), 0) == lax.broadcasted_iota(jnp.int32, (n, n), 1)
    return jnp.sum(jnp.where(same, row, 0.0), axis=1, keepdims=True)


def prep_body(
    place, q_ref, k_ref, v_ref, q_gain_ref, k_gain_ref, table_ref, qt_ref, kvt_ref, turned_ref, *, heads, group
):
    table = table_ref[...]
    q_gain = column(q_gain_ref[...])
    k_gain = column(k_gain_ref[...])
    qt = q_ref[...].astype(F32).T
    for h in range(heads):
        qt_ref[h * HD : (h + 1) * HD, :] = turn(qt[h * HD : (h + 1) * HD], q_gain, table, BF16)
    start = pl.multiple_of((place[0] * heads // group) * HD, HD)
    turned_ref[...] = k_ref[...].astype(F32).T
    kvt_ref[:HD, :] = turn(turned_ref[pl.ds(start, HD), :], k_gain, table, BF16)
    turned_ref[...] = v_ref[...].astype(F32).T
    kvt_ref[HD:, :] = turned_ref[pl.ds(start, HD), :].astype(BF16)


def prep(place, queries, key_input, value_input, q_gain, k_gain, table, heads):
    rows = queries.shape[0]
    return call(
        functools.partial(prep_body, heads=heads, group=HEADS // KV_HEADS),
        place,
        (queries, key_input, value_input, q_gain, k_gain, table),
        [
            full(queries.shape),
            full(key_input.shape),
            full(value_input.shape),
            full(q_gain.shape),
            full(k_gain.shape),
            pl.BlockSpec((table.shape[0], rows), lambda i, place: (0, place[1])),
        ],
        [
            jax.ShapeDtypeStruct((queries.shape[1], rows), BF16),
            jax.ShapeDtypeStruct((2 * HD, rows), BF16),
        ],
        scratch=[pltpu.VMEM((key_input.shape[1], rows), F32)],
        micros=1.5,
    )


def attend_body(place, qt_ref, *refs, blocks, heads, groups):
    count = len(refs) - 5 - groups
    kv_refs, out_refs = refs[:count], refs[count : count + groups]
    out_ref, k_ref, v_ref, num_ref, den_ref = refs[count + groups :]
    keys = kv_refs[0].shape[1]
    per = blocks // count
    for b in range(blocks):
        base = (b % per) * 2 * HD
        k_ref[b] = kv_refs[b // per][base : base + HD, :].astype(F32).T.astype(BF16)
        v_ref[b] = kv_refs[b // per][base + HD : base + 2 * HD, :]
    num_ref[...] = jnp.zeros_like(num_ref)
    den_ref[...] = jnp.zeros_like(den_ref)

    def one(b, carry):
        k = k_ref[b]
        v = v_ref[b]
        for h in range(heads):
            q = qt_ref[h * HD : (h + 1) * HD, :]
            p = jnp.exp2(mm(k, q) * (LOG2E * HD**-0.5))
            den_ref[h * 8 : (h + 1) * 8, :] += jnp.sum(p.reshape(keys // 8, 8, p.shape[1]), axis=0)
            num_ref[h * HD : (h + 1) * HD, :] += mm(v, p.astype(BF16))
        return carry

    lax.fori_loop(0, blocks, one, 0)
    for h in range(heads):
        den = jnp.sum(den_ref[h * 8 : (h + 1) * 8, :], axis=0, keepdims=True)
        num_ref[h * HD : (h + 1) * HD, :] = num_ref[h * HD : (h + 1) * HD, :] / den
    out_ref[...] = num_ref[...].T
    rows = out_refs[0].shape[0]
    for k in range(groups):
        at = pl.multiple_of((place[0] ^ k) * rows, rows)
        out_refs[k][...] = out_ref[pl.ds(at, rows), :].astype(BF16)


def attend(place, qt, kv_blocks, heads, groups):
    rows = qt.shape[1]
    keys = kv_blocks[0].shape[1]
    blocks = sum(b.shape[0] for b in kv_blocks) // (2 * HD)
    return call(
        functools.partial(attend_body, blocks=blocks, heads=heads, groups=groups),
        place,
        (qt, *kv_blocks),
        [full(qt.shape)] + [full(b.shape) for b in kv_blocks],
        [jax.ShapeDtypeStruct((rows // groups, qt.shape[0]), BF16)] * groups,
        scratch=[
            pltpu.VMEM((rows, qt.shape[0]), F32),
            pltpu.VMEM((blocks, keys, HD), BF16),
            pltpu.VMEM((blocks, HD, keys), BF16),
            pltpu.VMEM(qt.shape, F32),
            pltpu.VMEM((heads * 8, rows), F32),
        ],
        micros=12.0,
    )


def mix_body(place, *refs, groups):
    att_refs, w_refs, out_ref = refs[:groups], refs[groups : 2 * groups], refs[2 * groups]
    total = jnp.zeros(out_ref.shape, F32)
    for k in range(groups):
        total += mm(att_refs[k][...], w_refs[k][...]).astype(BF16).astype(F32)
    out_ref[...] = total.astype(BF16)


def mix(place, atts, weights):
    groups = len(weights)
    rows = atts[0].shape[0]
    depth, width = weights[0].shape
    tile = min(width, 512)
    return call(
        functools.partial(mix_body, groups=groups),
        place,
        (*atts, *weights),
        [full(a.shape) for a in atts] + [pl.BlockSpec((depth, tile), lambda j, place: (0, j))] * groups,
        [jax.ShapeDtypeStruct((rows, width), BF16)],
        grid=(width // tile,),
        out_specs=[pl.BlockSpec((rows, tile), lambda j, place: (0, j))],
        micros=2.5,
    )[0]


def expert_body(place, *refs, groups, tile):
    x_refs = refs[:groups]
    gain_ref, gate_hbm, up_hbm, down_hbm = refs[groups : groups + 4]
    out_refs = refs[groups + 4 : 2 * groups + 4]
    scaled_ref, hidden_ref, gate_ref, up_ref, down_ref, gate_sem, up_sem, down_sem = refs[2 * groups + 4 :]
    feat = x_refs[0].shape[1]
    width = groups * feat
    steps = gate_ref.shape[0]

    def spot(k):
        return pl.ds(pl.multiple_of((place[0] ^ k) * feat, feat), feat)

    def fetch_gate(j):
        cols = pl.ds(pl.multiple_of(j * tile, tile), tile)
        return pltpu.make_async_copy(gate_hbm.at[0, :, cols], gate_ref.at[j], gate_sem.at[j])

    def fetch_up(j):
        cols = pl.ds(pl.multiple_of(j * tile, tile), tile)
        return pltpu.make_async_copy(up_hbm.at[0, :, cols], up_ref.at[j], up_sem.at[j])

    def fetch_down(k):
        return pltpu.make_async_copy(down_hbm.at[0, :, spot(k)], down_ref.at[k], down_sem.at[k])

    for j in range(steps):
        fetch_gate(j).start()
        fetch_up(j).start()
    for k in range(groups):
        fetch_down(k).start()

    squares = 0.0
    for k in range(groups):
        x = x_refs[k][...].astype(F32)
        scaled_ref[:, spot(k)] = (x * gain_ref[:, spot(k)]).astype(BF16)
        squares += jnp.sum(x * x, axis=1, keepdims=True)
    scale = lax.rsqrt(squares / width + EPSILON)

    def one(j, carry):
        x = scaled_ref[...]
        fetch_gate(j).wait()
        gate = mm(x, gate_ref[j]) * scale
        fetch_up(j).wait()
        up = mm(x, up_ref[j]) * scale
        cols = pl.ds(pl.multiple_of(j * tile, tile), tile)
        hidden_ref[:, cols] = (gate / (1.0 + jnp.exp(-gate)) * up).astype(BF16)
        return carry

    lax.fori_loop(0, steps, one, 0)
    for k in range(groups):
        fetch_down(k).wait()
        out_refs[k][...] = mm(hidden_ref[...], down_ref[k]).astype(BF16)


def expert(place, xs, gain, gate, up, down):
    groups = len(xs)
    rows, feat = xs[0].shape
    depth, ff = gate.shape[1:]
    tile = min(ff, 256)
    steps = ff // tile
    return call(
        functools.partial(expert_body, groups=groups, tile=tile),
        place,
        (*xs, gain, gate, up, down),
        [full(x.shape) for x in xs] + [full(gain.shape), hbm(), hbm(), hbm()],
        [jax.ShapeDtypeStruct((rows, feat), BF16)] * groups,
        scratch=[
            pltpu.VMEM((rows, depth), BF16),
            pltpu.VMEM((rows, ff), BF16),
            pltpu.VMEM((steps, depth, tile), BF16),
            pltpu.VMEM((steps, depth, tile), BF16),
            pltpu.VMEM((groups, ff, feat), BF16),
            pltpu.SemaphoreType.DMA((steps,)),
            pltpu.SemaphoreType.DMA((steps,)),
            pltpu.SemaphoreType.DMA((groups,)),
        ],
        micros=9.0,
    )


def combine_body(place, slot_ref, scores_ref, *refs, chunks):
    row_refs, out_ref = refs[:chunks], refs[chunks]
    tokens = out_ref.shape[0]
    slots = row_refs[0].shape[0]
    scores = scores_ref[...]
    weight = scores / jnp.sum(scores, axis=0, keepdims=True)
    slot = slot_ref[...]
    total = jnp.zeros(out_ref.shape, F32)
    for k in range(2):
        picked = jnp.zeros(out_ref.shape, F32)
        for c in range(chunks):
            rows = lax.broadcasted_iota(jnp.int32, (slots, tokens), 0) + c * slots
            pick = (rows == slot[k : k + 1, :]).astype(F32).astype(BF16)
            picked += mm(pick, row_refs[c][...], ((0,), (0,)))
        total += picked * column(weight[k : k + 1, :])
    out_ref[...] = total.astype(BF16)


def combine(place, slot, scores, rows):
    return call(
        functools.partial(combine_body, chunks=len(rows)),
        place,
        (slot, scores, *rows),
        [full(slot.shape), full(scores.shape)] + [full(r.shape) for r in rows],
        [jax.ShapeDtypeStruct((slot.shape[1], rows[0].shape[1]), BF16)],
        micros=1.5,
    )[0]


def local(
    table,
    queries,
    key_input,
    value_input,
    query_gain,
    key_gain,
    mix_out_weight,
    expert_input,
    ffn_gain,
    routes,
    route_scores,
    gate_weight,
    up_weight,
    down_weight,
):
    n_ep = lax.axis_size("ep")
    n_tp = lax.axis_size("tp")
    heads = queries.shape[1] // HD
    tokens, top = routes.shape
    width = expert_input.shape[1]
    feat = width // n_tp
    cap = 3 * tokens * top // (2 * n_ep)
    unit = 8 * CHUNKS
    cap = -(-cap // unit) * unit
    place = jnp.stack([lax.axis_index("tp"), lax.axis_index("ep")]).astype(jnp.int32)

    weights = {0: mix_out_weight}
    for k in range(2, n_tp, 2):
        weights[k] = send(mix_out_weight, "tp", k)

    *outbound, slot = dispatch(place, routes.T, expert_input, n_ep, cap, CHUNKS, feat)
    arrived = [lax.all_to_all(o, "ep", split_axis=0, concat_axis=0, tiled=True) for o in outbound]

    qt, kvt = prep(
        place, queries, key_input, value_input, query_gain[None], key_gain[None], table, heads
    )
    pair = jnp.concatenate([kvt, send(kvt, "ep", 1)], axis=0)
    blocks = [pair] + [send(pair, "ep", k) for k in sorted(range(2, n_ep, 2), key=lambda k: k ^ (n_ep // 2))]

    reduced = []
    for a in arrived:
        xs = {0: a}
        for k in range(2, n_tp, 2):
            xs[k] = send(a, "tp", k)
        for k in range(0, n_tp, 2):
            xs[k + 1] = send(xs[k], "tp", 1)
        parts = expert(
            place, [xs[k] for k in range(n_tp)], ffn_gain[None], gate_weight, up_weight, down_weight
        )
        other = {k: send(parts[k + 1], "tp", 1) for k in range(0, n_tp, 2)}
        total = parts[0].astype(F32) + other[0].astype(F32)
        for k in range(2, n_tp, 2):
            both = (parts[k].astype(F32) + other[k].astype(F32)).astype(BF16)
            total += send(both, "tp", k).astype(F32)
        reduced.append(total.astype(BF16))

    for k in range(0, n_tp, 2):
        weights[k + 1] = send(weights[k], "tp", 1)
    atts = attend(place, qt, blocks, heads, n_tp)
    atts = [atts[0]] + [send(atts[k], "tp", k) for k in range(1, n_tp)]
    mixed = mix(place, atts, [weights[k] for k in range(n_tp)])

    returned = [lax.all_to_all(r, "ep", split_axis=0, concat_axis=0, tiled=True) for r in reduced]
    out = combine(place, slot, route_scores.T, returned)
    return mixed, out


def solution(mesh):
    n_ep = mesh.shape["ep"]
    placed = (
        P(),
        P("ep", "tp"),
        P("ep", None),
        P("ep", None),
        P(),
        P(),
        P("tp", None),
        P("ep", None),
        P(),
        P("ep", None),
        P("ep", None),
        P("ep", None, "tp"),
        P("ep", None, "tp"),
        P("ep", "tp", None),
    )

    step = jax.shard_map(
        local,
        mesh=mesh,
        in_specs=placed,
        out_specs=(P(("ep", "tp"), None), P("ep", "tp")),
        check_vma=False,
    )

    def run(queries, *rest):
        table = jnp.asarray(rope_tables(queries.shape[0] // n_ep, n_ep))
        return step(table, queries, *rest)

    return run
```

profile of v0, /device:TPU:0, one launch (start us, length us, event | category | flops | bytes accessed | tf_op | source)
XLA Modules:
  0.0 126.0 jit_solution(7360319244302476629)
XLA Ops:
  0.6 0.1 pad_add_fusion.place
  0.7 1.1 copy-done.1
  1.8 0.0 copy-start.6
  1.8 0.7 copy-done.6
  2.5 1.1 shard_map.152
  3.6 21.6 %all_to_all.22 = bf16[8,64,512]{2,1,0:T(8,128)(2,1)S(1)} all-to-all(bf16[8,64,512]{2,1,0:T(8,128)(2,1)S(1)} %bitcast.14), channel_id=1, replica_groups=mesh['ep'=8,'tp'=4] {'ep'}, dimensions={0} | all-to-all | bytes 1048576 | tf_op jit(solution)/shard_map/all_to_all | solution.py:402
  25.2 1.5 %collective-permute-start.11 = (bf16[512,512]{1,0:T(8,128)(2,1)S(1)}, bf16[512,512]{1,0:T(8,128)(2,1)S(1)}, u32[]{:S(2)}, u32[]{:S(2)}) collective-permute-start(bf16[512,512]{1,0:T(8,128)(2,1)S(1)} %bitcast.11), channel_id=1, source_target_pairs={{0,2},{1,3},{2,0},{3,1},{4,6},{5,7},{6,4},{7,5},{8,10},{9,11},{10,... | collective-permute-start | bytes 1572872 | tf_op jit(solution)/shard_map/ppermute | solution.py:60
  26.7 0.0 collective-permute-start.10
  26.7 11.0 %collective-permute-done.11.refs_2_ = bf16[512,512]{1,0:T(8,128)(2,1)S(1)} collective-permute-done((bf16[512,512]{1,0:T(8,128)(2,1)S(1)}, bf16[512,512]{1,0:T(8,128)(2,1)S(1)}, u32[]{:S(2)}, u32[]{:S(2)}) %collective-permute-start.11) | collective-permute-done | bytes 524320 | tf_op jit(solution)/shard_map/ppermute | solution.py:60
  37.7 0.0 collective-permute-start.12
  37.7 0.0 collective-permute-done.10.refs_1_
  37.7 1.9 %collective-permute-done.12.refs_3_ = bf16[512,512]{1,0:T(8,128)(2,1)S(1)} collective-permute-done((bf16[512,512]{1,0:T(8,128)(2,1)S(1)}, bf16[512,512]{1,0:T(8,128)(2,1)S(1)}, u32[]{:S(2)}, u32[]{:S(2)}) %collective-permute-start.12) | collective-permute-done | bytes 524320 | tf_op jit(solution)/shard_map/ppermute | solution.py:60
  39.6 0.7 copy-done.5
  40.3 0.0 copy-start.8
  40.4 0.0 copy-start.9
  40.4 0.0 copy-start.10
  40.4 16.1 %shard_map.153 = (bf16[512,512]{1,0:T(8,128)(2,1)S(1)}, bf16[512,512]{1,0:T(8,128)(2,1)S(1)}, bf16[512,512]{1,0:T(8,128)(2,1)S(1)}, bf16[512,512]{1,0:T(8,128)(2,1)S(1)}) custom-call(s32[2]{0:T(128)S(1)} %pad_add_fusion.place, bf16[512,512]{1,0:T(8,128)(2,1)S(1)} %bitcast.13, bf16[512,512]{1,0:T(8,128)(2,1)S(1)} %collective-permute-done.10.refs_1_, ...), custom_call_target="tpu_custom_call" | custom-call | flops 4499999744 | tf_op jit(solution)/shard_map/pallas_call | solution.py:35
  56.5 0.2 collective-permute-start.14
  56.7 0.0 copy-done
  56.7 1.5 %collective-permute-start.8 = (bf16[256,2048]{1,0:T(8,128)(2,1)S(1)}, bf16[256,2048]{1,0:T(8,128)(2,1)S(1)}, u32[]{:S(2)}, u32[]{:S(2)}) collective-permute-start(bf16[256,2048]{1,0:T(8,128)(2,1)S(1)} %copy-done), channel_id=1, source_target_pairs={{0,2},{1,3},{2,0},{3,1},{4,6},{5,7},{6,4},{7,5},{8,10},{9,11},{10,... | collective-permute-start | bytes 3145736 | tf_op jit(solution)/shard_map/ppermute | solution.py:60
  58.2 0.1 collective-permute-start.13
  58.3 0.2 collective-permute-done.14
  58.4 0.1 add_convert_fusion.1
  58.6 1.6 %collective-permute-start.15 = (bf16[512,512]{1,0:T(8,128)(2,1)S(1)}, bf16[512,512]{1,0:T(8,128)(2,1)S(1)}, u32[]{:S(2)}, u32[]{:S(2)}) collective-permute-start(bf16[512,512]{1,0:T(8,128)(2,1)S(1)} %add_convert_fusion.1), channel_id=1, source_target_pairs={{0,2},{1,3},{2,0},{3,1},{4,6},{5,7},{6,4},{7,5},{8,10},{9,11},{10,... | collective-permute-start | bytes 1572872 | tf_op jit(solution)/shard_map/ppermute | solution.py:60
  60.2 0.0 copy-done.2
  60.2 0.0 copy-done.3
  60.2 0.0 copy-done.4
  60.2 0.0 copy-done.8
  60.2 0.0 copy-done.9
  60.2 0.0 copy-done.10
  60.2 1.0 shard_map.149
  61.2 0.0 copy-start.11
  61.2 0.7 copy-done.11
  61.9 1.5 %collective-permute-start = (bf16[128,512]{1,0:T(8,128)(2,1)S(1)}, bf16[128,512]{1,0:T(8,128)(2,1)S(1)}, u32[]{:S(2)}, u32[]{:S(2)}) collective-permute-start(bf16[128,512]{1,0:T(8,128)(2,1)S(1)} %get-tuple-element.15), channel_id=1, source_target_pairs={{0,4},{4,0},{8,12},{12,8},{16,20},{20,16},{24,28},{28,24},{1,5},{5... | collective-permute-start | bytes 393224 | tf_op jit(solution)/shard_map/ppermute | solution.py:60
  63.4 0.0 collective-permute-start.7
  63.4 3.8 %collective-permute-done = bf16[128,512]{1,0:T(8,128)(2,1)S(1)} collective-permute-done((bf16[128,512]{1,0:T(8,128)(2,1)S(1)}, bf16[128,512]{1,0:T(8,128)(2,1)S(1)}, u32[]{:S(2)}, u32[]{:S(2)}) %collective-permute-start) | collective-permute-done | bytes 131104 | tf_op jit(solution)/shard_map/ppermute | solution.py:60
  67.2 1.5 %collective-permute-start.1 = (bf16[256,512]{1,0:T(8,128)(2,1)S(1)}, bf16[256,512]{1,0:T(8,128)(2,1)}, u32[]{:S(2)}, u32[]{:S(2)}) collective-permute-start(bf16[256,512]{1,0:T(8,128)(2,1)S(1)} %constant_dynamic-update-slice_fusion.refs_0_), channel_id=1, source_target_pairs={{0,16},{4,20},{8,24},{12,28},{16,0},{20,4},{24,8},{28,12},{1,17},{... | collective-permute-start | bytes 786440 | tf_op jit(solution)/shard_map/ppermute | solution.py:60
  68.7 14.0 %collective-permute-done.8.refs_6_ = bf16[256,2048]{1,0:T(8,128)(2,1)S(1)} collective-permute-done((bf16[256,2048]{1,0:T(8,128)(2,1)S(1)}, bf16[256,2048]{1,0:T(8,128)(2,1)S(1)}, u32[]{:S(2)}, u32[]{:S(2)}) %collective-permute-start.8) | collective-permute-done | bytes 1048608 | tf_op jit(solution)/shard_map/ppermute | solution.py:60
  82.7 1.8 %collective-permute-start.2 = (bf16[256,512]{1,0:T(8,128)(2,1)S(1)}, bf16[256,512]{1,0:T(8,128)(2,1)}, u32[]{:S(2)}, u32[]{:S(2)}) collective-permute-start(bf16[256,512]{1,0:T(8,128)(2,1)S(1)} %constant_dynamic-update-slice_fusion.refs_0_), channel_id=1, source_target_pairs={{0,24},{4,28},{8,16},{12,20},{16,8},{20,12},{24,0},{28,4},{1,25},{... | collective-permute-start | bytes 786440 | tf_op jit(solution)/shard_map/ppermute | solution.py:60
  84.5 0.0 collective-permute-done.13
  84.5 0.1 collective-permute-start.3
  84.7 8.7 %collective-permute-done.15 = bf16[512,512]{1,0:T(8,128)(2,1)S(1)} collective-permute-done((bf16[512,512]{1,0:T(8,128)(2,1)S(1)}, bf16[512,512]{1,0:T(8,128)(2,1)S(1)}, u32[]{:S(2)}, u32[]{:S(2)}) %collective-permute-start.15) | collective-permute-done | bytes 524320 | tf_op jit(solution)/shard_map/ppermute | solution.py:60
  93.3 0.0 collective-permute-start.9
  93.3 1.0 add_convert_fusion
  94.3 4.4 %all-to-all-start.1 = ((bf16[8,64,512]{2,1,0:T(8,128)(2,1)}), bf16[8,64,512]{2,1,0:T(8,128)(2,1)}, u32[]{:S(2)}, u32[]{:S(2)}) async-start(bf16[8,64,512]{2,1,0:T(8,128)(2,1)} %bitcast.20), calls=%async_computation.1 | async-start | bytes 1048576 | tf_op jit(solution)/shard_map/all_to_all | solution.py:433
  98.7 0.0 collective-permute-done.1.refs_1_
  98.7 0.0 collective-permute-done.2.refs_2_
  98.7 0.0 collective-permute-done.3.refs_3_
  98.7 0.0 copy-start.12
  98.7 0.9 copy-done.12
  99.7 13.0 %shard_map.150 = (bf16[128,256]{1,0:T(8,128)(2,1)S(1)}, bf16[128,256]{1,0:T(8,128)(2,1)S(1)}, bf16[128,256]{1,0:T(8,128)(2,1)S(1)}, bf16[128,256]{1,0:T(8,128)(2,1)S(1)}) custom-call(s32[2]{0:T(128)S(1)} %pad_add_fusion.place, bf16[256,512]{1,0:T(8,128)(2,1)S(1)} %copy-done.12, bf16[256,512]{1,0:T(8,128)(2,1)S(1)} %constant_dynamic-update-slice_fusion.refs_0_, ...), custom_call_target="tpu_custom_call" | custom-call | flops 6000000000 | tf_op jit(solution)/shard_map/pallas_call | solution.py:35
  112.7 0.0 copy-start.7
  112.7 0.4 collective-permute-start.4
  113.0 1.5 %collective-permute-start.5 = (bf16[128,256]{1,0:T(8,128)(2,1)S(1)}, bf16[128,256]{1,0:T(8,128)(2,1)S(1)}, u32[]{:S(2)}, u32[]{:S(2)}) collective-permute-start(bf16[128,256]{1,0:T(8,128)(2,1)S(1)} %get-tuple-element.18), channel_id=1, source_target_pairs={{0,2},{1,3},{2,0},{3,1},{4,6},{5,7},{6,4},{7,5},{8,10},{9,11},{10,... | collective-permute-start | bytes 196616 | tf_op jit(solution)/shard_map/ppermute | solution.py:60
  114.6 0.1 collective-permute-start.6
  114.6 0.0 collective-permute-done.4.refs_1_
  114.6 2.7 %collective-permute-done.5.refs_2_ = bf16[128,256]{1,0:T(8,128)(2,1)S(1)} collective-permute-done((bf16[128,256]{1,0:T(8,128)(2,1)S(1)}, bf16[128,256]{1,0:T(8,128)(2,1)S(1)}, u32[]{:S(2)}, u32[]{:S(2)}) %collective-permute-start.5) | collective-permute-done | bytes 65568 | tf_op jit(solution)/shard_map/ppermute | solution.py:60
  117.3 1.5 %collective-permute-done.6.refs_3_ = bf16[128,256]{1,0:T(8,128)(2,1)S(1)} collective-permute-done((bf16[128,256]{1,0:T(8,128)(2,1)S(1)}, bf16[128,256]{1,0:T(8,128)(2,1)S(1)}, u32[]{:S(2)}, u32[]{:S(2)}) %collective-permute-start.6) | collective-permute-done | bytes 65568 | tf_op jit(solution)/shard_map/ppermute | solution.py:60
  118.8 0.0 collective-permute-done.7.refs_5_
  118.8 0.0 collective-permute-done.9.refs_7_
  118.8 4.5 %shard_map.151 = bf16[128,2048]{1,0:T(8,128)(2,1)} custom-call(s32[2]{0:T(128)S(1)} %pad_add_fusion.place, bf16[128,256]{1,0:T(8,128)(2,1)S(1)} %get-tuple-element.16.refs_0_, bf16[128,256]{1,0:T(8,128)(2,1)S(1)} %collective-permute-done.4.refs_1_, bf16[128,256]{1,0:T(8,128)(2,1)S(1)} %collective-permute-done.5.refs_2_, ...), custom_call_target="tpu_custom_call" | custom-call | flops 1250000000 | tf_op jit(solution)/shard_map/pallas_call | solution.py:35
  123.4 0.0 all-to-all-done.1
  123.4 0.0 copy-done.7
  123.4 2.6 %shard_map.154 = bf16[160,512]{1,0:T(8,128)(2,1)} custom-call(s32[2]{0:T(128)S(1)} %pad_add_fusion.place, s32[2,160]{1,0:T(2,128)S(1)} %get-tuple-element.20.slot_ref, f32[2,160]{1,0:T(2,128)S(1)} %bitcast.17, bf16[512,512]{1,0:T(8,128)(2,1)} %bitcast.10.refs_0_), custom_call_target="tpu_custom_call" | custom-call | flops 750000000 | tf_op jit(solution)/shard_map/pallas_call | solution.py:35
  (8 shorter events, 0.0 us)
Async XLA Ops:
  0.7 1.1 copy-start.1
  1.8 0.7 copy-start.6
  25.2 12.5 %collective-permute-start.11 = (bf16[512,512]{1,0:T(8,128)(2,1)S(1)}, bf16[512,512]{1,0:T(8,128)(2,1)S(1)}, u32[]{:S(2)}, u32[]{:S(2)}) collective-permute-start(bf16[512,512]{1,0:T(8,128)(2,1)S(1)} %bitcast.11), channel_id=1, source_target_pairs={{0,2},{1,3},{2,0},{3,1},{4,6},{5,7},{6,4},{7,5},{8,10},{9,11},{10,... | collective-permute-start | bytes 1572872 | tf_op jit(solution)/shard_map/ppermute | solution.py:60
  26.7 11.0 %collective-permute-start.10 = (bf16[512,512]{1,0:T(8,128)(2,1)S(1)}, bf16[512,512]{1,0:T(8,128)(2,1)S(1)}, u32[]{:S(2)}, u32[]{:S(2)}) collective-permute-start(bf16[512,512]{1,0:T(8,128)(2,1)S(1)} %bitcast.12), channel_id=1, source_target_pairs={{0,1},{1,0},{2,3},{3,2},{4,5},{5,4},{6,7},{7,6},{8,9},{9,8},{10,11... | collective-permute-start | bytes 1572872 | tf_op jit(solution)/shard_map/ppermute | solution.py:60
  37.7 1.9 %collective-permute-start.12 = (bf16[512,512]{1,0:T(8,128)(2,1)S(1)}, bf16[512,512]{1,0:T(8,128)(2,1)S(1)}, u32[]{:S(2)}, u32[]{:S(2)}) collective-permute-start(bf16[512,512]{1,0:T(8,128)(2,1)S(1)} %collective-permute-done.11.refs_2_), channel_id=1, source_target_pairs={{0,1},{1,0},{2,3},{3,2},{4,5},{5,4},{6,7},{7,6},{8,9},{9,8},{10,11... | collective-permute-start | bytes 1572872 | tf_op jit(solution)/shard_map/ppermute | solution.py:60
  39.6 0.7 copy-start.5
  40.3 16.3 %copy-start = (bf16[256,2048]{1,0:T(8,128)(2,1)S(1)}, bf16[256,2048]{1,0:T(8,128)(2,1)}, u32[]{:S(2)}) copy-start(bf16[256,2048]{1,0:T(8,128)(2,1)} %refs_4_.1) | copy-start | bytes 3145732
  40.3 19.8 %copy-start.2 = (bf16[512,256]{1,0:T(8,128)(2,1)S(1)}, bf16[512,256]{1,0:T(8,128)(2,1)}, u32[]{:S(2)}) copy-start(bf16[512,256]{1,0:T(8,128)(2,1)} %q_ref.1) | copy-start | bytes 786436
  40.3 19.8 %copy-start.3 = (bf16[512,256]{1,0:T(8,128)(2,1)S(1)}, bf16[512,256]{1,0:T(8,128)(2,1)}, u32[]{:S(2)}) copy-start(bf16[512,256]{1,0:T(8,128)(2,1)} %k_ref.1) | copy-start | bytes 786436
  40.3 19.8 %copy-start.4 = (bf16[512,256]{1,0:T(8,128)(2,1)S(1)}, bf16[512,256]{1,0:T(8,128)(2,1)}, u32[]{:S(2)}) copy-start(bf16[512,256]{1,0:T(8,128)(2,1)} %v_ref.1) | copy-start | bytes 786436
  40.3 19.8 %copy-start.8 = (f32[64]{0:T(128)S(1)}, f32[64]{0:T(128)}, u32[]{:S(2)}) copy-start(f32[64]{0:T(128)} %param.17) | copy-start | bytes 772
  40.4 19.8 %copy-start.9 = (f32[64]{0:T(128)S(1)}, f32[64]{0:T(128)}, u32[]{:S(2)}) copy-start(f32[64]{0:T(128)} %param.18) | copy-start | bytes 772
  40.4 19.8 %copy-start.10 = (f32[64,4096]{1,0:T(8,128)S(1)}, f32[64,4096]{1,0:T(8,128)}, u32[]{:S(2)}) copy-start(f32[64,4096]{1,0:T(8,128)} %constant.11.clone.table_ref) | copy-start | bytes 3145732
  56.5 2.0 %collective-permute-start.14 = (bf16[512,512]{1,0:T(8,128)(2,1)S(1)}, bf16[512,512]{1,0:T(8,128)(2,1)S(1)}, u32[]{:S(2)}, u32[]{:S(2)}) collective-permute-start(bf16[512,512]{1,0:T(8,128)(2,1)S(1)} %get-tuple-element.25), channel_id=1, source_target_pairs={{0,1},{1,0},{2,3},{3,2},{4,5},{5,4},{6,7},{7,6},{8,9},{9,8},{10,11... | collective-permute-start | bytes 1572872 | tf_op jit(solution)/shard_map/ppermute | solution.py:60
  56.7 26.0 %collective-permute-start.8 = (bf16[256,2048]{1,0:T(8,128)(2,1)S(1)}, bf16[256,2048]{1,0:T(8,128)(2,1)S(1)}, u32[]{:S(2)}, u32[]{:S(2)}) collective-permute-start(bf16[256,2048]{1,0:T(8,128)(2,1)S(1)} %copy-done), channel_id=1, source_target_pairs={{0,2},{1,3},{2,0},{3,1},{4,6},{5,7},{6,4},{7,5},{8,10},{9,11},{10,... | collective-permute-start | bytes 3145736 | tf_op jit(solution)/shard_map/ppermute | solution.py:60
  58.2 26.4 %collective-permute-start.13 = (bf16[512,512]{1,0:T(8,128)(2,1)S(1)}, bf16[512,512]{1,0:T(8,128)(2,1)S(1)}, u32[]{:S(2)}, u32[]{:S(2)}) collective-permute-start(bf16[512,512]{1,0:T(8,128)(2,1)S(1)} %get-tuple-element.23), channel_id=1, source_target_pairs={{0,1},{1,0},{2,3},{3,2},{4,5},{5,4},{6,7},{7,6},{8,9},{9,8},{10,11... | collective-permute-start | bytes 1572872 | tf_op jit(solution)/shard_map/ppermute | solution.py:60
  58.6 34.8 %collective-permute-start.15 = (bf16[512,512]{1,0:T(8,128)(2,1)S(1)}, bf16[512,512]{1,0:T(8,128)(2,1)S(1)}, u32[]{:S(2)}, u32[]{:S(2)}) collective-permute-start(bf16[512,512]{1,0:T(8,128)(2,1)S(1)} %add_convert_fusion.1), channel_id=1, source_target_pairs={{0,2},{1,3},{2,0},{3,1},{4,6},{5,7},{6,4},{7,5},{8,10},{9,11},{10,... | collective-permute-start | bytes 1572872 | tf_op jit(solution)/shard_map/ppermute | solution.py:60
  61.2 0.7 copy-start.11
  61.9 5.3 %collective-permute-start = (bf16[128,512]{1,0:T(8,128)(2,1)S(1)}, bf16[128,512]{1,0:T(8,128)(2,1)S(1)}, u32[]{:S(2)}, u32[]{:S(2)}) collective-permute-start(bf16[128,512]{1,0:T(8,128)(2,1)S(1)} %get-tuple-element.15), channel_id=1, source_target_pairs={{0,4},{4,0},{8,12},{12,8},{16,20},{20,16},{24,28},{28,24},{1,5},{5... | collective-permute-start | bytes 393224 | tf_op jit(solution)/shard_map/ppermute | solution.py:60
  63.4 55.5 %collective-permute-start.7 = (bf16[256,2048]{1,0:T(8,128)(2,1)S(1)}, bf16[256,2048]{1,0:T(8,128)(2,1)S(1)}, u32[]{:S(2)}, u32[]{:S(2)}) collective-permute-start(bf16[256,2048]{1,0:T(8,128)(2,1)S(1)} %copy-done), channel_id=1, source_target_pairs={{0,1},{1,0},{2,3},{3,2},{4,5},{5,4},{6,7},{7,6},{8,9},{9,8},{10,11... | collective-permute-start | bytes 3145736 | tf_op jit(solution)/shard_map/ppermute | solution.py:60
  67.2 31.5 %collective-permute-start.1 = (bf16[256,512]{1,0:T(8,128)(2,1)S(1)}, bf16[256,512]{1,0:T(8,128)(2,1)}, u32[]{:S(2)}, u32[]{:S(2)}) collective-permute-start(bf16[256,512]{1,0:T(8,128)(2,1)S(1)} %constant_dynamic-update-slice_fusion.refs_0_), channel_id=1, source_target_pairs={{0,16},{4,20},{8,24},{12,28},{16,0},{20,4},{24,8},{28,12},{1,17},{... | collective-permute-start | bytes 786440 | tf_op jit(solution)/shard_map/ppermute | solution.py:60
  82.7 16.0 %collective-permute-start.2 = (bf16[256,512]{1,0:T(8,128)(2,1)S(1)}, bf16[256,512]{1,0:T(8,128)(2,1)}, u32[]{:S(2)}, u32[]{:S(2)}) collective-permute-start(bf16[256,512]{1,0:T(8,128)(2,1)S(1)} %constant_dynamic-update-slice_fusion.refs_0_), channel_id=1, source_target_pairs={{0,24},{4,28},{8,16},{12,20},{16,8},{20,12},{24,0},{28,4},{1,25},{... | collective-permute-start | bytes 786440 | tf_op jit(solution)/shard_map/ppermute | solution.py:60
  84.5 14.2 %collective-permute-start.3 = (bf16[256,512]{1,0:T(8,128)(2,1)S(1)}, bf16[256,512]{1,0:T(8,128)(2,1)}, u32[]{:S(2)}, u32[]{:S(2)}) collective-permute-start(bf16[256,512]{1,0:T(8,128)(2,1)S(1)} %constant_dynamic-update-slice_fusion.refs_0_), channel_id=1, source_target_pairs={{0,8},{4,12},{8,0},{12,4},{16,24},{20,28},{24,16},{28,20},{1,9},{5... | collective-permute-start | bytes 786440 | tf_op jit(solution)/shard_map/ppermute | solution.py:60
  93.3 25.5 %collective-permute-start.9 = (bf16[256,2048]{1,0:T(8,128)(2,1)S(1)}, bf16[256,2048]{1,0:T(8,128)(2,1)}, u32[]{:S(2)}, u32[]{:S(2)}) collective-permute-start(bf16[256,2048]{1,0:T(8,128)(2,1)S(1)} %collective-permute-done.8.refs_6_), channel_id=1, source_target_pairs={{0,1},{1,0},{2,3},{3,2},{4,5},{5,4},{6,7},{7,6},{8,9},{9,8},{10,11... | collective-permute-start | bytes 3145736 | tf_op jit(solution)/shard_map/ppermute | solution.py:60
  94.3 29.0 %all-to-all-start.1 = ((bf16[8,64,512]{2,1,0:T(8,128)(2,1)}), bf16[8,64,512]{2,1,0:T(8,128)(2,1)}, u32[]{:S(2)}, u32[]{:S(2)}) async-start(bf16[8,64,512]{2,1,0:T(8,128)(2,1)} %bitcast.20), calls=%async_computation.1 | async-start | bytes 1048576 | tf_op jit(solution)/shard_map/all_to_all | solution.py:433
  98.7 1.0 copy-start.12
  112.7 10.7 %copy-start.7 = (f32[160,2]{0,1:T(2,128)S(1)}, f32[160,2]{0,1:T(2,128)}, u32[]{:S(2)}) copy-start(f32[160,2]{0,1:T(2,128)} %param.23) | copy-start | bytes 3844
  112.7 1.9 %collective-permute-start.4 = (bf16[128,256]{1,0:T(8,128)(2,1)S(1)}, bf16[128,256]{1,0:T(8,128)(2,1)S(1)}, u32[]{:S(2)}, u32[]{:S(2)}) collective-permute-start(bf16[128,256]{1,0:T(8,128)(2,1)S(1)} %get-tuple-element.17), channel_id=1, source_target_pairs={{0,1},{1,0},{2,3},{3,2},{4,5},{5,4},{6,7},{7,6},{8,9},{9,8},{10,11... | collective-permute-start | bytes 196616 | tf_op jit(solution)/shard_map/ppermute | solution.py:60
  113.0 4.3 %collective-permute-start.5 = (bf16[128,256]{1,0:T(8,128)(2,1)S(1)}, bf16[128,256]{1,0:T(8,128)(2,1)S(1)}, u32[]{:S(2)}, u32[]{:S(2)}) collective-permute-start(bf16[128,256]{1,0:T(8,128)(2,1)S(1)} %get-tuple-element.18), channel_id=1, source_target_pairs={{0,2},{1,3},{2,0},{3,1},{4,6},{5,7},{6,4},{7,5},{8,10},{9,11},{10,... | collective-permute-start | bytes 196616 | tf_op jit(solution)/shard_map/ppermute | solution.py:60
  114.6 4.3 %collective-permute-start.6 = (bf16[128,256]{1,0:T(8,128)(2,1)S(1)}, bf16[128,256]{1,0:T(8,128)(2,1)S(1)}, u32[]{:S(2)}, u32[]{:S(2)}) collective-permute-start(bf16[128,256]{1,0:T(8,128)(2,1)S(1)} %get-tuple-element.19), channel_id=1, source_target_pairs={{0,3},{1,2},{2,1},{3,0},{4,7},{5,6},{6,5},{7,4},{8,11},{9,10},{10,... | collective-permute-start | bytes 196616 | tf_op jit(solution)/shard_map/ppermute | solution.py:60
where the time goes:
time: 127 us; the launch traced here: 126 us
  waiting for transfers between devices  43.8 us (34%)
  Pallas kernels  38.3 us (30%)
  blocking collectives  21.6 us (17%)
  starting transfers between devices  16.2 us (13%)
  local copies, waits for them, and re-layouts  4.17 us (3%)
    ppermute x16, waiting for transfers between devices, send(): return lax.ppermute(x, axis, [(i, i ^ flip) for i in range(n)])  43.8 us
    pallas_call x6, Pallas kernels, call(): pl.pallas_call(body, grid_spec=pltpu.PrefetchScalarGridSpec(num_scalar_pr...  38.3 us
    all_to_all x1, blocking collectives, local(): lax.all_to_all(o, 'ep', split_axis=0, concat_axis=0, tiled=True)  21.6 us
    ppermute x16, starting transfers between devices, send(): return lax.ppermute(x, axis, [(i, i ^ flip) for i in range(n)])  11.8 us
    all_to_all x1, starting transfers between devices, local(): lax.all_to_all(r, 'ep', split_axis=0, concat_axis=0, tiled=True)  4.37 us
    unnamed x27, local copies, waits for them, and re-layouts  4.16 us
  transfers between devices with their start and end apart: 17, of which 8 were waited for; matrix products, arithmetic and copies ran while one was open for 1% of the time, Pallas kernels for 15%

commit v1 on v0

--- a/solution.py
+++ b/solution.py
@@ -20,7 +20,6 @@
 BF16 = jnp.bfloat16
 VMEM_LIMIT = 48 * 1024 * 1024
 FLOPS_PER_MICRO = 500_000_000
-CHUNKS = 1
 
 
 def full(shape):
@@ -60,8 +59,8 @@
     return lax.ppermute(x, axis, [(i, i ^ flip) for i in range(n)])
 
 
-def dispatch_body(place, routes_ref, x_hbm, *outs, experts, cap, chunks):
-    out_refs, slot_ref, x_ref, sem = outs[:chunks], *outs[chunks:]
+def dispatch_body(place, routes_ref, x_hbm, *outs, experts, cap):
+    out_ref, slot_ref, x_ref, sem = outs
     tokens, feat = x_ref.shape
     cols = pl.ds(pl.multiple_of(place[0] * feat, feat), feat)
     fetch = pltpu.make_async_copy(x_hbm.at[:, cols], x_ref, sem)
@@ -76,30 +75,26 @@
     before = (row < col).astype(F32).astype(BF16)
     count = mm(hits.astype(BF16), before)
     slot = jnp.where(hits > 0.5, count, -1.0).astype(jnp.int32)
-    part = cap // chunks
 
     def flat(choice, expert):
         at = jnp.sum(count * choice, axis=0, keepdims=True).astype(jnp.int32)
-        piece = sum([(at >= c * part).astype(jnp.int32) for c in range(1, chunks)], jnp.zeros_like(at))
-        return piece * (experts * part) + expert * part + at - piece * part
+        return (expert ^ place[1] ^ (experts // 2)) * cap + at
 
     slot_ref[0:1, :] = flat(first, routes[0:1, :])
     slot_ref[1:2, :] = flat(second, routes[1:2, :])
     fetch.wait()
     x = x_ref[...]
-    for c in range(chunks):
-        slots = lax.broadcasted_iota(jnp.int32, (part, tokens), 0) + c * part
-        for e in range(experts):
-            pick = (slots == slot[e : e + 1, :]).astype(F32).astype(BF16)
-            out_refs[c][e * part : (e + 1) * part, :] = mm(pick, x).astype(BF16)
-
-
-def dispatch(place, routes, expert_input, experts, cap, chunks, feat):
+    slots = lax.broadcasted_iota(jnp.int32, (cap, tokens), 0)
+    for e in range(experts):
+        pick = (slots == slot[e : e + 1, :]).astype(F32).astype(BF16)
+        out_ref[e * cap : (e + 1) * cap, :] = mm(pick, x).astype(BF16)
+
+
+def dispatch(place, routes, expert_input, experts, cap, feat):
     tokens = routes.shape[1]
-    outs = [jax.ShapeDtypeStruct((experts * cap // chunks, feat), BF16)] * chunks
-    outs += [jax.ShapeDtypeStruct((2, tokens), jnp.int32)]
-    return call(
-        functools.partial(dispatch_body, experts=experts, cap=cap, chunks=chunks),
+    outs = [jax.ShapeDtypeStruct((experts * cap, feat), BF16), jax.ShapeDtypeStruct((2, tokens), jnp.int32)]
+    return call(
+        functools.partial(dispatch_body, experts=experts, cap=cap),
         place,
         (routes, expert_input),
         [full(routes.shape), hbm()],
@@ -142,8 +137,37 @@
 
 
 def prep_body(
-    place, q_ref, k_ref, v_ref, q_gain_ref, k_gain_ref, table_ref, qt_ref, kvt_ref, turned_ref, *, heads, group
+    place,
+    q_hbm,
+    k_hbm,
+    v_hbm,
+    q_gain_ref,
+    k_gain_ref,
+    table_hbm,
+    qt_ref,
+    kvt_ref,
+    turned_ref,
+    q_ref,
+    k_ref,
+    v_ref,
+    table_ref,
+    sems,
+    *,
+    heads,
+    group,
 ):
+    rows = q_ref.shape[0]
+    cols = pl.ds(pl.multiple_of(place[1] * rows, rows), rows)
+    copies = [
+        pltpu.make_async_copy(src, dst, sems.at[i])
+        for i, (src, dst) in enumerate(
+            ((k_hbm, k_ref), (table_hbm.at[:, cols], table_ref), (v_hbm, v_ref), (q_hbm, q_ref))
+        )
+    ]
+    for c in copies:
+        c.start()
+    for c in copies:
+        c.wait()
     table = table_ref[...]
     q_gain = column(q_gain_ref[...])
     k_gain = column(k_gain_ref[...])
@@ -164,19 +188,26 @@
         place,
         (queries, key_input, value_input, q_gain, k_gain, table),
         [
-            full(queries.shape),
-            full(key_input.shape),
-            full(value_input.shape),
+            hbm(),
+            hbm(),
+            hbm(),
             full(q_gain.shape),
             full(k_gain.shape),
-            pl.BlockSpec((table.shape[0], rows), lambda i, place: (0, place[1])),
+            hbm(),
         ],
         [
             jax.ShapeDtypeStruct((queries.shape[1], rows), BF16),
             jax.ShapeDtypeStruct((2 * HD, rows), BF16),
         ],
-        scratch=[pltpu.VMEM((key_input.shape[1], rows), F32)],
-        micros=1.5,
+        scratch=[
+            pltpu.VMEM((key_input.shape[1], rows), F32),
+            pltpu.VMEM(queries.shape, BF16),
+            pltpu.VMEM(key_input.shape, BF16),
+            pltpu.VMEM(value_input.shape, BF16),
+            pltpu.VMEM((table.shape[0], rows), F32),
+            pltpu.SemaphoreType.DMA((4,)),
+        ],
+        micros=2.0,
     )
 
 
@@ -260,12 +291,14 @@
     )[0]
 
 
-def expert_body(place, *refs, groups, tile):
+def expert_body(place, *refs, groups, tile, experts):
     x_refs = refs[:groups]
     gain_ref, gate_hbm, up_hbm, down_hbm = refs[groups : groups + 4]
-    out_refs = refs[groups + 4 : 2 * groups + 4]
-    scaled_ref, hidden_ref, gate_ref, up_ref, down_ref, gate_sem, up_sem, down_sem = refs[2 * groups + 4 :]
-    feat = x_refs[0].shape[1]
+    out_refs = refs[groups + 4 : 3 * groups + 4]
+    scaled_ref, hidden_ref, gate_ref, up_ref, down_ref, gate_sem, up_sem, down_sem = refs[3 * groups + 4 :]
+    rows, feat = x_refs[0].shape
+    cap = rows // experts
+    half = rows // 2
     width = groups * feat
     steps = gate_ref.shape[0]
 
@@ -273,57 +306,65 @@
         return pl.ds(pl.multiple_of((place[0] ^ k) * feat, feat), feat)
 
     def fetch_gate(j):
-        cols = pl.ds(pl.multiple_of(j * tile, tile), tile)
+        cols = slice(j * tile, (j + 1) * tile)
         return pltpu.make_async_copy(gate_hbm.at[0, :, cols], gate_ref.at[j], gate_sem.at[j])
 
     def fetch_up(j):
-        cols = pl.ds(pl.multiple_of(j * tile, tile), tile)
+        cols = slice(j * tile, (j + 1) * tile)
         return pltpu.make_async_copy(up_hbm.at[0, :, cols], up_ref.at[j], up_sem.at[j])
 
     def fetch_down(k):
         return pltpu.make_async_copy(down_hbm.at[0, :, spot(k)], down_ref.at[k], down_sem.at[k])
 
+    fetch_gate(0).start()
+    fetch_up(0).start()
+    parts = []
+    for i in range(experts):
+        at = pl.multiple_of((place[1] ^ i ^ (experts // 2)) * cap, cap)
+        squares = 0.0
+        for k in range(groups):
+            x = x_refs[k][pl.ds(at, cap), :].astype(F32)
+            scaled_ref[i * cap : (i + 1) * cap, spot(k)] = (x * gain_ref[:, spot(k)]).astype(BF16)
+            squares += x * x
+        parts.append(jnp.sum(squares, axis=1, keepdims=True))
+    scale = lax.rsqrt(jnp.concatenate(parts, axis=0) / width + EPSILON)
+
+    waiting = list(range(groups))
+    share = -(-groups // steps)
+    started = []
     for j in range(steps):
-        fetch_gate(j).start()
-        fetch_up(j).start()
-    for k in range(groups):
-        fetch_down(k).start()
-
-    squares = 0.0
-    for k in range(groups):
-        x = x_refs[k][...].astype(F32)
-        scaled_ref[:, spot(k)] = (x * gain_ref[:, spot(k)]).astype(BF16)
-        squares += jnp.sum(x * x, axis=1, keepdims=True)
-    scale = lax.rsqrt(squares / width + EPSILON)
-
-    def one(j, carry):
+        if j + 1 < steps:
+            fetch_gate(j + 1).start()
+            fetch_up(j + 1).start()
+        for k in waiting[:share]:
+            fetch_down(k).start()
+            started.append(k)
+        waiting = waiting[share:]
         x = scaled_ref[...]
         fetch_gate(j).wait()
         gate = mm(x, gate_ref[j]) * scale
         fetch_up(j).wait()
         up = mm(x, up_ref[j]) * scale
-        cols = pl.ds(pl.multiple_of(j * tile, tile), tile)
-        hidden_ref[:, cols] = (gate / (1.0 + jnp.exp(-gate)) * up).astype(BF16)
-        return carry
-
-    lax.fori_loop(0, steps, one, 0)
+        hidden_ref[:, j * tile : (j + 1) * tile] = (gate / (1.0 + jnp.exp(-gate)) * up).astype(BF16)
     for k in range(groups):
         fetch_down(k).wait()
-        out_refs[k][...] = mm(hidden_ref[...], down_ref[k]).astype(BF16)
-
-
-def expert(place, xs, gain, gate, up, down):
+        part = mm(hidden_ref[...], down_ref[k]).astype(BF16)
+        out_refs[2 * k][...] = part[:half]
+        out_refs[2 * k + 1][...] = part[half:]
+
+
+def expert(place, xs, gain, gate, up, down, experts):
     groups = len(xs)
     rows, feat = xs[0].shape
     depth, ff = gate.shape[1:]
     tile = min(ff, 256)
     steps = ff // tile
     return call(
-        functools.partial(expert_body, groups=groups, tile=tile),
+        functools.partial(expert_body, groups=groups, tile=tile, experts=experts),
         place,
         (*xs, gain, gate, up, down),
         [full(x.shape) for x in xs] + [full(gain.shape), hbm(), hbm(), hbm()],
-        [jax.ShapeDtypeStruct((rows, feat), BF16)] * groups,
+        [jax.ShapeDtypeStruct((rows // 2, feat), BF16)] * (2 * groups),
         scratch=[
             pltpu.VMEM((rows, depth), BF16),
             pltpu.VMEM((rows, ff), BF16),
@@ -334,35 +375,59 @@
             pltpu.SemaphoreType.DMA((steps,)),
             pltpu.SemaphoreType.DMA((groups,)),
         ],
-        micros=9.0,
-    )
-
-
-def combine_body(place, slot_ref, scores_ref, *refs, chunks):
-    row_refs, out_ref = refs[:chunks], refs[chunks]
+        micros=11.0,
+    )
+
+
+def finish_body(place, *refs, terms):
+    total = 0.0
+    for r in refs[:terms]:
+        total += r[...].astype(F32)
+    total = total.astype(BF16)
+    outs = refs[terms:]
+    rows = outs[0].shape[0]
+    for i, o in enumerate(outs):
+        o[...] = total[i * rows : (i + 1) * rows]
+
+
+def finish(place, terms, pieces):
+    rows, feat = terms[0].shape
+    return call(
+        functools.partial(finish_body, terms=len(terms)),
+        place,
+        tuple(terms),
+        [full(t.shape) for t in terms],
+        [jax.ShapeDtypeStruct((rows // pieces, feat), BF16)] * pieces,
+        micros=0.5,
+    )
+
+
+def combine_body(place, slot_ref, scores_ref, *refs, blocks):
+    out_ref, rows_ref = refs[blocks:]
     tokens = out_ref.shape[0]
-    slots = row_refs[0].shape[0]
+    cap = refs[0].shape[0]
+    for i in range(blocks):
+        rows_ref[i * cap : (i + 1) * cap, :] = refs[i][...]
     scores = scores_ref[...]
     weight = scores / jnp.sum(scores, axis=0, keepdims=True)
     slot = slot_ref[...]
+    rows = lax.broadcasted_iota(jnp.int32, (blocks * cap, tokens), 0)
     total = jnp.zeros(out_ref.shape, F32)
     for k in range(2):
-        picked = jnp.zeros(out_ref.shape, F32)
-        for c in range(chunks):
-            rows = lax.broadcasted_iota(jnp.int32, (slots, tokens), 0) + c * slots
-            pick = (rows == slot[k : k + 1, :]).astype(F32).astype(BF16)
-            picked += mm(pick, row_refs[c][...], ((0,), (0,)))
-        total += picked * column(weight[k : k + 1, :])
+        pick = (rows == slot[k : k + 1, :]).astype(F32).astype(BF16)
+        total += mm(pick, rows_ref[...], ((0,), (0,))) * column(weight[k : k + 1, :])
     out_ref[...] = total.astype(BF16)
 
 
 def combine(place, slot, scores, rows):
-    return call(
-        functools.partial(combine_body, chunks=len(rows)),
+    cap, feat = rows[0].shape
+    return call(
+        functools.partial(combine_body, blocks=len(rows)),
         place,
         (slot, scores, *rows),
         [full(slot.shape), full(scores.shape)] + [full(r.shape) for r in rows],
-        [jax.ShapeDtypeStruct((slot.shape[1], rows[0].shape[1]), BF16)],
+        [jax.ShapeDtypeStruct((slot.shape[1], feat), BF16)],
+        scratch=[pltpu.VMEM((len(rows) * cap, feat), BF16)],
         micros=1.5,
     )[0]
 
@@ -390,47 +455,51 @@
     width = expert_input.shape[1]
     feat = width // n_tp
     cap = 3 * tokens * top // (2 * n_ep)
-    unit = 8 * CHUNKS
-    cap = -(-cap // unit) * unit
+    cap = -(-cap // 8) * 8
     place = jnp.stack([lax.axis_index("tp"), lax.axis_index("ep")]).astype(jnp.int32)
+    half = n_ep // 2
 
     weights = {0: mix_out_weight}
     for k in range(2, n_tp, 2):
         weights[k] = send(mix_out_weight, "tp", k)
-
-    *outbound, slot = dispatch(place, routes.T, expert_input, n_ep, cap, CHUNKS, feat)
-    arrived = [lax.all_to_all(o, "ep", split_axis=0, concat_axis=0, tiled=True) for o in outbound]
+    for k in range(0, n_tp, 2):
+        weights[k + 1] = send(weights[k], "tp", 1)
 
     qt, kvt = prep(
         place, queries, key_input, value_input, query_gain[None], key_gain[None], table, heads
     )
-    pair = jnp.concatenate([kvt, send(kvt, "ep", 1)], axis=0)
-    blocks = [pair] + [send(pair, "ep", k) for k in sorted(range(2, n_ep, 2), key=lambda k: k ^ (n_ep // 2))]
-
-    reduced = []
-    for a in arrived:
-        xs = {0: a}
-        for k in range(2, n_tp, 2):
-            xs[k] = send(a, "tp", k)
-        for k in range(0, n_tp, 2):
-            xs[k + 1] = send(xs[k], "tp", 1)
-        parts = expert(
-            place, [xs[k] for k in range(n_tp)], ffn_gain[None], gate_weight, up_weight, down_weight
-        )
-        other = {k: send(parts[k + 1], "tp", 1) for k in range(0, n_tp, 2)}
-        total = parts[0].astype(F32) + other[0].astype(F32)
-        for k in range(2, n_tp, 2):
-            both = (parts[k].astype(F32) + other[k].astype(F32)).astype(BF16)
-            total += send(both, "tp", k).astype(F32)
-        reduced.append(total.astype(BF16))
-
+    blocks = [kvt]
+    blocks += [send(kvt, "ep", k) for k in range(n_ep - 2, 0, -2)]
+    blocks.append(send(kvt, "ep", 1))
+    blocks += [send(b, "ep", 1) for b in blocks[1:half]]
+
+    outbound, slot = dispatch(place, routes.T, expert_input, n_ep, cap, feat)
+    arrived = lax.all_to_all(outbound, "ep", split_axis=0, concat_axis=0, tiled=True)
+    xs = {0: arrived}
+    for k in range(2, n_tp, 2):
+        xs[k] = send(arrived, "tp", k)
     for k in range(0, n_tp, 2):
-        weights[k + 1] = send(weights[k], "tp", 1)
+        xs[k + 1] = send(xs[k], "tp", 1)
+
     atts = attend(place, qt, blocks, heads, n_tp)
     atts = [atts[0]] + [send(atts[k], "tp", k) for k in range(1, n_tp)]
+
+    parts = expert(
+        place, [xs[k] for k in range(n_tp)], ffn_gain[None], gate_weight, up_weight, down_weight, n_ep
+    )
+    returned = []
+    for side in range(2):
+        mine = {k: (parts[2 * k + side], send(parts[2 * k + 2 + side], "tp", 1)) for k in range(0, n_tp, 2)}
+        terms = list(mine[0])
+        for k in range(2, n_tp, 2):
+            (both,) = finish(place, mine[k], 1)
+            terms.append(send(both, "tp", k))
+        pieces = finish(place, terms, half)
+        for i, piece in enumerate(pieces):
+            k = i ^ half if side == 0 else i
+            returned.append(send(piece, "ep", k) if k else piece)
+
     mixed = mix(place, atts, [weights[k] for k in range(n_tp)])
-
-    returned = [lax.all_to_all(r, "ep", split_axis=0, concat_axis=0, tiled=True) for r in reduced]
     out = combine(place, slot, route_scores.T, returned)
     return mixed, out
 

time: 127 us -> 132 us (1.039)
  starting transfers between devices: 16.2 us -> 30 us
  waiting for transfers between devices: 43.8 us -> 34.6 us
  local copies, waits for them, and re-layouts: 4.17 us -> 7.16 us
    ppermute x16 -> x29, starting transfers between devices: 11.8 us -> 30 us  [send(): return lax.ppermute(x, axis, [(i, i ^ flip) for i in range(n)])]
    ppermute x16 -> x29, waiting for transfers between devices: 43.8 us -> 34.6 us  [send(): return lax.ppermute(x, axis, [(i, i ^ flip) for i in range(n)])]
    all_to_all x1 -> x0, starting transfers between devices: 4.37 us -> none  [local(): lax.all_to_all(r, 'ep', split_axis=0, concat_axis=0, tiled=True)]
    unnamed x27 -> x22, local copies, waits for them, and re-layouts: 4.16 us -> 7.16 us
    pallas_call x6 -> x10, Pallas kernels: 38.3 us -> 37.1 us  [call(): pl.pallas_call(body, grid_spec=pltpu.PrefetchScalarGridSpec(num_scalar_pr...]
  transfers between devices with their start and end apart: 17 -> 29, of which waited for: 8 -> 9; matrix products, arithmetic and copies ran while one was open for 1% -> 0% of each run, Pallas kernels for 15% -> 26%
where the time goes in v1:
time: 132 us; the launch traced here: 131 us
  Pallas kernels  37.1 us (28%)
  waiting for transfers between devices  34.6 us (26%)
  starting transfers between devices  30 us (23%)
  blocking collectives  21.6 us (16%)
  local copies, waits for them, and re-layouts  7.16 us (5%)
    pallas_call x10, Pallas kernels, call(): pl.pallas_call(body, grid_spec=pltpu.PrefetchScalarGridSpec(num_scalar_pr...  37.1 us
    ppermute x29, waiting for transfers between devices, send(): return lax.ppermute(x, axis, [(i, i ^ flip) for i in range(n)])  34.6 us
    ppermute x29, starting transfers between devices, send(): return lax.ppermute(x, axis, [(i, i ^ flip) for i in range(n)])  30 us
    all_to_all x1, blocking collectives, local(): lax.all_to_all(outbound, 'ep', split_axis=0, concat_axis=0, tiled=True)  21.6 us
    unnamed x22, local copies, waits for them, and re-layouts  7.16 us
  transfers between devices with their start and end apart: 29, of which 9 were waited for; matrix products, arithmetic and copies ran while one was open for 0% of the time, Pallas kernels for 26%

profile of v1, /device:TPU:0, one launch (start us, length us, event | category | flops | bytes accessed | tf_op | source)
XLA Modules:
  0.0 131.4 jit_solution(2316942633594160569)
XLA Ops:
  0.6 0.1 pad_add_fusion.place
  0.7 1.1 copy-done.1
  1.8 0.7 copy-done.6
  2.5 1.1 shard_map.152
  3.6 21.6 %all_to_all.11 = bf16[8,64,512]{2,1,0:T(8,128)(2,1)S(1)} all-to-all(bf16[8,64,512]{2,1,0:T(8,128)(2,1)S(1)} %bitcast.12), channel_id=1, replica_groups=mesh['ep'=8,'tp'=4] {'ep'}, dimensions={0} | all-to-all | bytes 1048576 | tf_op jit(solution)/shard_map/all_to_all | solution.py:477
  25.2 1.5 %collective-permute-start.14 = (bf16[512,512]{1,0:T(8,128)(2,1)S(1)}, bf16[512,512]{1,0:T(8,128)(2,1)S(1)}, u32[]{:S(2)}, u32[]{:S(2)}) collective-permute-start(bf16[512,512]{1,0:T(8,128)(2,1)S(1)} %bitcast.9), channel_id=1, source_target_pairs={{0,2},{1,3},{2,0},{3,1},{4,6},{5,7},{6,4},{7,5},{8,10},{9,11},{10,... | collective-permute-start | bytes 1572872 | tf_op jit(solution)/shard_map/ppermute | solution.py:59
  26.7 0.5 collective-permute-start.11
  27.2 0.0 collective-permute-start.13
  27.2 12.8 %collective-permute-done.14.refs_2_ = bf16[512,512]{1,0:T(8,128)(2,1)S(1)} collective-permute-done((bf16[512,512]{1,0:T(8,128)(2,1)S(1)}, bf16[512,512]{1,0:T(8,128)(2,1)S(1)}, u32[]{:S(2)}, u32[]{:S(2)}) %collective-permute-start.14) | collective-permute-done | bytes 524320 | tf_op jit(solution)/shard_map/ppermute | solution.py:59
  40.0 0.0 collective-permute-start.15
  40.0 0.9 copy-done.2
  40.9 0.9 copy-done.3
  41.9 0.9 copy-done.4
  42.8 0.7 copy-done.8
  43.5 0.7 copy-done.9
  44.1 1.2 copy-done.10
  45.4 1.1 shard_map.149
  46.5 1.2 collective-permute-start
  47.7 1.4 %collective-permute-start.1 = (bf16[128,512]{1,0:T(8,128)(2,1)S(1)}, bf16[128,512]{1,0:T(8,128)(2,1)S(1)}, u32[]{:S(2)}, u32[]{:S(2)}) collective-permute-start(bf16[128,512]{1,0:T(8,128)(2,1)S(1)} %get-tuple-element.27.refs_0_), channel_id=1, source_target_pairs={{0,16},{4,20},{8,24},{12,28},{16,0},{20,4},{24,8},{28,12},{1,17},{... | collective-permute-start | bytes 393224 | tf_op jit(solution)/shard_map/ppermute | solution.py:59
  49.1 5.7 %collective-permute-done.refs_1_ = bf16[128,512]{1,0:T(8,128)(2,1)S(1)} collective-permute-done((bf16[128,512]{1,0:T(8,128)(2,1)S(1)}, bf16[128,512]{1,0:T(8,128)(2,1)S(1)}, u32[]{:S(2)}, u32[]{:S(2)}) %collective-permute-start) | collective-permute-done | bytes 131104 | tf_op jit(solution)/shard_map/ppermute | solution.py:59
  54.8 4.8 %collective-permute-start.2 = (bf16[128,512]{1,0:T(8,128)(2,1)S(1)}, bf16[128,512]{1,0:T(8,128)(2,1)S(1)}, u32[]{:S(2)}, u32[]{:S(2)}) collective-permute-start(bf16[128,512]{1,0:T(8,128)(2,1)S(1)} %get-tuple-element.27.refs_0_), channel_id=1, source_target_pairs={{0,8},{4,12},{8,0},{12,4},{16,24},{20,28},{24,16},{28,20},{1,9},{5... | collective-permute-start | bytes 393224 | tf_op jit(solution)/shard_map/ppermute | solution.py:59
  59.6 1.9 %collective-permute-done.1.refs_2_ = bf16[128,512]{1,0:T(8,128)(2,1)S(1)} collective-permute-done((bf16[128,512]{1,0:T(8,128)(2,1)S(1)}, bf16[128,512]{1,0:T(8,128)(2,1)S(1)}, u32[]{:S(2)}, u32[]{:S(2)}) %collective-permute-start.1) | collective-permute-done | bytes 131104 | tf_op jit(solution)/shard_map/ppermute | solution.py:59
  61.5 0.2 collective-permute-start.3
  61.7 2.5 %collective-permute-done.2.refs_3_ = bf16[128,512]{1,0:T(8,128)(2,1)S(1)} collective-permute-done((bf16[128,512]{1,0:T(8,128)(2,1)S(1)}, bf16[128,512]{1,0:T(8,128)(2,1)S(1)}, u32[]{:S(2)}, u32[]{:S(2)}) %collective-permute-start.2) | collective-permute-done | bytes 131104 | tf_op jit(solution)/shard_map/ppermute | solution.py:59
  64.2 2.0 %collective-permute-start.5 = (bf16[128,512]{1,0:T(8,128)(2,1)S(1)}, bf16[128,512]{1,0:T(8,128)(2,1)S(1)}, u32[]{:S(2)}, u32[]{:S(2)}) collective-permute-start(bf16[128,512]{1,0:T(8,128)(2,1)S(1)} %collective-permute-done.1.refs_2_), channel_id=1, source_target_pairs={{0,4},{4,0},{8,12},{12,8},{16,20},{20,16},{24,28},{28,24},{1,5},{5... | collective-permute-start | bytes 393224 | tf_op jit(solution)/shard_map/ppermute | solution.py:59
  66.2 0.0 collective-permute-done.15.refs_3_
  66.2 0.1 collective-permute-start.6
  66.3 15.7 %shard_map.153 = (bf16[256,512]{1,0:T(8,128)(2,1)S(1)}, bf16[256,512]{1,0:T(8,128)(2,1)S(1)}, bf16[256,512]{1,0:T(8,128)(2,1)S(1)}, bf16[256,512]{1,0:T(8,128)(2...) custom-call(s32[2]{0:T(128)S(1)} %pad_add_fusion.place, ...), custom_call_target="tpu_custom_call" | custom-call | flops 5500000256 | tf_op jit(solution)/shard_map/pallas_call | solution.py:34
  82.0 0.1 collective-permute-start.10
  82.1 0.0 collective-permute-done.11.refs_6_
  82.1 0.5 collective-permute-start.12
  82.6 0.0 collective-permute-done.4.refs_5_
  82.6 0.1 collective-permute-start.24
  82.7 12.0 %shard_map.150 = (bf16[128,256]{1,0:T(8,128)(2,1)S(1)}, bf16[128,256]{1,0:T(8,128)(2,1)S(1)}, bf16[128,256]{1,0:T(8,128)(2,1)S(1)}, bf16[128,256]{1,0:T(8,128)(2,1)S(1)}) custom-call(s32[2]{0:T(128)S(1)} %pad_add_fusion.place, bf16[256,512]{1,0:T(8,128)(2,1)S(1)} %get-tuple-element.26.qt_ref, bf16[128,512]{1,0:T(8,128)(2,1)S(1)} %get-tuple-element.27.refs_0_, ...), custom_call_target="tpu_custom_call" | custom-call | flops 6000000000 | tf_op jit(solution)/shard_map/pallas_call | solution.py:34
  94.8 0.5 collective-permute-start.7
  95.3 0.1 collective-permute-start.17
  95.3 0.8 collective-permute-done.7.refs_1_
  96.2 0.4 collective-permute-start.23
  96.5 1.5 %collective-permute-start.8 = (bf16[128,256]{1,0:T(8,128)(2,1)S(1)}, bf16[128,256]{1,0:T(8,128)(2,1)S(1)}, u32[]{:S(2)}, u32[]{:S(2)}) collective-permute-start(bf16[128,256]{1,0:T(8,128)(2,1)S(1)} %get-tuple-element.30), channel_id=1, source_target_pairs={{0,2},{1,3},{2,0},{3,1},{4,6},{5,7},{6,4},{7,5},{8,10},{9,11},{10,... | collective-permute-start | bytes 196616 | tf_op jit(solution)/shard_map/ppermute | solution.py:59
  98.0 0.6 shard_map.156
  98.6 2.1 %collective-permute-done.8.refs_2_ = bf16[128,256]{1,0:T(8,128)(2,1)S(1)} collective-permute-done((bf16[128,256]{1,0:T(8,128)(2,1)S(1)}, bf16[128,256]{1,0:T(8,128)(2,1)S(1)}, u32[]{:S(2)}, u32[]{:S(2)}) %collective-permute-start.8) | collective-permute-done | bytes 65568 | tf_op jit(solution)/shard_map/ppermute | solution.py:59
  100.8 1.5 %collective-permute-start.25 = (bf16[256,512]{1,0:T(8,128)(2,1)S(1)}, bf16[256,512]{1,0:T(8,128)(2,1)S(1)}, u32[]{:S(2)}, u32[]{:S(2)}) collective-permute-start(bf16[256,512]{1,0:T(8,128)(2,1)S(1)} %shard_map.156), channel_id=1, source_target_pairs={{0,2},{1,3},{2,0},{3,1},{4,6},{5,7},{6,4},{7,5},{8,10},{9,11},{10,... | collective-permute-start | bytes 786440 | tf_op jit(solution)/shard_map/ppermute | solution.py:59
  102.3 0.0 collective-permute-done.17.refs_1_
  102.3 0.6 shard_map.154
  102.9 0.0 collective-permute-done.23.refs_1_
  102.9 0.6 collective-permute-start.18
  103.5 6.4 %collective-permute-done.25.refs_2_ = bf16[256,512]{1,0:T(8,128)(2,1)S(1)} collective-permute-done((bf16[256,512]{1,0:T(8,128)(2,1)S(1)}, bf16[256,512]{1,0:T(8,128)(2,1)S(1)}, u32[]{:S(2)}, u32[]{:S(2)}) %collective-permute-start.25) | collective-permute-done | bytes 262176 | tf_op jit(solution)/shard_map/ppermute | solution.py:59
  109.9 0.6 shard_map.157
  110.6 0.0 collective-permute-done.16.refs_1_
  110.6 2.0 %collective-permute-start.26 = (bf16[64,512]{1,0:T(8,128)(2,1)S(1)}, bf16[64,512]{1,0:T(8,128)(2,1)S(1)}, u32[]{:S(2)}, u32[]{:S(2)}) collective-permute-start(bf16[64,512]{1,0:T(8,128)(2,1)S(1)} %get-tuple-element.47), channel_id=1, source_target_pairs={{0,4},{4,0},{8,12},{12,8},{16,20},{20,16},{24,28},{28,24},{1,5},{5... | collective-permute-start | bytes 196616 | tf_op jit(solution)/shard_map/ppermute | solution.py:59
  112.6 1.7 %collective-permute-done.18.refs_2_ = bf16[256,512]{1,0:T(8,128)(2,1)S(1)} collective-permute-done((bf16[256,512]{1,0:T(8,128)(2,1)S(1)}, bf16[256,512]{1,0:T(8,128)(2,1)S(1)}, u32[]{:S(2)}, u32[]{:S(2)}) %collective-permute-start.18) | collective-permute-done | bytes 262176 | tf_op jit(solution)/shard_map/ppermute | solution.py:59
  114.3 0.4 collective-permute-start.27
  114.7 0.6 shard_map.155
  115.3 0.0 collective-permute-done.9.refs_3_
  115.3 3.1 %collective-permute-start.28 = (bf16[64,512]{1,0:T(8,128)(2,1)S(1)}, bf16[64,512]{1,0:T(8,128)(2,1)S(1)}, u32[]{:S(2)}, u32[]{:S(2)}) collective-permute-start(bf16[64,512]{1,0:T(8,128)(2,1)S(1)} %get-tuple-element.49), channel_id=1, source_target_pairs={{0,12},{4,8},{8,4},{12,0},{16,28},{20,24},{24,20},{28,16},{1,13},{... | collective-permute-start | bytes 196616 | tf_op jit(solution)/shard_map/ppermute | solution.py:59
  118.4 0.4 collective-permute-start.19
  118.8 2.1 %collective-permute-start.20 = (bf16[64,512]{1,0:T(8,128)(2,1)S(1)}, bf16[64,512]{1,0:T(8,128)(2,1)S(1)}, u32[]{:S(2)}, u32[]{:S(2)}) collective-permute-start(bf16[64,512]{1,0:T(8,128)(2,1)S(1)} %get-tuple-element.39), channel_id=1, source_target_pairs={{0,20},{4,16},{8,28},{12,24},{16,4},{20,0},{24,12},{28,8},{1,21},{... | collective-permute-start | bytes 196616 | tf_op jit(solution)/shard_map/ppermute | solution.py:59
  120.9 1.4 %collective-permute-start.21 = (bf16[64,512]{1,0:T(8,128)(2,1)S(1)}, bf16[64,512]{1,0:T(8,128)(2,1)S(1)}, u32[]{:S(2)}, u32[]{:S(2)}) collective-permute-start(bf16[64,512]{1,0:T(8,128)(2,1)S(1)} %get-tuple-element.40), channel_id=1, source_target_pairs={{0,24},{4,28},{8,16},{12,20},{16,8},{20,12},{24,0},{28,4},{1,25},{... | collective-permute-start | bytes 196616 | tf_op jit(solution)/shard_map/ppermute | solution.py:59
  122.4 3.8 %collective-permute-start.22 = (bf16[64,512]{1,0:T(8,128)(2,1)S(1)}, bf16[64,512]{1,0:T(8,128)(2,1)S(1)}, u32[]{:S(2)}, u32[]{:S(2)}) collective-permute-start(bf16[64,512]{1,0:T(8,128)(2,1)S(1)} %get-tuple-element.41), channel_id=1, source_target_pairs={{0,28},{4,24},{8,20},{12,16},{16,12},{20,8},{24,4},{28,0},{1,29},{... | collective-permute-start | bytes 196616 | tf_op jit(solution)/shard_map/ppermute | solution.py:59
  126.1 3.1 %shard_map.151 = bf16[128,2048]{1,0:T(8,128)(2,1)} custom-call(s32[2]{0:T(128)S(1)} %pad_add_fusion.place, bf16[128,256]{1,0:T(8,128)(2,1)S(1)} %get-tuple-element.28.refs_0_, bf16[128,256]{1,0:T(8,128)(2,1)S(1)} %collective-permute-done.7.refs_1_, bf16[128,256]{1,0:T(8,128)(2,1)S(1)} %collective-permute-done.8.refs_2_, ...), custom_call_target="tpu_custom_call" | custom-call | flops 1250000000 | tf_op jit(solution)/shard_map/pallas_call | solution.py:34
  129.2 0.0 collective-permute-done.19.refs_0_
  129.2 0.6 collective-permute-done.20.refs_1_
  129.8 0.0 collective-permute-done.21.refs_2_
  129.8 1.6 %shard_map.158 = bf16[160,512]{1,0:T(8,128)(2,1)} custom-call(s32[2]{0:T(128)S(1)} %pad_add_fusion.place, s32[2,160]{1,0:T(2,128)S(1)} %get-tuple-element.32.slot_ref, f32[2,160]{1,0:T(2,128)S(1)} %bitcast.15, bf16[64,512]{1,0:T(8,128)(2,1)S(1)} %collective-permute-done.19.refs_0_, bf16[64,512]{1,0:T(8,128)(2,1)S(1)} %collective-permute-done.20.refs_1_, ...), custom_call_target="tpu_custom_call" | custom-call | flops 750000000 | tf_op jit(solution)/shard_map/pallas_call | solution.py:34
  (28 shorter events, 0.1 us)
Async XLA Ops:
  0.6 65.7 %copy-start.5 = (f32[2048]{0:T(1024)S(1)}, f32[2048]{0:T(1024)}, u32[]{:S(2)}) copy-start(f32[2048]{0:T(1024)} %param.21) | copy-start | bytes 24580
  0.7 1.1 copy-start.1
  1.8 0.7 copy-start.6
  25.2 14.8 %collective-permute-start.14 = (bf16[512,512]{1,0:T(8,128)(2,1)S(1)}, bf16[512,512]{1,0:T(8,128)(2,1)S(1)}, u32[]{:S(2)}, u32[]{:S(2)}) collective-permute-start(bf16[512,512]{1,0:T(8,128)(2,1)S(1)} %bitcast.9), channel_id=1, source_target_pairs={{0,2},{1,3},{2,0},{3,1},{4,6},{5,7},{6,4},{7,5},{8,10},{9,11},{10,... | collective-permute-start | bytes 1572872 | tf_op jit(solution)/shard_map/ppermute | solution.py:59
  26.7 55.4 %collective-permute-start.11 = (bf16[256,2048]{1,0:T(8,128)(2,1)}, bf16[256,2048]{1,0:T(8,128)(2,1)S(1)}, u32[]{:S(2)}, u32[]{:S(2)}) collective-permute-start(bf16[256,2048]{1,0:T(8,128)(2,1)} %refs_4_.1), channel_id=1, source_target_pairs={{0,2},{1,3},{2,0},{3,1},{4,6},{5,7},{6,4},{7,5},{8,10},{9,11},{10,... | collective-permute-start | bytes 3145736 | tf_op jit(solution)/shard_map/ppermute | solution.py:59
  27.2 37.0 %collective-permute-start.13 = (bf16[512,512]{1,0:T(8,128)(2,1)S(1)}, bf16[512,512]{1,0:T(8,128)(2,1)S(1)}, u32[]{:S(2)}, u32[]{:S(2)}) collective-permute-start(bf16[512,512]{1,0:T(8,128)(2,1)S(1)} %bitcast.10), channel_id=1, source_target_pairs={{0,1},{1,0},{2,3},{3,2},{4,5},{5,4},{6,7},{7,6},{8,9},{9,8},{10,11... | collective-permute-start | bytes 1572872 | tf_op jit(solution)/shard_map/ppermute | solution.py:59
  40.0 26.3 %collective-permute-start.15 = (bf16[512,512]{1,0:T(8,128)(2,1)S(1)}, bf16[512,512]{1,0:T(8,128)(2,1)S(1)}, u32[]{:S(2)}, u32[]{:S(2)}) collective-permute-start(bf16[512,512]{1,0:T(8,128)(2,1)S(1)} %collective-permute-done.14.refs_2_), channel_id=1, source_target_pairs={{0,1},{1,0},{2,3},{3,2},{4,5},{5,4},{6,7},{7,6},{8,9},{9,8},{10,11... | collective-permute-start | bytes 1572872 | tf_op jit(solution)/shard_map/ppermute | solution.py:59
  40.0 1.0 copy-start.2
  40.9 0.9 copy-start.3
  41.9 0.9 copy-start.4
  42.8 0.7 copy-start.8
  43.5 0.7 copy-start.9
  44.1 1.2 copy-start.10
  46.5 8.3 %collective-permute-start = (bf16[128,512]{1,0:T(8,128)(2,1)S(1)}, bf16[128,512]{1,0:T(8,128)(2,1)S(1)}, u32[]{:S(2)}, u32[]{:S(2)}) collective-permute-start(bf16[128,512]{1,0:T(8,128)(2,1)S(1)} %get-tuple-element.27.refs_0_), channel_id=1, source_target_pairs={{0,24},{4,28},{8,16},{12,20},{16,8},{20,12},{24,0},{28,4},{1,25},{... | collective-permute-start | bytes 393224 | tf_op jit(solution)/shard_map/ppermute | solution.py:59
  47.7 13.8 %collective-permute-start.1 = (bf16[128,512]{1,0:T(8,128)(2,1)S(1)}, bf16[128,512]{1,0:T(8,128)(2,1)S(1)}, u32[]{:S(2)}, u32[]{:S(2)}) collective-permute-start(bf16[128,512]{1,0:T(8,128)(2,1)S(1)} %get-tuple-element.27.refs_0_), channel_id=1, source_target_pairs={{0,16},{4,20},{8,24},{12,28},{16,0},{20,4},{24,8},{28,12},{1,17},{... | collective-permute-start | bytes 393224 | tf_op jit(solution)/shard_map/ppermute | solution.py:59
  54.8 9.4 %collective-permute-start.2 = (bf16[128,512]{1,0:T(8,128)(2,1)S(1)}, bf16[128,512]{1,0:T(8,128)(2,1)S(1)}, u32[]{:S(2)}, u32[]{:S(2)}) collective-permute-start(bf16[128,512]{1,0:T(8,128)(2,1)S(1)} %get-tuple-element.27.refs_0_), channel_id=1, source_target_pairs={{0,8},{4,12},{8,0},{12,4},{16,24},{20,28},{24,16},{28,20},{1,9},{5... | collective-permute-start | bytes 393224 | tf_op jit(solution)/shard_map/ppermute | solution.py:59
  61.5 20.5 %collective-permute-start.3 = (bf16[128,512]{1,0:T(8,128)(2,1)S(1)}, bf16[128,512]{1,0:T(8,128)(2,1)S(1)}, u32[]{:S(2)}, u32[]{:S(2)}) collective-permute-start(bf16[128,512]{1,0:T(8,128)(2,1)S(1)} %get-tuple-element.27.refs_0_), channel_id=1, source_target_pairs={{0,4},{4,0},{8,12},{12,8},{16,20},{20,16},{24,28},{28,24},{1,5},{5... | collective-permute-start | bytes 393224 | tf_op jit(solution)/shard_map/ppermute | solution.py:59
  64.2 18.4 %collective-permute-start.4 = (bf16[128,512]{1,0:T(8,128)(2,1)S(1)}, bf16[128,512]{1,0:T(8,128)(2,1)S(1)}, u32[]{:S(2)}, u32[]{:S(2)}) collective-permute-start(bf16[128,512]{1,0:T(8,128)(2,1)S(1)} %collective-permute-done.refs_1_), channel_id=1, source_target_pairs={{0,4},{4,0},{8,12},{12,8},{16,20},{20,16},{24,28},{28,24},{1,5},{5... | collective-permute-start | bytes 393224 | tf_op jit(solution)/shard_map/ppermute | solution.py:59
  64.2 18.5 %collective-permute-start.5 = (bf16[128,512]{1,0:T(8,128)(2,1)S(1)}, bf16[128,512]{1,0:T(8,128)(2,1)S(1)}, u32[]{:S(2)}, u32[]{:S(2)}) collective-permute-start(bf16[128,512]{1,0:T(8,128)(2,1)S(1)} %collective-permute-done.1.refs_2_), channel_id=1, source_target_pairs={{0,4},{4,0},{8,12},{12,8},{16,20},{20,16},{24,28},{28,24},{1,5},{5... | collective-permute-start | bytes 393224 | tf_op jit(solution)/shard_map/ppermute | solution.py:59
  66.2 16.5 %collective-permute-start.6 = (bf16[128,512]{1,0:T(8,128)(2,1)S(1)}, bf16[128,512]{1,0:T(8,128)(2,1)S(1)}, u32[]{:S(2)}, u32[]{:S(2)}) collective-permute-start(bf16[128,512]{1,0:T(8,128)(2,1)S(1)} %collective-permute-done.2.refs_3_), channel_id=1, source_target_pairs={{0,4},{4,0},{8,12},{12,8},{16,20},{20,16},{24,28},{28,24},{1,5},{5... | collective-permute-start | bytes 393224 | tf_op jit(solution)/shard_map/ppermute | solution.py:59
  66.3 15.7 %copy-start = (bf16[256,2048]{1,0:T(8,128)(2,1)S(1)}, bf16[256,2048]{1,0:T(8,128)(2,1)}, u32[]{:S(2)}) copy-start(bf16[256,2048]{1,0:T(8,128)(2,1)} %refs_4_.1) | copy-start | bytes 3145732
  82.0 36.4 %collective-permute-start.10 = (bf16[256,2048]{1,0:T(8,128)(2,1)S(1)}, bf16[256,2048]{1,0:T(8,128)(2,1)S(1)}, u32[]{:S(2)}, u32[]{:S(2)}) collective-permute-start(bf16[256,2048]{1,0:T(8,128)(2,1)S(1)} %copy-done), channel_id=1, source_target_pairs={{0,1},{1,0},{2,3},{3,2},{4,5},{5,4},{6,7},{7,6},{8,9},{9,8},{10,11... | collective-permute-start | bytes 3145736 | tf_op jit(solution)/shard_map/ppermute | solution.py:59
  82.1 36.7 %collective-permute-start.12 = (bf16[256,2048]{1,0:T(8,128)(2,1)S(1)}, bf16[256,2048]{1,0:T(8,128)(2,1)S(1)}, u32[]{:S(2)}, u32[]{:S(2)}) collective-permute-start(bf16[256,2048]{1,0:T(8,128)(2,1)S(1)} %collective-permute-done.11.refs_6_), channel_id=1, source_target_pairs={{0,1},{1,0},{2,3},{3,2},{4,5},{5,4},{6,7},{7,6},{8,9},{9,8},{10,11... | collective-permute-start | bytes 3145736 | tf_op jit(solution)/shard_map/ppermute | solution.py:59
  82.6 13.9 %collective-permute-start.24 = (bf16[256,512]{1,0:T(8,128)(2,1)S(1)}, bf16[256,512]{1,0:T(8,128)(2,1)S(1)}, u32[]{:S(2)}, u32[]{:S(2)}) collective-permute-start(bf16[256,512]{1,0:T(8,128)(2,1)S(1)} %get-tuple-element.45), channel_id=1, source_target_pairs={{0,1},{1,0},{2,3},{3,2},{4,5},{5,4},{6,7},{7,6},{8,9},{9,8},{10,11... | collective-permute-start | bytes 786440 | tf_op jit(solution)/shard_map/ppermute | solution.py:59
  94.8 1.4 %collective-permute-start.7 = (bf16[128,256]{1,0:T(8,128)(2,1)S(1)}, bf16[128,256]{1,0:T(8,128)(2,1)S(1)}, u32[]{:S(2)}, u32[]{:S(2)}) collective-permute-start(bf16[128,256]{1,0:T(8,128)(2,1)S(1)} %get-tuple-element.29), channel_id=1, source_target_pairs={{0,1},{1,0},{2,3},{3,2},{4,5},{5,4},{6,7},{7,6},{8,9},{9,8},{10,11... | collective-permute-start | bytes 196616 | tf_op jit(solution)/shard_map/ppermute | solution.py:59
  95.3 7.0 %collective-permute-start.17 = (bf16[256,512]{1,0:T(8,128)(2,1)S(1)}, bf16[256,512]{1,0:T(8,128)(2,1)S(1)}, u32[]{:S(2)}, u32[]{:S(2)}) collective-permute-start(bf16[256,512]{1,0:T(8,128)(2,1)S(1)} %get-tuple-element.37), channel_id=1, source_target_pairs={{0,1},{1,0},{2,3},{3,2},{4,5},{5,4},{6,7},{7,6},{8,9},{9,8},{10,11... | collective-permute-start | bytes 786440 | tf_op jit(solution)/shard_map/ppermute | solution.py:59
  96.2 6.8 %collective-permute-start.23 = (bf16[256,512]{1,0:T(8,128)(2,1)S(1)}, bf16[256,512]{1,0:T(8,128)(2,1)S(1)}, u32[]{:S(2)}, u32[]{:S(2)}) collective-permute-start(bf16[256,512]{1,0:T(8,128)(2,1)S(1)} %get-tuple-element.43), channel_id=1, source_target_pairs={{0,1},{1,0},{2,3},{3,2},{4,5},{5,4},{6,7},{7,6},{8,9},{9,8},{10,11... | collective-permute-start | bytes 786440 | tf_op jit(solution)/shard_map/ppermute | solution.py:59
  96.5 4.3 %collective-permute-start.8 = (bf16[128,256]{1,0:T(8,128)(2,1)S(1)}, bf16[128,256]{1,0:T(8,128)(2,1)S(1)}, u32[]{:S(2)}, u32[]{:S(2)}) collective-permute-start(bf16[128,256]{1,0:T(8,128)(2,1)S(1)} %get-tuple-element.30), channel_id=1, source_target_pairs={{0,2},{1,3},{2,0},{3,1},{4,6},{5,7},{6,4},{7,5},{8,10},{9,11},{10,... | collective-permute-start | bytes 196616 | tf_op jit(solution)/shard_map/ppermute | solution.py:59
  98.0 31.8 %copy-start.7 = (f32[160,2]{0,1:T(2,128)S(1)}, f32[160,2]{0,1:T(2,128)}, u32[]{:S(2)}) copy-start(f32[160,2]{0,1:T(2,128)} %param.23) | copy-start | bytes 3844
  100.8 9.1 %collective-permute-start.25 = (bf16[256,512]{1,0:T(8,128)(2,1)S(1)}, bf16[256,512]{1,0:T(8,128)(2,1)S(1)}, u32[]{:S(2)}, u32[]{:S(2)}) collective-permute-start(bf16[256,512]{1,0:T(8,128)(2,1)S(1)} %shard_map.156), channel_id=1, source_target_pairs={{0,2},{1,3},{2,0},{3,1},{4,6},{5,7},{6,4},{7,5},{8,10},{9,11},{10,... | collective-permute-start | bytes 786440 | tf_op jit(solution)/shard_map/ppermute | solution.py:59
  102.3 8.3 %collective-permute-start.16 = (bf16[256,512]{1,0:T(8,128)(2,1)S(1)}, bf16[256,512]{1,0:T(8,128)(2,1)S(1)}, u32[]{:S(2)}, u32[]{:S(2)}) collective-permute-start(bf16[256,512]{1,0:T(8,128)(2,1)S(1)} %get-tuple-element.35), channel_id=1, source_target_pairs={{0,1},{1,0},{2,3},{3,2},{4,5},{5,4},{6,7},{7,6},{8,9},{9,8},{10,11... | collective-permute-start | bytes 786440 | tf_op jit(solution)/shard_map/ppermute | solution.py:59
  102.9 11.4 %collective-permute-start.18 = (bf16[256,512]{1,0:T(8,128)(2,1)S(1)}, bf16[256,512]{1,0:T(8,128)(2,1)S(1)}, u32[]{:S(2)}, u32[]{:S(2)}) collective-permute-start(bf16[256,512]{1,0:T(8,128)(2,1)S(1)} %shard_map.154), channel_id=1, source_target_pairs={{0,2},{1,3},{2,0},{3,1},{4,6},{5,7},{6,4},{7,5},{8,10},{9,11},{10,... | collective-permute-start | bytes 786440 | tf_op jit(solution)/shard_map/ppermute | solution.py:59
  109.9 5.4 %collective-permute-start.9 = (bf16[128,256]{1,0:T(8,128)(2,1)S(1)}, bf16[128,256]{1,0:T(8,128)(2,1)S(1)}, u32[]{:S(2)}, u32[]{:S(2)}) collective-permute-start(bf16[128,256]{1,0:T(8,128)(2,1)S(1)} %get-tuple-element.31), channel_id=1, source_target_pairs={{0,3},{1,2},{2,1},{3,0},{4,7},{5,6},{6,5},{7,4},{8,11},{9,10},{10,... | collective-permute-start | bytes 196616 | tf_op jit(solution)/shard_map/ppermute | solution.py:59
  110.6 10.3 %collective-permute-start.26 = (bf16[64,512]{1,0:T(8,128)(2,1)S(1)}, bf16[64,512]{1,0:T(8,128)(2,1)S(1)}, u32[]{:S(2)}, u32[]{:S(2)}) collective-permute-start(bf16[64,512]{1,0:T(8,128)(2,1)S(1)} %get-tuple-element.47), channel_id=1, source_target_pairs={{0,4},{4,0},{8,12},{12,8},{16,20},{20,16},{24,28},{28,24},{1,5},{5... | collective-permute-start | bytes 196616 | tf_op jit(solution)/shard_map/ppermute | solution.py:59
  114.3 8.0 %collective-permute-start.27 = (bf16[64,512]{1,0:T(8,128)(2,1)S(1)}, bf16[64,512]{1,0:T(8,128)(2,1)S(1)}, u32[]{:S(2)}, u32[]{:S(2)}) collective-permute-start(bf16[64,512]{1,0:T(8,128)(2,1)S(1)} %get-tuple-element.48), channel_id=1, source_target_pairs={{0,8},{4,12},{8,0},{12,4},{16,24},{20,28},{24,16},{28,20},{1,9},{5... | collective-permute-start | bytes 196616 | tf_op jit(solution)/shard_map/ppermute | solution.py:59
  115.3 13.8 %collective-permute-start.28 = (bf16[64,512]{1,0:T(8,128)(2,1)S(1)}, bf16[64,512]{1,0:T(8,128)(2,1)S(1)}, u32[]{:S(2)}, u32[]{:S(2)}) collective-permute-start(bf16[64,512]{1,0:T(8,128)(2,1)S(1)} %get-tuple-element.49), channel_id=1, source_target_pairs={{0,12},{4,8},{8,4},{12,0},{16,28},{20,24},{24,20},{28,16},{1,13},{... | collective-permute-start | bytes 196616 | tf_op jit(solution)/shard_map/ppermute | solution.py:59
  118.4 10.7 %collective-permute-start.19 = (bf16[64,512]{1,0:T(8,128)(2,1)S(1)}, bf16[64,512]{1,0:T(8,128)(2,1)S(1)}, u32[]{:S(2)}, u32[]{:S(2)}) collective-permute-start(bf16[64,512]{1,0:T(8,128)(2,1)S(1)} %get-tuple-element.38), channel_id=1, source_target_pairs={{0,16},{4,20},{8,24},{12,28},{16,0},{20,4},{24,8},{28,12},{1,17},{... | collective-permute-start | bytes 196616 | tf_op jit(solution)/shard_map/ppermute | solution.py:59
  118.8 11.0 %collective-permute-start.20 = (bf16[64,512]{1,0:T(8,128)(2,1)S(1)}, bf16[64,512]{1,0:T(8,128)(2,1)S(1)}, u32[]{:S(2)}, u32[]{:S(2)}) collective-permute-start(bf16[64,512]{1,0:T(8,128)(2,1)S(1)} %get-tuple-element.39), channel_id=1, source_target_pairs={{0,20},{4,16},{8,28},{12,24},{16,4},{20,0},{24,12},{28,8},{1,21},{... | collective-permute-start | bytes 196616 | tf_op jit(solution)/shard_map/ppermute | solution.py:59
  120.9 8.9 %collective-permute-start.21 = (bf16[64,512]{1,0:T(8,128)(2,1)S(1)}, bf16[64,512]{1,0:T(8,128)(2,1)S(1)}, u32[]{:S(2)}, u32[]{:S(2)}) collective-permute-start(bf16[64,512]{1,0:T(8,128)(2,1)S(1)} %get-tuple-element.40), channel_id=1, source_target_pairs={{0,24},{4,28},{8,16},{12,20},{16,8},{20,12},{24,0},{28,4},{1,25},{... | collective-permute-start | bytes 196616 | tf_op jit(solution)/shard_map/ppermute | solution.py:59
  122.4 7.4 %collective-permute-start.22 = (bf16[64,512]{1,0:T(8,128)(2,1)S(1)}, bf16[64,512]{1,0:T(8,128)(2,1)S(1)}, u32[]{:S(2)}, u32[]{:S(2)}) collective-permute-start(bf16[64,512]{1,0:T(8,128)(2,1)S(1)} %get-tuple-element.41), channel_id=1, source_target_pairs={{0,28},{4,24},{8,20},{12,16},{16,12},{20,8},{24,4},{28,0},{1,29},{... | collective-permute-start | bytes 196616 | tf_op jit(solution)/shard_map/ppermute | solution.py:59

commit v2 on v1

--- a/solution.py
+++ b/solution.py
@@ -18,7 +18,7 @@
 LOG2E = 1.4426950408889634
 F32 = jnp.float32
 BF16 = jnp.bfloat16
-VMEM_LIMIT = 48 * 1024 * 1024
+VMEM_LIMIT = 24 * 1024 * 1024
 FLOPS_PER_MICRO = 500_000_000
 
 
@@ -28,6 +28,10 @@
 
 def hbm():
     return pl.BlockSpec(memory_space=pltpu.HBM)
+
+
+def far_memory(x):
+    return pltpu.with_memory_space_constraint(x, pltpu.HBM)
 
 
 def call(body, place, args, in_specs, outs, grid=(1,), scratch=(), out_specs=None, micros=1.0):
@@ -293,31 +297,17 @@
 
 def expert_body(place, *refs, groups, tile, experts):
     x_refs = refs[:groups]
-    gain_ref, gate_hbm, up_hbm, down_hbm = refs[groups : groups + 4]
+    gain_ref, gate_ref, up_ref, down_ref = refs[groups : groups + 4]
     out_refs = refs[groups + 4 : 3 * groups + 4]
-    scaled_ref, hidden_ref, gate_ref, up_ref, down_ref, gate_sem, up_sem, down_sem = refs[3 * groups + 4 :]
+    scaled_ref, hidden_ref = refs[3 * groups + 4 :]
     rows, feat = x_refs[0].shape
     cap = rows // experts
     half = rows // 2
     width = groups * feat
-    steps = gate_ref.shape[0]
 
     def spot(k):
         return pl.ds(pl.multiple_of((place[0] ^ k) * feat, feat), feat)
 
-    def fetch_gate(j):
-        cols = slice(j * tile, (j + 1) * tile)
-        return pltpu.make_async_copy(gate_hbm.at[0, :, cols], gate_ref.at[j], gate_sem.at[j])
-
-    def fetch_up(j):
-        cols = slice(j * tile, (j + 1) * tile)
-        return pltpu.make_async_copy(up_hbm.at[0, :, cols], up_ref.at[j], up_sem.at[j])
-
-    def fetch_down(k):
-        return pltpu.make_async_copy(down_hbm.at[0, :, spot(k)], down_ref.at[k], down_sem.at[k])
-
-    fetch_gate(0).start()
-    fetch_up(0).start()
     parts = []
     for i in range(experts):
         at = pl.multiple_of((place[1] ^ i ^ (experts // 2)) * cap, cap)
@@ -329,26 +319,14 @@
         parts.append(jnp.sum(squares, axis=1, keepdims=True))
     scale = lax.rsqrt(jnp.concatenate(parts, axis=0) / width + EPSILON)
 
-    waiting = list(range(groups))
-    share = -(-groups // steps)
-    started = []
-    for j in range(steps):
-        if j + 1 < steps:
-            fetch_gate(j + 1).start()
-            fetch_up(j + 1).start()
-        for k in waiting[:share]:
-            fetch_down(k).start()
-            started.append(k)
-        waiting = waiting[share:]
+    for j in range(gate_ref.shape[1] // tile):
         x = scaled_ref[...]
-        fetch_gate(j).wait()
-        gate = mm(x, gate_ref[j]) * scale
-        fetch_up(j).wait()
-        up = mm(x, up_ref[j]) * scale
-        hidden_ref[:, j * tile : (j + 1) * tile] = (gate / (1.0 + jnp.exp(-gate)) * up).astype(BF16)
+        cols = slice(j * tile, (j + 1) * tile)
+        gate = mm(x, gate_ref[:, cols]) * scale
+        up = mm(x, up_ref[:, cols]) * scale
+        hidden_ref[:, cols] = (gate / (1.0 + jnp.exp(-gate)) * up).astype(BF16)
     for k in range(groups):
-        fetch_down(k).wait()
-        part = mm(hidden_ref[...], down_ref[k]).astype(BF16)
+        part = mm(hidden_ref[...], down_ref[:, spot(k)]).astype(BF16)
         out_refs[2 * k][...] = part[:half]
         out_refs[2 * k + 1][...] = part[half:]
 
@@ -356,26 +334,17 @@
 def expert(place, xs, gain, gate, up, down, experts):
     groups = len(xs)
     rows, feat = xs[0].shape
-    depth, ff = gate.shape[1:]
+    depth, ff = gate.shape
     tile = min(ff, 256)
-    steps = ff // tile
+    vmem = pl.BlockSpec(memory_space=pltpu.VMEM)
     return call(
         functools.partial(expert_body, groups=groups, tile=tile, experts=experts),
         place,
         (*xs, gain, gate, up, down),
-        [full(x.shape) for x in xs] + [full(gain.shape), hbm(), hbm(), hbm()],
+        [full(x.shape) for x in xs] + [full(gain.shape), vmem, vmem, vmem],
         [jax.ShapeDtypeStruct((rows // 2, feat), BF16)] * (2 * groups),
-        scratch=[
-            pltpu.VMEM((rows, depth), BF16),
-            pltpu.VMEM((rows, ff), BF16),
-            pltpu.VMEM((steps, depth, tile), BF16),
-            pltpu.VMEM((steps, depth, tile), BF16),
-            pltpu.VMEM((groups, ff, feat), BF16),
-            pltpu.SemaphoreType.DMA((steps,)),
-            pltpu.SemaphoreType.DMA((steps,)),
-            pltpu.SemaphoreType.DMA((groups,)),
-        ],
-        micros=11.0,
+        scratch=[pltpu.VMEM((rows, depth), BF16), pltpu.VMEM((rows, ff), BF16)],
+        micros=9.0,
     )
 
 
@@ -466,14 +435,16 @@
         weights[k + 1] = send(weights[k], "tp", 1)
 
     qt, kvt = prep(
-        place, queries, key_input, value_input, query_gain[None], key_gain[None], table, heads
+        place,
+        *map(far_memory, (queries, key_input, value_input, query_gain[None], key_gain[None], table)),
+        heads,
     )
     blocks = [kvt]
     blocks += [send(kvt, "ep", k) for k in range(n_ep - 2, 0, -2)]
     blocks.append(send(kvt, "ep", 1))
     blocks += [send(b, "ep", 1) for b in blocks[1:half]]
 
-    outbound, slot = dispatch(place, routes.T, expert_input, n_ep, cap, feat)
+    outbound, slot = dispatch(place, far_memory(routes.T), far_memory(expert_input), n_ep, cap, feat)
     arrived = lax.all_to_all(outbound, "ep", split_axis=0, concat_axis=0, tiled=True)
     xs = {0: arrived}
     for k in range(2, n_tp, 2):
@@ -481,11 +452,11 @@
     for k in range(0, n_tp, 2):
         xs[k + 1] = send(xs[k], "tp", 1)
 
-    atts = attend(place, qt, blocks, heads, n_tp)
+    atts = attend(place, far_memory(qt), blocks, heads, n_tp)
     atts = [atts[0]] + [send(atts[k], "tp", k) for k in range(1, n_tp)]
 
     parts = expert(
-        place, [xs[k] for k in range(n_tp)], ffn_gain[None], gate_weight, up_weight, down_weight, n_ep
+        place, [xs[k] for k in range(n_tp)], far_memory(ffn_gain[None]), gate_weight[0], up_weight[0], down_weight[0], n_ep
     )
     returned = []
     for side in range(2):
@@ -500,7 +471,7 @@
             returned.append(send(piece, "ep", k) if k else piece)
 
     mixed = mix(place, atts, [weights[k] for k in range(n_tp)])
-    out = combine(place, slot, route_scores.T, returned)
+    out = combine(place, slot, far_memory(route_scores.T), returned)
     return mixed, out
 
 

time: 132 us -> 128 us (0.970)
  Pallas kernels: 37.1 us -> 35 us
  local copies, waits for them, and re-layouts: 7.16 us -> 5.08 us
    pallas_call x10, Pallas kernels: 37.1 us -> 35 us  [call(): pl.pallas_call(body, grid_spec=pltpu.PrefetchScalarGridSpec(num_scalar_pr...]
    unnamed x22 -> x10, local copies, waits for them, and re-layouts: 7.16 us -> 5.08 us
  transfers between devices with their start and end apart: 29 -> 29, of which waited for: 9 -> 9; matrix products, arithmetic and copies ran while one was open for 0% -> 0% of each run, Pallas kernels for 26% -> 24%
where the time goes in v2:
time: 128 us; the launch traced here: 127 us
  Pallas kernels  35 us (27%)
  waiting for transfers between devices  34.6 us (27%)
  starting transfers between devices  30 us (23%)
  blocking collectives  21.6 us (17%)
  local copies, waits for them, and re-layouts  5.08 us (4%)
    pallas_call x10, Pallas kernels, call(): pl.pallas_call(body, grid_spec=pltpu.PrefetchScalarGridSpec(num_scalar_pr...  35 us
    ppermute x29, waiting for transfers between devices, send(): return lax.ppermute(x, axis, [(i, i ^ flip) for i in range(n)])  34.6 us
    ppermute x29, starting transfers between devices, send(): return lax.ppermute(x, axis, [(i, i ^ flip) for i in range(n)])  30 us
    all_to_all x1, blocking collectives, local(): lax.all_to_all(outbound, 'ep', split_axis=0, concat_axis=0, tiled=True)  21.6 us
    unnamed x10, local copies, waits for them, and re-layouts  5.08 us
  transfers between devices with their start and end apart: 29, of which 9 were waited for; matrix products, arithmetic and copies ran while one was open for 0% of the time, Pallas kernels for 24%

profile of v2, /device:TPU:0, one launch (start us, length us, event | category | flops | bytes accessed | tf_op | source)
XLA Modules:
  0.0 127.2 jit_solution(9059386890646033411)
XLA Ops:
  0.6 0.1 pad_add_fusion.place
  0.7 2.8 %shard_map.152 = (bf16[512,512]{1,0:T(8,128)(2,1)S(1)}, s32[2,160]{1,0:T(2,128)S(1)}) custom-call(s32[2]{0:T(128)S(1)} %pad_add_fusion.place, s32[2,160]{1,0:T(2,128)} %bitcast.20, bf16[160,2048]{1,0:T(8,128)(2,1)} %x_hbm.1), custom_call_target="tpu_custom_call" | custom-call | flops 750000000 | tf_op jit(solution)/shard_map/pallas_call | solution.py:38
  3.5 21.6 %all_to_all.11 = bf16[8,64,512]{2,1,0:T(8,128)(2,1)S(1)} all-to-all(bf16[8,64,512]{2,1,0:T(8,128)(2,1)S(1)} %bitcast.15), channel_id=1, replica_groups=mesh['ep'=8,'tp'=4] {'ep'}, dimensions={0} | all-to-all | bytes 1048576 | tf_op jit(solution)/shard_map/all_to_all | solution.py:448
  25.1 1.5 %collective-permute-start.14 = (bf16[512,512]{1,0:T(8,128)(2,1)S(1)}, bf16[512,512]{1,0:T(8,128)(2,1)S(1)}, u32[]{:S(2)}, u32[]{:S(2)}) collective-permute-start(bf16[512,512]{1,0:T(8,128)(2,1)S(1)} %bitcast.12), channel_id=1, source_target_pairs={{0,2},{1,3},{2,0},{3,1},{4,6},{5,7},{6,4},{7,5},{8,10},{9,11},{10,... | collective-permute-start | bytes 1572872 | tf_op jit(solution)/shard_map/ppermute | solution.py:63
  26.7 0.5 collective-permute-start.11
  27.2 0.0 collective-permute-start.13
  27.2 12.8 %collective-permute-done.14.refs_2_ = bf16[512,512]{1,0:T(8,128)(2,1)S(1)} collective-permute-done((bf16[512,512]{1,0:T(8,128)(2,1)S(1)}, bf16[512,512]{1,0:T(8,128)(2,1)S(1)}, u32[]{:S(2)}, u32[]{:S(2)}) %collective-permute-start.14) | collective-permute-done | bytes 524320 | tf_op jit(solution)/shard_map/ppermute | solution.py:63
  39.9 0.0 collective-permute-start.15
  39.9 2.9 %shard_map.149 = (bf16[256,512]{1,0:T(8,128)(2,1)S(1)}, bf16[128,512]{1,0:T(8,128)(2,1)S(1)}) custom-call(s32[2]{0:T(128)S(1)} %pad_add_fusion.place, bf16[512,256]{1,0:T(8,128)(2,1)} %q_hbm.1, bf16[512,256]{1,0:T(8,128)(2,1)} %k_hbm.1, bf16[512,256]{1,0:T(8,128)(2,1)} %v_hbm.1, f32[1,64]{1,0:T(1,128)} %bitcast.22, f32[1,64]{1,0:T(1,128)} %bitcast.23, ...), custom_call_target="tpu_custom_call" | custom-call | flops 1000000000 | tf_op jit(solution)/shard_map/pallas_call | solution.py:38
  42.8 0.0 copy-start.4
  42.8 0.7 copy-done.4
  43.5 1.1 collective-permute-start
  44.7 1.4 %collective-permute-start.1 = (bf16[128,512]{1,0:T(8,128)(2,1)S(1)}, bf16[128,512]{1,0:T(8,128)(2,1)S(1)}, u32[]{:S(2)}, u32[]{:S(2)}) collective-permute-start(bf16[128,512]{1,0:T(8,128)(2,1)S(1)} %get-tuple-element.27.refs_0_), channel_id=1, source_target_pairs={{0,16},{4,20},{8,24},{12,28},{16,0},{20,4},{24,8},{28,12},{1,17},{... | collective-permute-start | bytes 393224 | tf_op jit(solution)/shard_map/ppermute | solution.py:63
  46.0 5.7 %collective-permute-done.refs_1_ = bf16[128,512]{1,0:T(8,128)(2,1)S(1)} collective-permute-done((bf16[128,512]{1,0:T(8,128)(2,1)S(1)}, bf16[128,512]{1,0:T(8,128)(2,1)S(1)}, u32[]{:S(2)}, u32[]{:S(2)}) %collective-permute-start) | collective-permute-done | bytes 131104 | tf_op jit(solution)/shard_map/ppermute | solution.py:63
  51.8 4.8 %collective-permute-start.2 = (bf16[128,512]{1,0:T(8,128)(2,1)S(1)}, bf16[128,512]{1,0:T(8,128)(2,1)S(1)}, u32[]{:S(2)}, u32[]{:S(2)}) collective-permute-start(bf16[128,512]{1,0:T(8,128)(2,1)S(1)} %get-tuple-element.27.refs_0_), channel_id=1, source_target_pairs={{0,8},{4,12},{8,0},{12,4},{16,24},{20,28},{24,16},{28,20},{1,9},{5... | collective-permute-start | bytes 393224 | tf_op jit(solution)/shard_map/ppermute | solution.py:63
  56.6 1.9 %collective-permute-done.1.refs_2_ = bf16[128,512]{1,0:T(8,128)(2,1)S(1)} collective-permute-done((bf16[128,512]{1,0:T(8,128)(2,1)S(1)}, bf16[128,512]{1,0:T(8,128)(2,1)S(1)}, u32[]{:S(2)}, u32[]{:S(2)}) %collective-permute-start.1) | collective-permute-done | bytes 131104 | tf_op jit(solution)/shard_map/ppermute | solution.py:63
  58.5 0.2 collective-permute-start.3
  58.7 2.5 %collective-permute-done.2.refs_3_ = bf16[128,512]{1,0:T(8,128)(2,1)S(1)} collective-permute-done((bf16[128,512]{1,0:T(8,128)(2,1)S(1)}, bf16[128,512]{1,0:T(8,128)(2,1)S(1)}, u32[]{:S(2)}, u32[]{:S(2)}) %collective-permute-start.2) | collective-permute-done | bytes 131104 | tf_op jit(solution)/shard_map/ppermute | solution.py:63
  61.2 2.0 %collective-permute-start.5 = (bf16[128,512]{1,0:T(8,128)(2,1)S(1)}, bf16[128,512]{1,0:T(8,128)(2,1)S(1)}, u32[]{:S(2)}, u32[]{:S(2)}) collective-permute-start(bf16[128,512]{1,0:T(8,128)(2,1)S(1)} %collective-permute-done.1.refs_2_), channel_id=1, source_target_pairs={{0,4},{4,0},{8,12},{12,8},{16,20},{20,16},{24,28},{28,24},{1,5},{5... | collective-permute-start | bytes 393224 | tf_op jit(solution)/shard_map/ppermute | solution.py:63
  63.2 0.0 collective-permute-done.15.refs_3_
  63.2 0.1 collective-permute-start.6
  63.3 2.2 %copy-done.2 = bf16[1,2048,1024]{2,1,0:T(8,128)(2,1)S(1)} copy-done((bf16[1,2048,1024]{2,1,0:T(8,128)(2,1)S(1)}, bf16[1,2048,1024]{2,1,0:T(8,128)(2,1)}, u32[]{:S(2)}) %copy-start.2) | copy-done | bytes 4194328
  65.5 2.2 %copy-done.3 = bf16[1,1024,2048]{2,1,0:T(8,128)(2,1)S(1)} copy-done((bf16[1,1024,2048]{2,1,0:T(8,128)(2,1)S(1)}, bf16[1,1024,2048]{2,1,0:T(8,128)(2,1)}, u32[]{:S(2)}) %copy-start.3) | copy-done | bytes 4194328
  67.7 8.7 %shard_map.153 = (bf16[256,512]{1,0:T(8,128)(2,1)S(1)}, bf16[256,512]{1,0:T(8,128)(2,1)S(1)}, bf16[256,512]{1,0:T(8,128)(2,1)S(1)}, bf16[256,512]{1,0:T(8,128)(2...) custom-call(s32[2]{0:T(128)S(1)} %pad_add_fusion.place, ...), custom_call_target="tpu_custom_call" | custom-call | flops 4499999744 | tf_op jit(solution)/shard_map/pallas_call | solution.py:38
  76.4 0.1 collective-permute-start.10
  76.4 0.0 collective-permute-done.11.refs_6_
  76.4 0.5 collective-permute-start.12
  76.9 0.0 collective-permute-done.4.refs_5_
  76.9 0.1 collective-permute-start.24
  77.0 12.8 %shard_map.150 = (bf16[128,256]{1,0:T(8,128)(2,1)S(1)}, bf16[128,256]{1,0:T(8,128)(2,1)S(1)}, bf16[128,256]{1,0:T(8,128)(2,1)S(1)}, bf16[128,256]{1,0:T(8,128)(2,1)S(1)}) custom-call(s32[2]{0:T(128)S(1)} %pad_add_fusion.place, bf16[256,512]{1,0:T(8,128)(2,1)} %copy-done.4, bf16[128,512]{1,0:T(8,128)(2,1)S(1)} %get-tuple-element.27.refs_0_, ...), custom_call_target="tpu_custom_call" | custom-call | flops 6000000000 | tf_op jit(solution)/shard_map/pallas_call | solution.py:38
  89.9 0.5 collective-permute-start.7
  90.3 0.1 collective-permute-start.17
  90.4 0.8 collective-permute-done.7.refs_1_
  91.2 0.4 collective-permute-start.23
  91.6 1.5 %collective-permute-start.8 = (bf16[128,256]{1,0:T(8,128)(2,1)S(1)}, bf16[128,256]{1,0:T(8,128)(2,1)S(1)}, u32[]{:S(2)}, u32[]{:S(2)}) collective-permute-start(bf16[128,256]{1,0:T(8,128)(2,1)S(1)} %get-tuple-element.30), channel_id=1, source_target_pairs={{0,2},{1,3},{2,0},{3,1},{4,6},{5,7},{6,4},{7,5},{8,10},{9,11},{10,... | collective-permute-start | bytes 196616 | tf_op jit(solution)/shard_map/ppermute | solution.py:63
  93.1 0.6 shard_map.156
  93.7 2.1 %collective-permute-done.8.refs_2_ = bf16[128,256]{1,0:T(8,128)(2,1)S(1)} collective-permute-done((bf16[128,256]{1,0:T(8,128)(2,1)S(1)}, bf16[128,256]{1,0:T(8,128)(2,1)S(1)}, u32[]{:S(2)}, u32[]{:S(2)}) %collective-permute-start.8) | collective-permute-done | bytes 65568 | tf_op jit(solution)/shard_map/ppermute | solution.py:63
  95.9 1.5 %collective-permute-start.25 = (bf16[256,512]{1,0:T(8,128)(2,1)S(1)}, bf16[256,512]{1,0:T(8,128)(2,1)S(1)}, u32[]{:S(2)}, u32[]{:S(2)}) collective-permute-start(bf16[256,512]{1,0:T(8,128)(2,1)S(1)} %shard_map.156), channel_id=1, source_target_pairs={{0,2},{1,3},{2,0},{3,1},{4,6},{5,7},{6,4},{7,5},{8,10},{9,11},{10,... | collective-permute-start | bytes 786440 | tf_op jit(solution)/shard_map/ppermute | solution.py:63
  97.4 0.0 collective-permute-done.17.refs_1_
  97.4 0.0 collective-permute-start.16
  97.4 0.6 shard_map.154
  98.0 0.0 collective-permute-done.23.refs_1_
  98.0 0.6 collective-permute-start.18
  98.6 6.4 %collective-permute-done.25.refs_2_ = bf16[256,512]{1,0:T(8,128)(2,1)S(1)} collective-permute-done((bf16[256,512]{1,0:T(8,128)(2,1)S(1)}, bf16[256,512]{1,0:T(8,128)(2,1)S(1)}, u32[]{:S(2)}, u32[]{:S(2)}) %collective-permute-start.25) | collective-permute-done | bytes 262176 | tf_op jit(solution)/shard_map/ppermute | solution.py:63
  105.0 0.0 collective-permute-start.9
  105.0 0.6 shard_map.157
  105.6 0.0 collective-permute-done.16.refs_1_
  105.7 2.0 %collective-permute-start.26 = (bf16[64,512]{1,0:T(8,128)(2,1)S(1)}, bf16[64,512]{1,0:T(8,128)(2,1)S(1)}, u32[]{:S(2)}, u32[]{:S(2)}) collective-permute-start(bf16[64,512]{1,0:T(8,128)(2,1)S(1)} %get-tuple-element.47), channel_id=1, source_target_pairs={{0,4},{4,0},{8,12},{12,8},{16,20},{20,16},{24,28},{28,24},{1,5},{5... | collective-permute-start | bytes 196616 | tf_op jit(solution)/shard_map/ppermute | solution.py:63
  107.7 1.7 %collective-permute-done.18.refs_2_ = bf16[256,512]{1,0:T(8,128)(2,1)S(1)} collective-permute-done((bf16[256,512]{1,0:T(8,128)(2,1)S(1)}, bf16[256,512]{1,0:T(8,128)(2,1)S(1)}, u32[]{:S(2)}, u32[]{:S(2)}) %collective-permute-start.18) | collective-permute-done | bytes 262176 | tf_op jit(solution)/shard_map/ppermute | solution.py:63
  109.4 0.4 collective-permute-start.27
  109.8 0.6 shard_map.155
  110.4 0.0 collective-permute-done.9.refs_3_
  110.5 3.1 %collective-permute-start.28 = (bf16[64,512]{1,0:T(8,128)(2,1)S(1)}, bf16[64,512]{1,0:T(8,128)(2,1)S(1)}, u32[]{:S(2)}, u32[]{:S(2)}) collective-permute-start(bf16[64,512]{1,0:T(8,128)(2,1)S(1)} %get-tuple-element.49), channel_id=1, source_target_pairs={{0,12},{4,8},{8,4},{12,0},{16,28},{20,24},{24,20},{28,16},{1,13},{... | collective-permute-start | bytes 196616 | tf_op jit(solution)/shard_map/ppermute | solution.py:63
  113.6 0.4 collective-permute-start.19
  113.9 0.0 collective-permute-done.12.refs_7_
  113.9 2.1 %collective-permute-start.20 = (bf16[64,512]{1,0:T(8,128)(2,1)S(1)}, bf16[64,512]{1,0:T(8,128)(2,1)S(1)}, u32[]{:S(2)}, u32[]{:S(2)}) collective-permute-start(bf16[64,512]{1,0:T(8,128)(2,1)S(1)} %get-tuple-element.39), channel_id=1, source_target_pairs={{0,20},{4,16},{8,28},{12,24},{16,4},{20,0},{24,12},{28,8},{1,21},{... | collective-permute-start | bytes 196616 | tf_op jit(solution)/shard_map/ppermute | solution.py:63
  116.0 0.0 collective-permute-done.26.refs_5_
  116.0 1.5 %collective-permute-start.21 = (bf16[64,512]{1,0:T(8,128)(2,1)S(1)}, bf16[64,512]{1,0:T(8,128)(2,1)S(1)}, u32[]{:S(2)}, u32[]{:S(2)}) collective-permute-start(bf16[64,512]{1,0:T(8,128)(2,1)S(1)} %get-tuple-element.40), channel_id=1, source_target_pairs={{0,24},{4,28},{8,16},{12,20},{16,8},{20,12},{24,0},{28,4},{1,25},{... | collective-permute-start | bytes 196616 | tf_op jit(solution)/shard_map/ppermute | solution.py:63
  117.5 0.0 collective-permute-done.27.refs_6_
  117.5 3.8 %collective-permute-start.22 = (bf16[64,512]{1,0:T(8,128)(2,1)S(1)}, bf16[64,512]{1,0:T(8,128)(2,1)S(1)}, u32[]{:S(2)}, u32[]{:S(2)}) collective-permute-start(bf16[64,512]{1,0:T(8,128)(2,1)S(1)} %get-tuple-element.41), channel_id=1, source_target_pairs={{0,28},{4,24},{8,20},{12,16},{16,12},{20,8},{24,4},{28,0},{1,29},{... | collective-permute-start | bytes 196616 | tf_op jit(solution)/shard_map/ppermute | solution.py:63
  121.2 3.1 %shard_map.151 = bf16[128,2048]{1,0:T(8,128)(2,1)} custom-call(s32[2]{0:T(128)S(1)} %pad_add_fusion.place, bf16[128,256]{1,0:T(8,128)(2,1)S(1)} %get-tuple-element.28.refs_0_, bf16[128,256]{1,0:T(8,128)(2,1)S(1)} %collective-permute-done.7.refs_1_, bf16[128,256]{1,0:T(8,128)(2,1)S(1)} %collective-permute-done.8.refs_2_, ...), custom_call_target="tpu_custom_call" | custom-call | flops 1250000000 | tf_op jit(solution)/shard_map/pallas_call | solution.py:38
  124.3 0.0 collective-permute-done.28.refs_7_
  124.3 0.6 collective-permute-done.20.refs_1_
  124.9 2.3 %shard_map.158 = bf16[160,512]{1,0:T(8,128)(2,1)} custom-call(s32[2]{0:T(128)S(1)} %pad_add_fusion.place, s32[2,160]{1,0:T(2,128)S(1)} %get-tuple-element.32.slot_ref, f32[2,160]{1,0:T(2,128)} %bitcast.21, bf16[64,512]{1,0:T(8,128)(2,1)S(1)} %collective-permute-done.19.refs_0_, bf16[64,512]{1,0:T(8,128)(2,1)S(1)} %collective-permute-done.20.refs_1_, ...), custom_call_target="tpu_custom_call" | custom-call | flops 750000000 | tf_op jit(solution)/shard_map/pallas_call | solution.py:38
  (16 shorter events, 0.0 us)
Async XLA Ops:
  0.6 62.6 %copy-start.1 = (bf16[1,2048,1024]{2,1,0:T(8,128)(2,1)S(1)}, bf16[1,2048,1024]{2,1,0:T(8,128)(2,1)}, u32[]{:S(2)}) copy-start(bf16[1,2048,1024]{2,1,0:T(8,128)(2,1)} %param.24) | copy-start | bytes 12582916
  25.1 14.8 %collective-permute-start.14 = (bf16[512,512]{1,0:T(8,128)(2,1)S(1)}, bf16[512,512]{1,0:T(8,128)(2,1)S(1)}, u32[]{:S(2)}, u32[]{:S(2)}) collective-permute-start(bf16[512,512]{1,0:T(8,128)(2,1)S(1)} %bitcast.12), channel_id=1, source_target_pairs={{0,2},{1,3},{2,0},{3,1},{4,6},{5,7},{6,4},{7,5},{8,10},{9,11},{10,... | collective-permute-start | bytes 1572872 | tf_op jit(solution)/shard_map/ppermute | solution.py:63
  26.7 49.8 %collective-permute-start.11 = (bf16[256,2048]{1,0:T(8,128)(2,1)}, bf16[256,2048]{1,0:T(8,128)(2,1)S(1)}, u32[]{:S(2)}, u32[]{:S(2)}) collective-permute-start(bf16[256,2048]{1,0:T(8,128)(2,1)} %refs_4_.1), channel_id=1, source_target_pairs={{0,2},{1,3},{2,0},{3,1},{4,6},{5,7},{6,4},{7,5},{8,10},{9,11},{10,... | collective-permute-start | bytes 3145736 | tf_op jit(solution)/shard_map/ppermute | solution.py:63
  27.2 34.0 %collective-permute-start.13 = (bf16[512,512]{1,0:T(8,128)(2,1)S(1)}, bf16[512,512]{1,0:T(8,128)(2,1)S(1)}, u32[]{:S(2)}, u32[]{:S(2)}) collective-permute-start(bf16[512,512]{1,0:T(8,128)(2,1)S(1)} %bitcast.13), channel_id=1, source_target_pairs={{0,1},{1,0},{2,3},{3,2},{4,5},{5,4},{6,7},{7,6},{8,9},{9,8},{10,11... | collective-permute-start | bytes 1572872 | tf_op jit(solution)/shard_map/ppermute | solution.py:63
  39.9 23.3 %collective-permute-start.15 = (bf16[512,512]{1,0:T(8,128)(2,1)S(1)}, bf16[512,512]{1,0:T(8,128)(2,1)S(1)}, u32[]{:S(2)}, u32[]{:S(2)}) collective-permute-start(bf16[512,512]{1,0:T(8,128)(2,1)S(1)} %collective-permute-done.14.refs_2_), channel_id=1, source_target_pairs={{0,1},{1,0},{2,3},{3,2},{4,5},{5,4},{6,7},{7,6},{8,9},{9,8},{10,11... | collective-permute-start | bytes 1572872 | tf_op jit(solution)/shard_map/ppermute | solution.py:63
  42.8 0.7 copy-start.4
  43.5 8.3 %collective-permute-start = (bf16[128,512]{1,0:T(8,128)(2,1)S(1)}, bf16[128,512]{1,0:T(8,128)(2,1)S(1)}, u32[]{:S(2)}, u32[]{:S(2)}) collective-permute-start(bf16[128,512]{1,0:T(8,128)(2,1)S(1)} %get-tuple-element.27.refs_0_), channel_id=1, source_target_pairs={{0,24},{4,28},{8,16},{12,20},{16,8},{20,12},{24,0},{28,4},{1,25},{... | collective-permute-start | bytes 393224 | tf_op jit(solution)/shard_map/ppermute | solution.py:63
  44.7 13.8 %collective-permute-start.1 = (bf16[128,512]{1,0:T(8,128)(2,1)S(1)}, bf16[128,512]{1,0:T(8,128)(2,1)S(1)}, u32[]{:S(2)}, u32[]{:S(2)}) collective-permute-start(bf16[128,512]{1,0:T(8,128)(2,1)S(1)} %get-tuple-element.27.refs_0_), channel_id=1, source_target_pairs={{0,16},{4,20},{8,24},{12,28},{16,0},{20,4},{24,8},{28,12},{1,17},{... | collective-permute-start | bytes 393224 | tf_op jit(solution)/shard_map/ppermute | solution.py:63
  51.8 9.4 %collective-permute-start.2 = (bf16[128,512]{1,0:T(8,128)(2,1)S(1)}, bf16[128,512]{1,0:T(8,128)(2,1)S(1)}, u32[]{:S(2)}, u32[]{:S(2)}) collective-permute-start(bf16[128,512]{1,0:T(8,128)(2,1)S(1)} %get-tuple-element.27.refs_0_), channel_id=1, source_target_pairs={{0,8},{4,12},{8,0},{12,4},{16,24},{20,28},{24,16},{28,20},{1,9},{5... | collective-permute-start | bytes 393224 | tf_op jit(solution)/shard_map/ppermute | solution.py:63
  58.5 17.9 %collective-permute-start.3 = (bf16[128,512]{1,0:T(8,128)(2,1)S(1)}, bf16[128,512]{1,0:T(8,128)(2,1)S(1)}, u32[]{:S(2)}, u32[]{:S(2)}) collective-permute-start(bf16[128,512]{1,0:T(8,128)(2,1)S(1)} %get-tuple-element.27.refs_0_), channel_id=1, source_target_pairs={{0,4},{4,0},{8,12},{12,8},{16,20},{20,16},{24,28},{28,24},{1,5},{5... | collective-permute-start | bytes 393224 | tf_op jit(solution)/shard_map/ppermute | solution.py:63
  61.2 15.8 %collective-permute-start.4 = (bf16[128,512]{1,0:T(8,128)(2,1)S(1)}, bf16[128,512]{1,0:T(8,128)(2,1)S(1)}, u32[]{:S(2)}, u32[]{:S(2)}) collective-permute-start(bf16[128,512]{1,0:T(8,128)(2,1)S(1)} %collective-permute-done.refs_1_), channel_id=1, source_target_pairs={{0,4},{4,0},{8,12},{12,8},{16,20},{20,16},{24,28},{28,24},{1,5},{5... | collective-permute-start | bytes 393224 | tf_op jit(solution)/shard_map/ppermute | solution.py:63
  61.2 15.9 %collective-permute-start.5 = (bf16[128,512]{1,0:T(8,128)(2,1)S(1)}, bf16[128,512]{1,0:T(8,128)(2,1)S(1)}, u32[]{:S(2)}, u32[]{:S(2)}) collective-permute-start(bf16[128,512]{1,0:T(8,128)(2,1)S(1)} %collective-permute-done.1.refs_2_), channel_id=1, source_target_pairs={{0,4},{4,0},{8,12},{12,8},{16,20},{20,16},{24,28},{28,24},{1,5},{5... | collective-permute-start | bytes 393224 | tf_op jit(solution)/shard_map/ppermute | solution.py:63
  63.2 13.8 %collective-permute-start.6 = (bf16[128,512]{1,0:T(8,128)(2,1)S(1)}, bf16[128,512]{1,0:T(8,128)(2,1)S(1)}, u32[]{:S(2)}, u32[]{:S(2)}) collective-permute-start(bf16[128,512]{1,0:T(8,128)(2,1)S(1)} %collective-permute-done.2.refs_3_), channel_id=1, source_target_pairs={{0,4},{4,0},{8,12},{12,8},{16,20},{20,16},{24,28},{28,24},{1,5},{5... | collective-permute-start | bytes 393224 | tf_op jit(solution)/shard_map/ppermute | solution.py:63
  63.3 2.2 %copy-start.2 = (bf16[1,2048,1024]{2,1,0:T(8,128)(2,1)S(1)}, bf16[1,2048,1024]{2,1,0:T(8,128)(2,1)}, u32[]{:S(2)}) copy-start(bf16[1,2048,1024]{2,1,0:T(8,128)(2,1)} %param.25) | copy-start | bytes 12582916
  65.5 2.2 %copy-start.3 = (bf16[1,1024,2048]{2,1,0:T(8,128)(2,1)S(1)}, bf16[1,1024,2048]{2,1,0:T(8,128)(2,1)}, u32[]{:S(2)}) copy-start(bf16[1,1024,2048]{2,1,0:T(8,128)(2,1)} %param.26) | copy-start | bytes 12582916
  67.7 8.7 %copy-start = (bf16[256,2048]{1,0:T(8,128)(2,1)S(1)}, bf16[256,2048]{1,0:T(8,128)(2,1)}, u32[]{:S(2)}) copy-start(bf16[256,2048]{1,0:T(8,128)(2,1)} %refs_4_.1) | copy-start | bytes 3145732
  76.4 37.2 %collective-permute-start.10 = (bf16[256,2048]{1,0:T(8,128)(2,1)S(1)}, bf16[256,2048]{1,0:T(8,128)(2,1)S(1)}, u32[]{:S(2)}, u32[]{:S(2)}) collective-permute-start(bf16[256,2048]{1,0:T(8,128)(2,1)S(1)} %copy-done), channel_id=1, source_target_pairs={{0,1},{1,0},{2,3},{3,2},{4,5},{5,4},{6,7},{7,6},{8,9},{9,8},{10,11... | collective-permute-start | bytes 3145736 | tf_op jit(solution)/shard_map/ppermute | solution.py:63
  76.4 37.5 %collective-permute-start.12 = (bf16[256,2048]{1,0:T(8,128)(2,1)S(1)}, bf16[256,2048]{1,0:T(8,128)(2,1)S(1)}, u32[]{:S(2)}, u32[]{:S(2)}) collective-permute-start(bf16[256,2048]{1,0:T(8,128)(2,1)S(1)} %collective-permute-done.11.refs_6_), channel_id=1, source_target_pairs={{0,1},{1,0},{2,3},{3,2},{4,5},{5,4},{6,7},{7,6},{8,9},{9,8},{10,11... | collective-permute-start | bytes 3145736 | tf_op jit(solution)/shard_map/ppermute | solution.py:63
  76.9 14.7 %collective-permute-start.24 = (bf16[256,512]{1,0:T(8,128)(2,1)S(1)}, bf16[256,512]{1,0:T(8,128)(2,1)S(1)}, u32[]{:S(2)}, u32[]{:S(2)}) collective-permute-start(bf16[256,512]{1,0:T(8,128)(2,1)S(1)} %get-tuple-element.45), channel_id=1, source_target_pairs={{0,1},{1,0},{2,3},{3,2},{4,5},{5,4},{6,7},{7,6},{8,9},{9,8},{10,11... | collective-permute-start | bytes 786440 | tf_op jit(solution)/shard_map/ppermute | solution.py:63
  89.9 1.4 %collective-permute-start.7 = (bf16[128,256]{1,0:T(8,128)(2,1)S(1)}, bf16[128,256]{1,0:T(8,128)(2,1)S(1)}, u32[]{:S(2)}, u32[]{:S(2)}) collective-permute-start(bf16[128,256]{1,0:T(8,128)(2,1)S(1)} %get-tuple-element.29), channel_id=1, source_target_pairs={{0,1},{1,0},{2,3},{3,2},{4,5},{5,4},{6,7},{7,6},{8,9},{9,8},{10,11... | collective-permute-start | bytes 196616 | tf_op jit(solution)/shard_map/ppermute | solution.py:63
  90.3 7.0 %collective-permute-start.17 = (bf16[256,512]{1,0:T(8,128)(2,1)S(1)}, bf16[256,512]{1,0:T(8,128)(2,1)S(1)}, u32[]{:S(2)}, u32[]{:S(2)}) collective-permute-start(bf16[256,512]{1,0:T(8,128)(2,1)S(1)} %get-tuple-element.37), channel_id=1, source_target_pairs={{0,1},{1,0},{2,3},{3,2},{4,5},{5,4},{6,7},{7,6},{8,9},{9,8},{10,11... | collective-permute-start | bytes 786440 | tf_op jit(solution)/shard_map/ppermute | solution.py:63
  91.2 6.8 %collective-permute-start.23 = (bf16[256,512]{1,0:T(8,128)(2,1)S(1)}, bf16[256,512]{1,0:T(8,128)(2,1)S(1)}, u32[]{:S(2)}, u32[]{:S(2)}) collective-permute-start(bf16[256,512]{1,0:T(8,128)(2,1)S(1)} %get-tuple-element.43), channel_id=1, source_target_pairs={{0,1},{1,0},{2,3},{3,2},{4,5},{5,4},{6,7},{7,6},{8,9},{9,8},{10,11... | collective-permute-start | bytes 786440 | tf_op jit(solution)/shard_map/ppermute | solution.py:63
  91.6 4.3 %collective-permute-start.8 = (bf16[128,256]{1,0:T(8,128)(2,1)S(1)}, bf16[128,256]{1,0:T(8,128)(2,1)S(1)}, u32[]{:S(2)}, u32[]{:S(2)}) collective-permute-start(bf16[128,256]{1,0:T(8,128)(2,1)S(1)} %get-tuple-element.30), channel_id=1, source_target_pairs={{0,2},{1,3},{2,0},{3,1},{4,6},{5,7},{6,4},{7,5},{8,10},{9,11},{10,... | collective-permute-start | bytes 196616 | tf_op jit(solution)/shard_map/ppermute | solution.py:63
  95.9 9.1 %collective-permute-start.25 = (bf16[256,512]{1,0:T(8,128)(2,1)S(1)}, bf16[256,512]{1,0:T(8,128)(2,1)S(1)}, u32[]{:S(2)}, u32[]{:S(2)}) collective-permute-start(bf16[256,512]{1,0:T(8,128)(2,1)S(1)} %shard_map.156), channel_id=1, source_target_pairs={{0,2},{1,3},{2,0},{3,1},{4,6},{5,7},{6,4},{7,5},{8,10},{9,11},{10,... | collective-permute-start | bytes 786440 | tf_op jit(solution)/shard_map/ppermute | solution.py:63
  97.4 8.3 %collective-permute-start.16 = (bf16[256,512]{1,0:T(8,128)(2,1)S(1)}, bf16[256,512]{1,0:T(8,128)(2,1)S(1)}, u32[]{:S(2)}, u32[]{:S(2)}) collective-permute-start(bf16[256,512]{1,0:T(8,128)(2,1)S(1)} %get-tuple-element.35), channel_id=1, source_target_pairs={{0,1},{1,0},{2,3},{3,2},{4,5},{5,4},{6,7},{7,6},{8,9},{9,8},{10,11... | collective-permute-start | bytes 786440 | tf_op jit(solution)/shard_map/ppermute | solution.py:63
  98.0 11.4 %collective-permute-start.18 = (bf16[256,512]{1,0:T(8,128)(2,1)S(1)}, bf16[256,512]{1,0:T(8,128)(2,1)S(1)}, u32[]{:S(2)}, u32[]{:S(2)}) collective-permute-start(bf16[256,512]{1,0:T(8,128)(2,1)S(1)} %shard_map.154), channel_id=1, source_target_pairs={{0,2},{1,3},{2,0},{3,1},{4,6},{5,7},{6,4},{7,5},{8,10},{9,11},{10,... | collective-permute-start | bytes 786440 | tf_op jit(solution)/shard_map/ppermute | solution.py:63
  105.0 5.4 %collective-permute-start.9 = (bf16[128,256]{1,0:T(8,128)(2,1)S(1)}, bf16[128,256]{1,0:T(8,128)(2,1)S(1)}, u32[]{:S(2)}, u32[]{:S(2)}) collective-permute-start(bf16[128,256]{1,0:T(8,128)(2,1)S(1)} %get-tuple-element.31), channel_id=1, source_target_pairs={{0,3},{1,2},{2,1},{3,0},{4,7},{5,6},{6,5},{7,4},{8,11},{9,10},{10,... | collective-permute-start | bytes 196616 | tf_op jit(solution)/shard_map/ppermute | solution.py:63
  105.7 10.3 %collective-permute-start.26 = (bf16[64,512]{1,0:T(8,128)(2,1)S(1)}, bf16[64,512]{1,0:T(8,128)(2,1)S(1)}, u32[]{:S(2)}, u32[]{:S(2)}) collective-permute-start(bf16[64,512]{1,0:T(8,128)(2,1)S(1)} %get-tuple-element.47), channel_id=1, source_target_pairs={{0,4},{4,0},{8,12},{12,8},{16,20},{20,16},{24,28},{28,24},{1,5},{5... | collective-permute-start | bytes 196616 | tf_op jit(solution)/shard_map/ppermute | solution.py:63
  109.4 8.0 %collective-permute-start.27 = (bf16[64,512]{1,0:T(8,128)(2,1)S(1)}, bf16[64,512]{1,0:T(8,128)(2,1)S(1)}, u32[]{:S(2)}, u32[]{:S(2)}) collective-permute-start(bf16[64,512]{1,0:T(8,128)(2,1)S(1)} %get-tuple-element.48), channel_id=1, source_target_pairs={{0,8},{4,12},{8,0},{12,4},{16,24},{20,28},{24,16},{28,20},{1,9},{5... | collective-permute-start | bytes 196616 | tf_op jit(solution)/shard_map/ppermute | solution.py:63
  110.5 13.8 %collective-permute-start.28 = (bf16[64,512]{1,0:T(8,128)(2,1)S(1)}, bf16[64,512]{1,0:T(8,128)(2,1)S(1)}, u32[]{:S(2)}, u32[]{:S(2)}) collective-permute-start(bf16[64,512]{1,0:T(8,128)(2,1)S(1)} %get-tuple-element.49), channel_id=1, source_target_pairs={{0,12},{4,8},{8,4},{12,0},{16,28},{20,24},{24,20},{28,16},{1,13},{... | collective-permute-start | bytes 196616 | tf_op jit(solution)/shard_map/ppermute | solution.py:63
  113.6 10.7 %collective-permute-start.19 = (bf16[64,512]{1,0:T(8,128)(2,1)S(1)}, bf16[64,512]{1,0:T(8,128)(2,1)S(1)}, u32[]{:S(2)}, u32[]{:S(2)}) collective-permute-start(bf16[64,512]{1,0:T(8,128)(2,1)S(1)} %get-tuple-element.38), channel_id=1, source_target_pairs={{0,16},{4,20},{8,24},{12,28},{16,0},{20,4},{24,8},{28,12},{1,17},{... | collective-permute-start | bytes 196616 | tf_op jit(solution)/shard_map/ppermute | solution.py:63
  113.9 11.0 %collective-permute-start.20 = (bf16[64,512]{1,0:T(8,128)(2,1)S(1)}, bf16[64,512]{1,0:T(8,128)(2,1)S(1)}, u32[]{:S(2)}, u32[]{:S(2)}) collective-permute-start(bf16[64,512]{1,0:T(8,128)(2,1)S(1)} %get-tuple-element.39), channel_id=1, source_target_pairs={{0,20},{4,16},{8,28},{12,24},{16,4},{20,0},{24,12},{28,8},{1,21},{... | collective-permute-start | bytes 196616 | tf_op jit(solution)/shard_map/ppermute | solution.py:63
  116.0 8.9 %collective-permute-start.21 = (bf16[64,512]{1,0:T(8,128)(2,1)S(1)}, bf16[64,512]{1,0:T(8,128)(2,1)S(1)}, u32[]{:S(2)}, u32[]{:S(2)}) collective-permute-start(bf16[64,512]{1,0:T(8,128)(2,1)S(1)} %get-tuple-element.40), channel_id=1, source_target_pairs={{0,24},{4,28},{8,16},{12,20},{16,8},{20,12},{24,0},{28,4},{1,25},{... | collective-permute-start | bytes 196616 | tf_op jit(solution)/shard_map/ppermute | solution.py:63
  117.5 7.4 %collective-permute-start.22 = (bf16[64,512]{1,0:T(8,128)(2,1)S(1)}, bf16[64,512]{1,0:T(8,128)(2,1)S(1)}, u32[]{:S(2)}, u32[]{:S(2)}) collective-permute-start(bf16[64,512]{1,0:T(8,128)(2,1)S(1)} %get-tuple-element.41), channel_id=1, source_target_pairs={{0,28},{4,24},{8,20},{12,16},{16,12},{20,8},{24,4},{28,0},{1,29},{... | collective-permute-start | bytes 196616 | tf_op jit(solution)/shard_map/ppermute | solution.py:63

commit v3 on v2

--- a/solution.py
+++ b/solution.py
@@ -89,9 +89,8 @@
     fetch.wait()
     x = x_ref[...]
     slots = lax.broadcasted_iota(jnp.int32, (cap, tokens), 0)
-    for e in range(experts):
-        pick = (slots == slot[e : e + 1, :]).astype(F32).astype(BF16)
-        out_ref[e * cap : (e + 1) * cap, :] = mm(pick, x).astype(BF16)
+    picks = [(slots == slot[e : e + 1, :]).astype(F32) for e in range(experts)]
+    out_ref[...] = mm(jnp.concatenate(picks, axis=0).astype(BF16), x).astype(BF16)
 
 
 def dispatch(place, routes, expert_input, experts, cap, feat):
@@ -200,7 +199,7 @@
             hbm(),
         ],
         [
-            jax.ShapeDtypeStruct((queries.shape[1], rows), BF16),
+            pltpu.HBM((queries.shape[1], rows), BF16),
             jax.ShapeDtypeStruct((2 * HD, rows), BF16),
         ],
         scratch=[
@@ -215,18 +214,22 @@
     )
 
 
-def attend_body(place, qt_ref, *refs, blocks, heads, groups):
-    count = len(refs) - 5 - groups
-    kv_refs, out_refs = refs[:count], refs[count : count + groups]
-    out_ref, k_ref, v_ref, num_ref, den_ref = refs[count + groups :]
+def attend_body(place, qt_ref, *refs, blocks, heads, count, groups):
+    if groups:
+        num_in, den_in = refs[:2]
+        refs = refs[2:]
+        kv_refs, out_refs = refs[:count], refs[count : count + groups]
+        out_ref, k_ref, v_ref, num_ref, den_ref = refs[count + groups :]
+        num_ref[...] = num_in[...]
+        den_ref[...] = den_in[...]
+    else:
+        kv_refs, (num_ref, den_ref, k_ref, v_ref) = refs[:count], refs[count:]
+        num_ref[...] = jnp.zeros_like(num_ref)
+        den_ref[...] = jnp.zeros_like(den_ref)
     keys = kv_refs[0].shape[1]
-    per = blocks // count
     for b in range(blocks):
-        base = (b % per) * 2 * HD
-        k_ref[b] = kv_refs[b // per][base : base + HD, :].astype(F32).T.astype(BF16)
-        v_ref[b] = kv_refs[b // per][base + HD : base + 2 * HD, :]
-    num_ref[...] = jnp.zeros_like(num_ref)
-    den_ref[...] = jnp.zeros_like(den_ref)
+        k_ref[b] = kv_refs[b][:HD, :].astype(F32).T.astype(BF16)
+        v_ref[b] = kv_refs[b][HD:, :]
 
     def one(b, carry):
         k = k_ref[b]
@@ -239,34 +242,36 @@
         return carry
 
     lax.fori_loop(0, blocks, one, 0)
-    for h in range(heads):
-        den = jnp.sum(den_ref[h * 8 : (h + 1) * 8, :], axis=0, keepdims=True)
-        num_ref[h * HD : (h + 1) * HD, :] = num_ref[h * HD : (h + 1) * HD, :] / den
-    out_ref[...] = num_ref[...].T
-    rows = out_refs[0].shape[0]
-    for k in range(groups):
-        at = pl.multiple_of((place[0] ^ k) * rows, rows)
-        out_refs[k][...] = out_ref[pl.ds(at, rows), :].astype(BF16)
-
-
-def attend(place, qt, kv_blocks, heads, groups):
+    if groups:
+        for h in range(heads):
+            den = jnp.sum(den_ref[h * 8 : (h + 1) * 8, :], axis=0, keepdims=True)
+            num_ref[h * HD : (h + 1) * HD, :] = num_ref[h * HD : (h + 1) * HD, :] / den
+        out_ref[...] = num_ref[...].T
+        rows = out_refs[0].shape[0]
+        for k in range(groups):
+            at = pl.multiple_of((place[0] ^ k) * rows, rows)
+            out_refs[k][...] = out_ref[pl.ds(at, rows), :].astype(BF16)
+
+
+def attend(place, qt, sums, kv_blocks, heads, groups):
     rows = qt.shape[1]
     keys = kv_blocks[0].shape[1]
-    blocks = sum(b.shape[0] for b in kv_blocks) // (2 * HD)
-    return call(
-        functools.partial(attend_body, blocks=blocks, heads=heads, groups=groups),
-        place,
-        (qt, *kv_blocks),
-        [full(qt.shape)] + [full(b.shape) for b in kv_blocks],
-        [jax.ShapeDtypeStruct((rows // groups, qt.shape[0]), BF16)] * groups,
-        scratch=[
-            pltpu.VMEM((rows, qt.shape[0]), F32),
-            pltpu.VMEM((blocks, keys, HD), BF16),
-            pltpu.VMEM((blocks, HD, keys), BF16),
-            pltpu.VMEM(qt.shape, F32),
-            pltpu.VMEM((heads * 8, rows), F32),
-        ],
-        micros=12.0,
+    count = len(kv_blocks)
+    held = [pltpu.HBM(qt.shape, F32), pltpu.HBM((heads * 8, rows), F32)]
+    scratch = [pltpu.VMEM((count, keys, HD), BF16), pltpu.VMEM((count, HD, keys), BF16)]
+    if groups:
+        outs = [jax.ShapeDtypeStruct((rows // groups, qt.shape[0]), BF16)] * groups
+        scratch = [pltpu.VMEM((rows, qt.shape[0]), F32)] + scratch + [pltpu.VMEM(h.shape, F32) for h in held]
+    else:
+        outs = held
+    return call(
+        functools.partial(attend_body, blocks=count, heads=heads, count=count, groups=groups),
+        place,
+        (qt, *sums, *kv_blocks),
+        [full(qt.shape)] + [full(x.shape) for x in sums] + [full(b.shape) for b in kv_blocks],
+        outs,
+        scratch=scratch,
+        micros=7.0,
     )
 
 
@@ -345,29 +350,6 @@
         [jax.ShapeDtypeStruct((rows // 2, feat), BF16)] * (2 * groups),
         scratch=[pltpu.VMEM((rows, depth), BF16), pltpu.VMEM((rows, ff), BF16)],
         micros=9.0,
-    )
-
-
-def finish_body(place, *refs, terms):
-    total = 0.0
-    for r in refs[:terms]:
-        total += r[...].astype(F32)
-    total = total.astype(BF16)
-    outs = refs[terms:]
-    rows = outs[0].shape[0]
-    for i, o in enumerate(outs):
-        o[...] = total[i * rows : (i + 1) * rows]
-
-
-def finish(place, terms, pieces):
-    rows, feat = terms[0].shape
-    return call(
-        functools.partial(finish_body, terms=len(terms)),
-        place,
-        tuple(terms),
-        [full(t.shape) for t in terms],
-        [jax.ShapeDtypeStruct((rows // pieces, feat), BF16)] * pieces,
-        micros=0.5,
     )
 
 
@@ -452,7 +434,8 @@
     for k in range(0, n_tp, 2):
         xs[k + 1] = send(xs[k], "tp", 1)
 
-    atts = attend(place, far_memory(qt), blocks, heads, n_tp)
+    sums = attend(place, far_memory(qt), (), blocks[:half], heads, 0)
+    atts = attend(place, far_memory(qt), [far_memory(x) for x in sums], blocks[half:], heads, n_tp)
     atts = [atts[0]] + [send(atts[k], "tp", k) for k in range(1, n_tp)]
 
     parts = expert(
@@ -463,15 +446,15 @@
         mine = {k: (parts[2 * k + side], send(parts[2 * k + 2 + side], "tp", 1)) for k in range(0, n_tp, 2)}
         terms = list(mine[0])
         for k in range(2, n_tp, 2):
-            (both,) = finish(place, mine[k], 1)
+            both = (mine[k][0].astype(F32) + mine[k][1].astype(F32)).astype(BF16)
             terms.append(send(both, "tp", k))
-        pieces = finish(place, terms, half)
-        for i, piece in enumerate(pieces):
+        for i in range(half):
+            piece = sum(t[i * cap : (i + 1) * cap].astype(F32) for t in terms).astype(BF16)
             k = i ^ half if side == 0 else i
             returned.append(send(piece, "ep", k) if k else piece)
 
     mixed = mix(place, atts, [weights[k] for k in range(n_tp)])
-    out = combine(place, slot, far_memory(route_scores.T), returned)
+    out = combine(place, slot, route_scores.T, returned)
     return mixed, out
 
 

time: 128 us -> 115 us (0.90)
  starting transfers between devices: 30 us -> 23.4 us
  local copies, waits for them, and re-layouts: 5.08 us -> 0.02 us
    ppermute x29, starting transfers between devices: 30 us -> 23.4 us  [send(): return lax.ppermute(x, axis, [(i, i ^ flip) for i in range(n)])]
    unnamed x10, local copies, waits for them, and re-layouts: 5.08 us -> 0.02 us
    pallas_call x10 -> x7, Pallas kernels: 35 us -> 34.9 us  [call(): pl.pallas_call(body, grid_spec=pltpu.PrefetchScalarGridSpec(num_scalar_pr...]
  transfers between devices with their start and end apart: 29 -> 29, of which waited for: 9 -> 7; matrix products, arithmetic and copies ran while one was open for 0% -> 0% of each run, Pallas kernels for 24% -> 27%
where the time goes in v3:
time: 115 us
  Pallas kernels  34.9 us (30%)
  waiting for transfers between devices  33.5 us (29%)
  starting transfers between devices  23.4 us (20%)
  blocking collectives  21.6 us (19%)
    pallas_call x7, Pallas kernels, call(): pl.pallas_call(body, grid_spec=pltpu.PrefetchScalarGridSpec(num_scalar_pr...  34.9 us
    ppermute x29, waiting for transfers between devices, send(): return lax.ppermute(x, axis, [(i, i ^ flip) for i in range(n)])  33.5 us
    ppermute x29, starting transfers between devices, send(): return lax.ppermute(x, axis, [(i, i ^ flip) for i in range(n)])  23.4 us
    all_to_all x1, blocking collectives, local(): lax.all_to_all(outbound, 'ep', split_axis=0, concat_axis=0, tiled=True)  21.6 us
  transfers between devices with their start and end apart: 29, of which 7 were waited for; matrix products, arithmetic and copies ran while one was open for 0% of the time, Pallas kernels for 27%

profile of v3, /device:TPU:0, one launch (start us, length us, event | category | flops | bytes accessed | tf_op | source)
XLA Modules:
  0.0 114.6 jit_solution(1326030244574915141)
XLA Ops:
  0.6 0.1 pad_add_fusion.place
  0.7 2.4 %shard_map.153 = (bf16[512,512]{1,0:T(8,128)(2,1)S(1)}, s32[2,160]{1,0:T(2,128)S(1)}) custom-call(s32[2]{0:T(128)S(1)} %pad_add_fusion.place, s32[2,160]{1,0:T(2,128)} %bitcast.21, bf16[160,2048]{1,0:T(8,128)(2,1)} %x_hbm.1), custom_call_target="tpu_custom_call" | custom-call | flops 750000000 | tf_op jit(solution)/shard_map/pallas_call | solution.py:38
  3.2 21.6 %all_to_all.11 = bf16[8,64,512]{2,1,0:T(8,128)(2,1)S(1)} all-to-all(bf16[8,64,512]{2,1,0:T(8,128)(2,1)S(1)} %bitcast.15), channel_id=1, replica_groups=mesh['ep'=8,'tp'=4] {'ep'}, dimensions={0} | all-to-all | bytes 1048576 | tf_op jit(solution)/shard_map/all_to_all | solution.py:430
  24.8 1.5 %collective-permute-start.14 = (bf16[512,512]{1,0:T(8,128)(2,1)S(1)}, bf16[512,512]{1,0:T(8,128)(2,1)S(1)}, u32[]{:S(2)}, u32[]{:S(2)}) collective-permute-start(bf16[512,512]{1,0:T(8,128)(2,1)S(1)} %bitcast.12), channel_id=1, source_target_pairs={{0,2},{1,3},{2,0},{3,1},{4,6},{5,7},{6,4},{7,5},{8,10},{9,11},{10,... | collective-permute-start | bytes 1572872 | tf_op jit(solution)/shard_map/ppermute | solution.py:63
  26.3 0.5 collective-permute-start.11
  26.8 3.4 %shard_map.149 = (bf16[256,512]{1,0:T(8,128)(2,1)}, bf16[128,512]{1,0:T(8,128)(2,1)S(1)}) custom-call(s32[2]{0:T(128)S(1)} %pad_add_fusion.place, bf16[512,256]{1,0:T(8,128)(2,1)} %q_hbm.1, bf16[512,256]{1,0:T(8,128)(2,1)} %k_hbm.1, bf16[512,256]{1,0:T(8,128)(2,1)} %v_hbm.1, f32[1,64]{1,0:T(1,128)} %bitcast.22, f32[1,64]{1,0:T(1,128)} %bitcast.23, ...), custom_call_target="tpu_custom_call" | custom-call | flops 1000000000 | tf_op jit(solution)/shard_map/pallas_call | solution.py:38
  30.2 1.2 %collective-permute-start = (bf16[128,512]{1,0:T(8,128)(2,1)S(1)}, bf16[128,512]{1,0:T(8,128)(2,1)S(1)}, u32[]{:S(2)}, u32[]{:S(2)}) collective-permute-start(bf16[128,512]{1,0:T(8,128)(2,1)S(1)} %get-tuple-element.21.refs_0_), channel_id=1, source_target_pairs={{0,24},{4,28},{8,16},{12,20},{16,8},{20,12},{24,0},{28,4},{1,25},{... | collective-permute-start | bytes 393224 | tf_op jit(solution)/shard_map/ppermute | solution.py:63
  31.5 0.0 collective-permute-start.13
  31.5 8.1 %collective-permute-done.14.refs_2_ = bf16[512,512]{1,0:T(8,128)(2,1)S(1)} collective-permute-done((bf16[512,512]{1,0:T(8,128)(2,1)S(1)}, bf16[512,512]{1,0:T(8,128)(2,1)S(1)}, u32[]{:S(2)}, u32[]{:S(2)}) %collective-permute-start.14) | collective-permute-done | bytes 524320 | tf_op jit(solution)/shard_map/ppermute | solution.py:63
  39.6 0.0 collective-permute-start.15
  39.6 1.1 collective-permute-start.1
  40.6 0.0 collective-permute-done.refs_1_
  40.6 0.6 collective-permute-start.2
  41.3 7.9 %collective-permute-done.1.refs_2_ = bf16[128,512]{1,0:T(8,128)(2,1)S(1)} collective-permute-done((bf16[128,512]{1,0:T(8,128)(2,1)S(1)}, bf16[128,512]{1,0:T(8,128)(2,1)S(1)}, u32[]{:S(2)}, u32[]{:S(2)}) %collective-permute-start.1) | collective-permute-done | bytes 131104 | tf_op jit(solution)/shard_map/ppermute | solution.py:63
  49.2 0.7 collective-permute-start.3
  49.9 0.0 collective-permute-done.2.refs_3_
  49.9 1.3 %collective-permute-start.4 = (bf16[128,512]{1,0:T(8,128)(2,1)S(1)}, bf16[128,512]{1,0:T(8,128)(2,1)S(1)}, u32[]{:S(2)}, u32[]{:S(2)}) collective-permute-start(bf16[128,512]{1,0:T(8,128)(2,1)S(1)} %collective-permute-done.refs_1_), channel_id=1, source_target_pairs={{0,4},{4,0},{8,12},{12,8},{16,20},{20,16},{24,28},{28,24},{1,5},{5... | collective-permute-start | bytes 393224 | tf_op jit(solution)/shard_map/ppermute | solution.py:63
  51.2 8.1 %shard_map.150 = (f32[256,512]{1,0:T(8,128)}, f32[32,512]{1,0:T(8,128)}) custom-call(s32[2]{0:T(128)S(1)} %pad_add_fusion.place, bf16[256,512]{1,0:T(8,128)(2,1)} %get-tuple-element.20.qt_ref, bf16[128,512]{1,0:T(8,128)(2,1)S(1)} %get-tuple-element.21.refs_0_, bf16[128,512]{1,0:T(8,128)(2,1)S(1)} %collective-permute-done.refs_1_, ...), custom_call_target="tpu_custom_call" | custom-call | flops 3500000000 | tf_op jit(solution)/shard_map/pallas_call | solution.py:38
  59.4 0.0 collective-permute-done.13.refs_1_
  59.4 0.7 collective-permute-start.5
  60.1 0.0 collective-permute-done.15.refs_3_
  60.1 1.3 %collective-permute-start.6 = (bf16[128,512]{1,0:T(8,128)(2,1)S(1)}, bf16[128,512]{1,0:T(8,128)(2,1)S(1)}, u32[]{:S(2)}, u32[]{:S(2)}) collective-permute-start(bf16[128,512]{1,0:T(8,128)(2,1)S(1)} %collective-permute-done.2.refs_3_), channel_id=1, source_target_pairs={{0,4},{4,0},{8,12},{12,8},{16,20},{20,16},{24,28},{28,24},{1,5},{5... | collective-permute-start | bytes 393224 | tf_op jit(solution)/shard_map/ppermute | solution.py:63
  61.4 8.7 %shard_map.154 = (bf16[256,512]{1,0:T(8,128)(2,1)S(1)}, bf16[256,512]{1,0:T(8,128)(2,1)S(1)}, bf16[256,512]{1,0:T(8,128)(2,1)S(1)}, bf16[256,512]{1,0:T(8,128)(2...) custom-call(s32[2]{0:T(128)S(1)} %pad_add_fusion.place, ...), custom_call_target="tpu_custom_call" | custom-call | flops 4499999744 | tf_op jit(solution)/shard_map/pallas_call | solution.py:38
  70.1 0.0 collective-permute-done.3.refs_2_
  70.1 0.1 collective-permute-start.10
  70.2 0.0 collective-permute-done.11.refs_6_
  70.2 0.5 collective-permute-start.12
  70.7 0.0 collective-permute-done.4.refs_3_
  70.7 0.1 collective-permute-start.24
  70.8 0.0 collective-permute-done.5.refs_4_
  70.8 0.4 collective-permute-start.17
  71.2 0.0 collective-permute-done.6.refs_5_
  71.2 7.5 %shard_map.151 = (bf16[128,256]{1,0:T(8,128)(2,1)S(1)}, bf16[128,256]{1,0:T(8,128)(2,1)S(1)}, bf16[128,256]{1,0:T(8,128)(2,1)S(1)}, bf16[128,256]{1,0:T(8,128)(2,1)S(1)}) custom-call(s32[2]{0:T(128)S(1)} %pad_add_fusion.place, bf16[256,512]{1,0:T(8,128)(2,1)} %get-tuple-element.20.qt_ref, f32[256,512]{1,0:T(8,128)} %get-tuple-element.22.refs_0_, ...), custom_call_target="tpu_custom_call" | custom-call | flops 3500000000 | tf_op jit(solution)/shard_map/pallas_call | solution.py:38
  78.7 0.2 collective-permute-start.7
  78.9 0.0 collective-permute-done.24
  78.9 0.4 collective-permute-start.23
  79.3 0.1 add_convert_fusion
  79.4 0.7 collective-permute-done.7.refs_1_
  80.0 0.2 collective-permute-start.16
  80.2 0.0 collective-permute-done.17
  80.2 1.5 %collective-permute-start.25 = (bf16[256,512]{1,0:T(8,128)(2,1)S(1)}, bf16[256,512]{1,0:T(8,128)(2,1)S(1)}, u32[]{:S(2)}, u32[]{:S(2)}) collective-permute-start(bf16[256,512]{1,0:T(8,128)(2,1)S(1)} %add_convert_fusion), channel_id=1, source_target_pairs={{0,2},{1,3},{2,0},{3,1},{4,6},{5,7},{6,4},{7,5},{8,10},{9,11},{10,... | collective-permute-start | bytes 786440 | tf_op jit(solution)/shard_map/ppermute | solution.py:63
  81.7 0.1 add_convert_fusion.1
  81.8 0.0 collective-permute-done.23
  81.8 0.6 collective-permute-start.18
  82.4 7.0 %collective-permute-done.25 = bf16[256,512]{1,0:T(8,128)(2,1)S(1)} collective-permute-done((bf16[256,512]{1,0:T(8,128)(2,1)S(1)}, bf16[256,512]{1,0:T(8,128)(2,1)S(1)}, u32[]{:S(2)}, u32[]{:S(2)}) %collective-permute-start.25) | collective-permute-done | bytes 262176 | tf_op jit(solution)/shard_map/ppermute | solution.py:63
  89.4 1.5 %collective-permute-start.8 = (bf16[128,256]{1,0:T(8,128)(2,1)S(1)}, bf16[128,256]{1,0:T(8,128)(2,1)S(1)}, u32[]{:S(2)}, u32[]{:S(2)}) collective-permute-start(bf16[128,256]{1,0:T(8,128)(2,1)S(1)} %get-tuple-element.26), channel_id=1, source_target_pairs={{0,2},{1,3},{2,0},{3,1},{4,6},{5,7},{6,4},{7,5},{8,10},{9,11},{10,... | collective-permute-start | bytes 196616 | tf_op jit(solution)/shard_map/ppermute | solution.py:63
  90.9 0.1 add_convert_fusion.2
  91.0 4.8 %collective-permute-done.8.refs_2_ = bf16[128,256]{1,0:T(8,128)(2,1)S(1)} collective-permute-done((bf16[128,256]{1,0:T(8,128)(2,1)S(1)}, bf16[128,256]{1,0:T(8,128)(2,1)S(1)}, u32[]{:S(2)}, u32[]{:S(2)}) %collective-permute-start.8) | collective-permute-done | bytes 65568 | tf_op jit(solution)/shard_map/ppermute | solution.py:63
  95.8 0.6 collective-permute-start.9
  96.4 0.0 collective-permute-done.16
  96.4 0.7 collective-permute-start.26
  97.1 0.0 collective-permute-done.18
  97.1 0.1 add_convert_fusion.6
  97.2 2.9 %collective-permute-done.9.refs_3_ = bf16[128,256]{1,0:T(8,128)(2,1)S(1)} collective-permute-done((bf16[128,256]{1,0:T(8,128)(2,1)S(1)}, bf16[128,256]{1,0:T(8,128)(2,1)S(1)}, u32[]{:S(2)}, u32[]{:S(2)}) %collective-permute-start.9) | collective-permute-done | bytes 65568 | tf_op jit(solution)/shard_map/ppermute | solution.py:63
  100.1 2.7 %collective-permute-start.19 = (bf16[64,512]{1,0:T(8,128)(2,1)S(1)}, bf16[64,512]{1,0:T(8,128)(2,1)S(1)}, u32[]{:S(2)}, u32[]{:S(2)}) collective-permute-start(bf16[64,512]{1,0:T(8,128)(2,1)S(1)} %get-tuple-element.45), channel_id=1, source_target_pairs={{0,16},{4,20},{8,24},{12,28},{16,0},{20,4},{24,8},{28,12},{1,17},{... | collective-permute-start | bytes 196616 | tf_op jit(solution)/shard_map/ppermute | solution.py:63
  102.8 0.4 collective-permute-start.20
  103.2 2.3 %collective-permute-start.21 = (bf16[64,512]{1,0:T(8,128)(2,1)S(1)}, bf16[64,512]{1,0:T(8,128)(2,1)S(1)}, u32[]{:S(2)}, u32[]{:S(2)}) collective-permute-start(bf16[64,512]{1,0:T(8,128)(2,1)S(1)} %get-tuple-element.43), channel_id=1, source_target_pairs={{0,24},{4,28},{8,16},{12,20},{16,8},{20,12},{24,0},{28,4},{1,25},{... | collective-permute-start | bytes 196616 | tf_op jit(solution)/shard_map/ppermute | solution.py:63
  105.5 2.3 %collective-permute-start.22 = (bf16[64,512]{1,0:T(8,128)(2,1)S(1)}, bf16[64,512]{1,0:T(8,128)(2,1)S(1)}, u32[]{:S(2)}, u32[]{:S(2)}) collective-permute-start(bf16[64,512]{1,0:T(8,128)(2,1)S(1)} %get-tuple-element.42), channel_id=1, source_target_pairs={{0,28},{4,24},{8,20},{12,16},{16,12},{20,8},{24,4},{28,0},{1,29},{... | collective-permute-start | bytes 196616 | tf_op jit(solution)/shard_map/ppermute | solution.py:63
  107.8 3.1 %shard_map.152 = bf16[128,2048]{1,0:T(8,128)(2,1)} custom-call(s32[2]{0:T(128)S(1)} %pad_add_fusion.place, bf16[128,256]{1,0:T(8,128)(2,1)S(1)} %get-tuple-element.24.refs_0_, bf16[128,256]{1,0:T(8,128)(2,1)S(1)} %collective-permute-done.7.refs_1_, bf16[128,256]{1,0:T(8,128)(2,1)S(1)} %collective-permute-done.8.refs_2_, ...), custom_call_target="tpu_custom_call" | custom-call | flops 1250000000 | tf_op jit(solution)/shard_map/pallas_call | solution.py:38
  110.9 0.0 collective-permute-done.19.refs_0_
  110.9 2.1 %collective-permute-done.20.refs_1_ = bf16[64,512]{1,0:T(8,128)(2,1)S(1)} collective-permute-done((bf16[64,512]{1,0:T(8,128)(2,1)S(1)}, bf16[64,512]{1,0:T(8,128)(2,1)S(1)}, u32[]{:S(2)}, u32[]{:S(2)}) %collective-permute-start.20) | collective-permute-done | bytes 65568 | tf_op jit(solution)/shard_map/ppermute | solution.py:63
  113.0 0.0 collective-permute-done.21.refs_2_
  113.0 0.0 collective-permute-done.22.refs_3_
  113.0 1.6 %shard_map.155 = bf16[160,512]{1,0:T(8,128)(2,1)} custom-call(s32[2]{0:T(128)S(1)} %pad_add_fusion.place, s32[2,160]{1,0:T(2,128)S(1)} %get-tuple-element.28.slot_ref, f32[2,160]{1,0:T(2,128)S(1)} %bitcast.19, bf16[64,512]{1,0:T(8,128)(2,1)S(1)} %collective-permute-done.19.refs_0_, bf16[64,512]{1,0:T(8,128)(2,1)S(1)} %collective-permute-done.20.refs_1_, ...), custom_call_target="tpu_custom_call" | custom-call | flops 750000000 | tf_op jit(solution)/shard_map/pallas_call | solution.py:38
  (17 shorter events, 0.0 us)
Async XLA Ops:
  24.8 14.8 %collective-permute-start.14 = (bf16[512,512]{1,0:T(8,128)(2,1)S(1)}, bf16[512,512]{1,0:T(8,128)(2,1)S(1)}, u32[]{:S(2)}, u32[]{:S(2)}) collective-permute-start(bf16[512,512]{1,0:T(8,128)(2,1)S(1)} %bitcast.12), channel_id=1, source_target_pairs={{0,2},{1,3},{2,0},{3,1},{4,6},{5,7},{6,4},{7,5},{8,10},{9,11},{10,... | collective-permute-start | bytes 1572872 | tf_op jit(solution)/shard_map/ppermute | solution.py:63
  26.3 43.9 %collective-permute-start.11 = (bf16[256,2048]{1,0:T(8,128)(2,1)}, bf16[256,2048]{1,0:T(8,128)(2,1)S(1)}, u32[]{:S(2)}, u32[]{:S(2)}) collective-permute-start(bf16[256,2048]{1,0:T(8,128)(2,1)} %refs_4_.1), channel_id=1, source_target_pairs={{0,2},{1,3},{2,0},{3,1},{4,6},{5,7},{6,4},{7,5},{8,10},{9,11},{10,... | collective-permute-start | bytes 3145736 | tf_op jit(solution)/shard_map/ppermute | solution.py:63
  30.2 10.4 %collective-permute-start = (bf16[128,512]{1,0:T(8,128)(2,1)S(1)}, bf16[128,512]{1,0:T(8,128)(2,1)S(1)}, u32[]{:S(2)}, u32[]{:S(2)}) collective-permute-start(bf16[128,512]{1,0:T(8,128)(2,1)S(1)} %get-tuple-element.21.refs_0_), channel_id=1, source_target_pairs={{0,24},{4,28},{8,16},{12,20},{16,8},{20,12},{24,0},{28,4},{1,25},{... | collective-permute-start | bytes 393224 | tf_op jit(solution)/shard_map/ppermute | solution.py:63
  31.5 27.9 %collective-permute-start.13 = (bf16[512,512]{1,0:T(8,128)(2,1)S(1)}, bf16[512,512]{1,0:T(8,128)(2,1)S(1)}, u32[]{:S(2)}, u32[]{:S(2)}) collective-permute-start(bf16[512,512]{1,0:T(8,128)(2,1)S(1)} %bitcast.13), channel_id=1, source_target_pairs={{0,1},{1,0},{2,3},{3,2},{4,5},{5,4},{6,7},{7,6},{8,9},{9,8},{10,11... | collective-permute-start | bytes 1572872 | tf_op jit(solution)/shard_map/ppermute | solution.py:63
  39.6 20.5 %collective-permute-start.15 = (bf16[512,512]{1,0:T(8,128)(2,1)S(1)}, bf16[512,512]{1,0:T(8,128)(2,1)S(1)}, u32[]{:S(2)}, u32[]{:S(2)}) collective-permute-start(bf16[512,512]{1,0:T(8,128)(2,1)S(1)} %collective-permute-done.14.refs_2_), channel_id=1, source_target_pairs={{0,1},{1,0},{2,3},{3,2},{4,5},{5,4},{6,7},{7,6},{8,9},{9,8},{10,11... | collective-permute-start | bytes 1572872 | tf_op jit(solution)/shard_map/ppermute | solution.py:63
  39.6 9.6 %collective-permute-start.1 = (bf16[128,512]{1,0:T(8,128)(2,1)S(1)}, bf16[128,512]{1,0:T(8,128)(2,1)S(1)}, u32[]{:S(2)}, u32[]{:S(2)}) collective-permute-start(bf16[128,512]{1,0:T(8,128)(2,1)S(1)} %get-tuple-element.21.refs_0_), channel_id=1, source_target_pairs={{0,16},{4,20},{8,24},{12,28},{16,0},{20,4},{24,8},{28,12},{1,17},{... | collective-permute-start | bytes 393224 | tf_op jit(solution)/shard_map/ppermute | solution.py:63
  40.6 9.3 %collective-permute-start.2 = (bf16[128,512]{1,0:T(8,128)(2,1)S(1)}, bf16[128,512]{1,0:T(8,128)(2,1)S(1)}, u32[]{:S(2)}, u32[]{:S(2)}) collective-permute-start(bf16[128,512]{1,0:T(8,128)(2,1)S(1)} %get-tuple-element.21.refs_0_), channel_id=1, source_target_pairs={{0,8},{4,12},{8,0},{12,4},{16,24},{20,28},{24,16},{28,20},{1,9},{5... | collective-permute-start | bytes 393224 | tf_op jit(solution)/shard_map/ppermute | solution.py:63
  49.2 20.9 %collective-permute-start.3 = (bf16[128,512]{1,0:T(8,128)(2,1)S(1)}, bf16[128,512]{1,0:T(8,128)(2,1)S(1)}, u32[]{:S(2)}, u32[]{:S(2)}) collective-permute-start(bf16[128,512]{1,0:T(8,128)(2,1)S(1)} %get-tuple-element.21.refs_0_), channel_id=1, source_target_pairs={{0,4},{4,0},{8,12},{12,8},{16,20},{20,16},{24,28},{28,24},{1,5},{5... | collective-permute-start | bytes 393224 | tf_op jit(solution)/shard_map/ppermute | solution.py:63
  49.9 20.8 %collective-permute-start.4 = (bf16[128,512]{1,0:T(8,128)(2,1)S(1)}, bf16[128,512]{1,0:T(8,128)(2,1)S(1)}, u32[]{:S(2)}, u32[]{:S(2)}) collective-permute-start(bf16[128,512]{1,0:T(8,128)(2,1)S(1)} %collective-permute-done.refs_1_), channel_id=1, source_target_pairs={{0,4},{4,0},{8,12},{12,8},{16,20},{20,16},{24,28},{28,24},{1,5},{5... | collective-permute-start | bytes 393224 | tf_op jit(solution)/shard_map/ppermute | solution.py:63
  51.2 10.2 %copy-start.1 = (bf16[1,2048,1024]{2,1,0:T(8,128)(2,1)S(1)}, bf16[1,2048,1024]{2,1,0:T(8,128)(2,1)}, u32[]{:S(2)}) copy-start(bf16[1,2048,1024]{2,1,0:T(8,128)(2,1)} %param.24) | copy-start | bytes 12582916
  51.2 10.2 %copy-start.2 = (bf16[1,2048,1024]{2,1,0:T(8,128)(2,1)S(1)}, bf16[1,2048,1024]{2,1,0:T(8,128)(2,1)}, u32[]{:S(2)}) copy-start(bf16[1,2048,1024]{2,1,0:T(8,128)(2,1)} %param.25) | copy-start | bytes 12582916
  51.2 10.2 %copy-start.3 = (bf16[1,1024,2048]{2,1,0:T(8,128)(2,1)S(1)}, bf16[1,1024,2048]{2,1,0:T(8,128)(2,1)}, u32[]{:S(2)}) copy-start(bf16[1,1024,2048]{2,1,0:T(8,128)(2,1)} %param.26) | copy-start | bytes 12582916
  59.4 11.4 %collective-permute-start.5 = (bf16[128,512]{1,0:T(8,128)(2,1)S(1)}, bf16[128,512]{1,0:T(8,128)(2,1)S(1)}, u32[]{:S(2)}, u32[]{:S(2)}) collective-permute-start(bf16[128,512]{1,0:T(8,128)(2,1)S(1)} %collective-permute-done.1.refs_2_), channel_id=1, source_target_pairs={{0,4},{4,0},{8,12},{12,8},{16,20},{20,16},{24,28},{28,24},{1,5},{5... | collective-permute-start | bytes 393224 | tf_op jit(solution)/shard_map/ppermute | solution.py:63
  60.1 11.1 %collective-permute-start.6 = (bf16[128,512]{1,0:T(8,128)(2,1)S(1)}, bf16[128,512]{1,0:T(8,128)(2,1)S(1)}, u32[]{:S(2)}, u32[]{:S(2)}) collective-permute-start(bf16[128,512]{1,0:T(8,128)(2,1)S(1)} %collective-permute-done.2.refs_3_), channel_id=1, source_target_pairs={{0,4},{4,0},{8,12},{12,8},{16,20},{20,16},{24,28},{28,24},{1,5},{5... | collective-permute-start | bytes 393224 | tf_op jit(solution)/shard_map/ppermute | solution.py:63
  61.4 8.7 %copy-start = (bf16[256,2048]{1,0:T(8,128)(2,1)S(1)}, bf16[256,2048]{1,0:T(8,128)(2,1)}, u32[]{:S(2)}) copy-start(bf16[256,2048]{1,0:T(8,128)(2,1)} %refs_4_.1) | copy-start | bytes 3145732
  70.1 30.0 %collective-permute-start.10 = (bf16[256,2048]{1,0:T(8,128)(2,1)S(1)}, bf16[256,2048]{1,0:T(8,128)(2,1)S(1)}, u32[]{:S(2)}, u32[]{:S(2)}) collective-permute-start(bf16[256,2048]{1,0:T(8,128)(2,1)S(1)} %copy-done), channel_id=1, source_target_pairs={{0,1},{1,0},{2,3},{3,2},{4,5},{5,4},{6,7},{7,6},{8,9},{9,8},{10,11... | collective-permute-start | bytes 3145736 | tf_op jit(solution)/shard_map/ppermute | solution.py:63
  70.2 32.6 %collective-permute-start.12 = (bf16[256,2048]{1,0:T(8,128)(2,1)S(1)}, bf16[256,2048]{1,0:T(8,128)(2,1)S(1)}, u32[]{:S(2)}, u32[]{:S(2)}) collective-permute-start(bf16[256,2048]{1,0:T(8,128)(2,1)S(1)} %collective-permute-done.11.refs_6_), channel_id=1, source_target_pairs={{0,1},{1,0},{2,3},{3,2},{4,5},{5,4},{6,7},{7,6},{8,9},{9,8},{10,11... | collective-permute-start | bytes 3145736 | tf_op jit(solution)/shard_map/ppermute | solution.py:63
  70.7 8.2 %collective-permute-start.24 = (bf16[256,512]{1,0:T(8,128)(2,1)S(1)}, bf16[256,512]{1,0:T(8,128)(2,1)S(1)}, u32[]{:S(2)}, u32[]{:S(2)}) collective-permute-start(bf16[256,512]{1,0:T(8,128)(2,1)S(1)} %get-tuple-element.37), channel_id=1, source_target_pairs={{0,1},{1,0},{2,3},{3,2},{4,5},{5,4},{6,7},{7,6},{8,9},{9,8},{10,11... | collective-permute-start | bytes 786440 | tf_op jit(solution)/shard_map/ppermute | solution.py:63
  70.8 9.4 %collective-permute-start.17 = (bf16[256,512]{1,0:T(8,128)(2,1)S(1)}, bf16[256,512]{1,0:T(8,128)(2,1)S(1)}, u32[]{:S(2)}, u32[]{:S(2)}) collective-permute-start(bf16[256,512]{1,0:T(8,128)(2,1)S(1)} %get-tuple-element.33), channel_id=1, source_target_pairs={{0,1},{1,0},{2,3},{3,2},{4,5},{5,4},{6,7},{7,6},{8,9},{9,8},{10,11... | collective-permute-start | bytes 786440 | tf_op jit(solution)/shard_map/ppermute | solution.py:63
  78.7 1.3 %collective-permute-start.7 = (bf16[128,256]{1,0:T(8,128)(2,1)S(1)}, bf16[128,256]{1,0:T(8,128)(2,1)S(1)}, u32[]{:S(2)}, u32[]{:S(2)}) collective-permute-start(bf16[128,256]{1,0:T(8,128)(2,1)S(1)} %get-tuple-element.25), channel_id=1, source_target_pairs={{0,1},{1,0},{2,3},{3,2},{4,5},{5,4},{6,7},{7,6},{8,9},{9,8},{10,11... | collective-permute-start | bytes 196616 | tf_op jit(solution)/shard_map/ppermute | solution.py:63
  78.9 2.9 %collective-permute-start.23 = (bf16[256,512]{1,0:T(8,128)(2,1)S(1)}, bf16[256,512]{1,0:T(8,128)(2,1)S(1)}, u32[]{:S(2)}, u32[]{:S(2)}) collective-permute-start(bf16[256,512]{1,0:T(8,128)(2,1)S(1)} %get-tuple-element.35), channel_id=1, source_target_pairs={{0,1},{1,0},{2,3},{3,2},{4,5},{5,4},{6,7},{7,6},{8,9},{9,8},{10,11... | collective-permute-start | bytes 786440 | tf_op jit(solution)/shard_map/ppermute | solution.py:63
  79.3 33.7 %copy-start.4 = (f32[160,2]{0,1:T(2,128)S(1)}, f32[160,2]{0,1:T(2,128)}, u32[]{:S(2)}) copy-start(f32[160,2]{0,1:T(2,128)} %param.23) | copy-start | bytes 3844
  80.0 16.4 %collective-permute-start.16 = (bf16[256,512]{1,0:T(8,128)(2,1)S(1)}, bf16[256,512]{1,0:T(8,128)(2,1)S(1)}, u32[]{:S(2)}, u32[]{:S(2)}) collective-permute-start(bf16[256,512]{1,0:T(8,128)(2,1)S(1)} %get-tuple-element.31), channel_id=1, source_target_pairs={{0,1},{1,0},{2,3},{3,2},{4,5},{5,4},{6,7},{7,6},{8,9},{9,8},{10,11... | collective-permute-start | bytes 786440 | tf_op jit(solution)/shard_map/ppermute | solution.py:63
  80.2 9.2 %collective-permute-start.25 = (bf16[256,512]{1,0:T(8,128)(2,1)S(1)}, bf16[256,512]{1,0:T(8,128)(2,1)S(1)}, u32[]{:S(2)}, u32[]{:S(2)}) collective-permute-start(bf16[256,512]{1,0:T(8,128)(2,1)S(1)} %add_convert_fusion), channel_id=1, source_target_pairs={{0,2},{1,3},{2,0},{3,1},{4,6},{5,7},{6,4},{7,5},{8,10},{9,11},{10,... | collective-permute-start | bytes 786440 | tf_op jit(solution)/shard_map/ppermute | solution.py:63
  81.8 15.3 %collective-permute-start.18 = (bf16[256,512]{1,0:T(8,128)(2,1)S(1)}, bf16[256,512]{1,0:T(8,128)(2,1)S(1)}, u32[]{:S(2)}, u32[]{:S(2)}) collective-permute-start(bf16[256,512]{1,0:T(8,128)(2,1)S(1)} %add_convert_fusion.1), channel_id=1, source_target_pairs={{0,2},{1,3},{2,0},{3,1},{4,6},{5,7},{6,4},{7,5},{8,10},{9,11},{10,... | collective-permute-start | bytes 786440 | tf_op jit(solution)/shard_map/ppermute | solution.py:63
  89.4 6.4 %collective-permute-start.8 = (bf16[128,256]{1,0:T(8,128)(2,1)S(1)}, bf16[128,256]{1,0:T(8,128)(2,1)S(1)}, u32[]{:S(2)}, u32[]{:S(2)}) collective-permute-start(bf16[128,256]{1,0:T(8,128)(2,1)S(1)} %get-tuple-element.26), channel_id=1, source_target_pairs={{0,2},{1,3},{2,0},{3,1},{4,6},{5,7},{6,4},{7,5},{8,10},{9,11},{10,... | collective-permute-start | bytes 196616 | tf_op jit(solution)/shard_map/ppermute | solution.py:63
  95.8 4.3 %collective-permute-start.9 = (bf16[128,256]{1,0:T(8,128)(2,1)S(1)}, bf16[128,256]{1,0:T(8,128)(2,1)S(1)}, u32[]{:S(2)}, u32[]{:S(2)}) collective-permute-start(bf16[128,256]{1,0:T(8,128)(2,1)S(1)} %get-tuple-element.27), channel_id=1, source_target_pairs={{0,3},{1,2},{2,1},{3,0},{4,7},{5,6},{6,5},{7,4},{8,11},{9,10},{10,... | collective-permute-start | bytes 196616 | tf_op jit(solution)/shard_map/ppermute | solution.py:63
  96.4 6.8 %collective-permute-start.26 = (bf16[64,512]{1,0:T(8,128)(2,1)S(1)}, bf16[64,512]{1,0:T(8,128)(2,1)S(1)}, u32[]{:S(2)}, u32[]{:S(2)}) collective-permute-start(bf16[64,512]{1,0:T(8,128)(2,1)S(1)} %get-tuple-element.40), channel_id=1, source_target_pairs={{0,4},{4,0},{8,12},{12,8},{16,20},{20,16},{24,28},{28,24},{1,5},{5... | collective-permute-start | bytes 196616 | tf_op jit(solution)/shard_map/ppermute | solution.py:63
  97.1 8.4 %collective-permute-start.27 = (bf16[64,512]{1,0:T(8,128)(2,1)S(1)}, bf16[64,512]{1,0:T(8,128)(2,1)S(1)}, u32[]{:S(2)}, u32[]{:S(2)}) collective-permute-start(bf16[64,512]{1,0:T(8,128)(2,1)S(1)} %get-tuple-element.39), channel_id=1, source_target_pairs={{0,8},{4,12},{8,0},{12,4},{16,24},{20,28},{24,16},{28,20},{1,9},{5... | collective-permute-start | bytes 196616 | tf_op jit(solution)/shard_map/ppermute | solution.py:63
  100.1 10.7 %collective-permute-start.28 = (bf16[64,512]{1,0:T(8,128)(2,1)S(1)}, bf16[64,512]{1,0:T(8,128)(2,1)S(1)}, u32[]{:S(2)}, u32[]{:S(2)}) collective-permute-start(bf16[64,512]{1,0:T(8,128)(2,1)S(1)} %get-tuple-element.38), channel_id=1, source_target_pairs={{0,12},{4,8},{8,4},{12,0},{16,28},{20,24},{24,20},{28,16},{1,13},{... | collective-permute-start | bytes 196616 | tf_op jit(solution)/shard_map/ppermute | solution.py:63
  100.1 10.7 %collective-permute-start.19 = (bf16[64,512]{1,0:T(8,128)(2,1)S(1)}, bf16[64,512]{1,0:T(8,128)(2,1)S(1)}, u32[]{:S(2)}, u32[]{:S(2)}) collective-permute-start(bf16[64,512]{1,0:T(8,128)(2,1)S(1)} %get-tuple-element.45), channel_id=1, source_target_pairs={{0,16},{4,20},{8,24},{12,28},{16,0},{20,4},{24,8},{28,12},{1,17},{... | collective-permute-start | bytes 196616 | tf_op jit(solution)/shard_map/ppermute | solution.py:63
  102.8 10.2 %collective-permute-start.20 = (bf16[64,512]{1,0:T(8,128)(2,1)S(1)}, bf16[64,512]{1,0:T(8,128)(2,1)S(1)}, u32[]{:S(2)}, u32[]{:S(2)}) collective-permute-start(bf16[64,512]{1,0:T(8,128)(2,1)S(1)} %get-tuple-element.44), channel_id=1, source_target_pairs={{0,20},{4,16},{8,28},{12,24},{16,4},{20,0},{24,12},{28,8},{1,21},{... | collective-permute-start | bytes 196616 | tf_op jit(solution)/shard_map/ppermute | solution.py:63
  103.2 9.8 %collective-permute-start.21 = (bf16[64,512]{1,0:T(8,128)(2,1)S(1)}, bf16[64,512]{1,0:T(8,128)(2,1)S(1)}, u32[]{:S(2)}, u32[]{:S(2)}) collective-permute-start(bf16[64,512]{1,0:T(8,128)(2,1)S(1)} %get-tuple-element.43), channel_id=1, source_target_pairs={{0,24},{4,28},{8,16},{12,20},{16,8},{20,12},{24,0},{28,4},{1,25},{... | collective-permute-start | bytes 196616 | tf_op jit(solution)/shard_map/ppermute | solution.py:63
  105.5 7.5 %collective-permute-start.22 = (bf16[64,512]{1,0:T(8,128)(2,1)S(1)}, bf16[64,512]{1,0:T(8,128)(2,1)S(1)}, u32[]{:S(2)}, u32[]{:S(2)}) collective-permute-start(bf16[64,512]{1,0:T(8,128)(2,1)S(1)} %get-tuple-element.42), channel_id=1, source_target_pairs={{0,28},{4,24},{8,20},{12,16},{16,12},{20,8},{24,4},{28,0},{1,29},{... | collective-permute-start | bytes 196616 | tf_op jit(solution)/shard_map/ppermute | solution.py:63

commit v4 on v3

--- a/solution.py
+++ b/solution.py
@@ -20,6 +20,7 @@
 BF16 = jnp.bfloat16
 VMEM_LIMIT = 24 * 1024 * 1024
 FLOPS_PER_MICRO = 500_000_000
+SPAN = 4
 
 
 def full(shape):
@@ -214,34 +215,27 @@
     )
 
 
-def attend_body(place, qt_ref, *refs, blocks, heads, count, groups):
+def attend_body(place, qt_ref, *refs, heads, count, groups):
+    sums = refs[: len(refs) - count - 4 - (groups + 1 if groups else 0)]
+    refs = refs[len(sums) :]
     if groups:
-        num_in, den_in = refs[:2]
-        refs = refs[2:]
         kv_refs, out_refs = refs[:count], refs[count : count + groups]
         out_ref, k_ref, v_ref, num_ref, den_ref = refs[count + groups :]
-        num_ref[...] = num_in[...]
-        den_ref[...] = den_in[...]
     else:
         kv_refs, (num_ref, den_ref, k_ref, v_ref) = refs[:count], refs[count:]
-        num_ref[...] = jnp.zeros_like(num_ref)
-        den_ref[...] = jnp.zeros_like(den_ref)
+    num_ref[...] = sums[0][...] if sums else jnp.zeros_like(num_ref)
+    den_ref[...] = sums[1][...] if sums else jnp.zeros_like(den_ref)
     keys = kv_refs[0].shape[1]
-    for b in range(blocks):
-        k_ref[b] = kv_refs[b][:HD, :].astype(F32).T.astype(BF16)
-        v_ref[b] = kv_refs[b][HD:, :]
-
-    def one(b, carry):
-        k = k_ref[b]
-        v = v_ref[b]
+    for b in range(count):
+        k_ref[b * keys : (b + 1) * keys, :] = kv_refs[b][:HD, :].astype(F32).T.astype(BF16)
+        v_ref[:, b * keys : (b + 1) * keys] = kv_refs[b][HD:, :]
+    for b in range(0, count, SPAN):
+        at = slice(b * keys, min(b + SPAN, count) * keys)
         for h in range(heads):
             q = qt_ref[h * HD : (h + 1) * HD, :]
-            p = jnp.exp2(mm(k, q) * (LOG2E * HD**-0.5))
-            den_ref[h * 8 : (h + 1) * 8, :] += jnp.sum(p.reshape(keys // 8, 8, p.shape[1]), axis=0)
-            num_ref[h * HD : (h + 1) * HD, :] += mm(v, p.astype(BF16))
-        return carry
-
-    lax.fori_loop(0, blocks, one, 0)
+            p = jnp.exp2(mm(k_ref[at, :], q) * (LOG2E * HD**-0.5))
+            den_ref[h * 8 : (h + 1) * 8, :] += jnp.sum(p.reshape(p.shape[0] // 8, 8, p.shape[1]), axis=0)
+            num_ref[h * HD : (h + 1) * HD, :] += mm(v_ref[:, at], p.astype(BF16))
     if groups:
         for h in range(heads):
             den = jnp.sum(den_ref[h * 8 : (h + 1) * 8, :], axis=0, keepdims=True)
@@ -258,20 +252,20 @@
     keys = kv_blocks[0].shape[1]
     count = len(kv_blocks)
     held = [pltpu.HBM(qt.shape, F32), pltpu.HBM((heads * 8, rows), F32)]
-    scratch = [pltpu.VMEM((count, keys, HD), BF16), pltpu.VMEM((count, HD, keys), BF16)]
+    scratch = [pltpu.VMEM((count * keys, HD), BF16), pltpu.VMEM((HD, count * keys), BF16)]
     if groups:
         outs = [jax.ShapeDtypeStruct((rows // groups, qt.shape[0]), BF16)] * groups
         scratch = [pltpu.VMEM((rows, qt.shape[0]), F32)] + scratch + [pltpu.VMEM(h.shape, F32) for h in held]
     else:
         outs = held
     return call(
-        functools.partial(attend_body, blocks=count, heads=heads, count=count, groups=groups),
+        functools.partial(attend_body, heads=heads, count=count, groups=groups),
         place,
         (qt, *sums, *kv_blocks),
         [full(qt.shape)] + [full(x.shape) for x in sums] + [full(b.shape) for b in kv_blocks],
         outs,
         scratch=scratch,
-        micros=7.0,
+        micros=1.4 * count,
     )
 
 
@@ -421,10 +415,9 @@
         *map(far_memory, (queries, key_input, value_input, query_gain[None], key_gain[None], table)),
         heads,
     )
-    blocks = [kvt]
-    blocks += [send(kvt, "ep", k) for k in range(n_ep - 2, 0, -2)]
-    blocks.append(send(kvt, "ep", 1))
-    blocks += [send(b, "ep", 1) for b in blocks[1:half]]
+    along = [send(kvt, "ep", k) for k in range(n_ep - 2, 0, -2)]
+    beside = send(kvt, "ep", 1)
+    across = [send(b, "ep", 1) for b in along]
 
     outbound, slot = dispatch(place, far_memory(routes.T), far_memory(expert_input), n_ep, cap, feat)
     arrived = lax.all_to_all(outbound, "ep", split_axis=0, concat_axis=0, tiled=True)
@@ -434,8 +427,10 @@
     for k in range(0, n_tp, 2):
         xs[k + 1] = send(xs[k], "tp", 1)
 
-    sums = attend(place, far_memory(qt), (), blocks[:half], heads, 0)
-    atts = attend(place, far_memory(qt), [far_memory(x) for x in sums], blocks[half:], heads, n_tp)
+    qt = far_memory(qt)
+    sums = attend(place, qt, (), [kvt, beside], heads, 0)
+    sums = attend(place, qt, [far_memory(x) for x in sums], along, heads, 0)
+    atts = attend(place, qt, [far_memory(x) for x in sums], across, heads, n_tp)
     atts = [atts[0]] + [send(atts[k], "tp", k) for k in range(1, n_tp)]
 
     parts = expert(

time: 115 us -> 121 us (1.052)
  starting transfers between devices: 23.4 us -> 27.6 us
  waiting for transfers between devices: 33.5 us -> 35.7 us
    ppermute x29, starting transfers between devices: 23.4 us -> 27.6 us  [send(): return lax.ppermute(x, axis, [(i, i ^ flip) for i in range(n)])]
    ppermute x29, waiting for transfers between devices: 33.5 us -> 35.7 us  [send(): return lax.ppermute(x, axis, [(i, i ^ flip) for i in range(n)])]
    pallas_call x7 -> x8, Pallas kernels: 34.9 us -> 35.1 us  [call(): pl.pallas_call(body, grid_spec=pltpu.PrefetchScalarGridSpec(num_scalar_pr...]
  transfers between devices with their start and end apart: 29 -> 29, of which waited for: 7 -> 9; matrix products, arithmetic and copies ran while one was open for 0% -> 0% of each run, Pallas kernels for 27% -> 25%
where the time goes in v4:
time: 121 us
  waiting for transfers between devices  35.7 us (30%)
  Pallas kernels  35.1 us (29%)
  starting transfers between devices  27.6 us (23%)
  blocking collectives  21.6 us (18%)
    ppermute x29, waiting for transfers between devices, send(): return lax.ppermute(x, axis, [(i, i ^ flip) for i in range(n)])  35.7 us
    pallas_call x8, Pallas kernels, call(): pl.pallas_call(body, grid_spec=pltpu.PrefetchScalarGridSpec(num_scalar_pr...  35.1 us
    ppermute x29, starting transfers between devices, send(): return lax.ppermute(x, axis, [(i, i ^ flip) for i in range(n)])  27.6 us
    all_to_all x1, blocking collectives, local(): lax.all_to_all(outbound, 'ep', split_axis=0, concat_axis=0, tiled=True)  21.6 us
  transfers between devices with their start and end apart: 29, of which 9 were waited for; matrix products, arithmetic and copies ran while one was open for 0% of the time, Pallas kernels for 25%

profile of v4, /device:TPU:0, one launch (start us, length us, event | category | flops | bytes accessed | tf_op | source)
XLA Modules:
  0.0 121.2 jit_solution(9202694444148173333)
XLA Ops:
  0.6 0.1 pad_add_fusion.place
  0.7 2.7 %shard_map.154 = (bf16[512,512]{1,0:T(8,128)(2,1)S(1)}, s32[2,160]{1,0:T(2,128)S(1)}) custom-call(s32[2]{0:T(128)S(1)} %pad_add_fusion.place, s32[2,160]{1,0:T(2,128)} %bitcast.21, bf16[160,2048]{1,0:T(8,128)(2,1)} %x_hbm.1), custom_call_target="tpu_custom_call" | custom-call | flops 750000000 | tf_op jit(solution)/shard_map/pallas_call | solution.py:39
  3.4 21.6 %all_to_all.11 = bf16[8,64,512]{2,1,0:T(8,128)(2,1)S(1)} all-to-all(bf16[8,64,512]{2,1,0:T(8,128)(2,1)S(1)} %bitcast.15), channel_id=1, replica_groups=mesh['ep'=8,'tp'=4] {'ep'}, dimensions={0} | all-to-all | bytes 1048576 | tf_op jit(solution)/shard_map/all_to_all | solution.py:423
  25.0 1.5 %collective-permute-start.14 = (bf16[512,512]{1,0:T(8,128)(2,1)S(1)}, bf16[512,512]{1,0:T(8,128)(2,1)S(1)}, u32[]{:S(2)}, u32[]{:S(2)}) collective-permute-start(bf16[512,512]{1,0:T(8,128)(2,1)S(1)} %bitcast.12), channel_id=1, source_target_pairs={{0,2},{1,3},{2,0},{3,1},{4,6},{5,7},{6,4},{7,5},{8,10},{9,11},{10,... | collective-permute-start | bytes 1572872 | tf_op jit(solution)/shard_map/ppermute | solution.py:64
  26.6 0.0 collective-permute-start.13
  26.6 11.0 %collective-permute-done.14.refs_2_ = bf16[512,512]{1,0:T(8,128)(2,1)S(1)} collective-permute-done((bf16[512,512]{1,0:T(8,128)(2,1)S(1)}, bf16[512,512]{1,0:T(8,128)(2,1)S(1)}, u32[]{:S(2)}, u32[]{:S(2)}) %collective-permute-start.14) | collective-permute-done | bytes 524320 | tf_op jit(solution)/shard_map/ppermute | solution.py:64
  37.6 0.0 collective-permute-start.15
  37.6 1.5 %collective-permute-start.11 = (bf16[256,2048]{1,0:T(8,128)(2,1)}, bf16[256,2048]{1,0:T(8,128)(2,1)S(1)}, u32[]{:S(2)}, u32[]{:S(2)}) collective-permute-start(bf16[256,2048]{1,0:T(8,128)(2,1)} %refs_4_.1), channel_id=1, source_target_pairs={{0,2},{1,3},{2,0},{3,1},{4,6},{5,7},{6,4},{7,5},{8,10},{9,11},{10,... | collective-permute-start | bytes 3145736 | tf_op jit(solution)/shard_map/ppermute | solution.py:64
  39.1 4.4 %shard_map.149 = (bf16[256,512]{1,0:T(8,128)(2,1)}, bf16[128,512]{1,0:T(8,128)(2,1)S(1)}) custom-call(s32[2]{0:T(128)S(1)} %pad_add_fusion.place, bf16[512,256]{1,0:T(8,128)(2,1)} %q_hbm.1, bf16[512,256]{1,0:T(8,128)(2,1)} %k_hbm.1, bf16[512,256]{1,0:T(8,128)(2,1)} %v_hbm.1, f32[1,64]{1,0:T(1,128)} %bitcast.22, f32[1,64]{1,0:T(1,128)} %bitcast.23, ...), custom_call_target="tpu_custom_call" | custom-call | flops 1000000000 | tf_op jit(solution)/shard_map/pallas_call | solution.py:39
  43.5 1.5 %collective-permute-start = (bf16[128,512]{1,0:T(8,128)(2,1)S(1)}, bf16[128,512]{1,0:T(8,128)(2,1)S(1)}, u32[]{:S(2)}, u32[]{:S(2)}) collective-permute-start(bf16[128,512]{1,0:T(8,128)(2,1)S(1)} %get-tuple-element.23.refs_0_), channel_id=1, source_target_pairs={{0,4},{4,0},{8,12},{12,8},{16,20},{20,16},{24,28},{28,24},{1,5},{5... | collective-permute-start | bytes 393224 | tf_op jit(solution)/shard_map/ppermute | solution.py:64
  45.0 2.2 %collective-permute-start.1 = (bf16[128,512]{1,0:T(8,128)(2,1)S(1)}, bf16[128,512]{1,0:T(8,128)(2,1)S(1)}, u32[]{:S(2)}, u32[]{:S(2)}) collective-permute-start(bf16[128,512]{1,0:T(8,128)(2,1)S(1)} %get-tuple-element.23.refs_0_), channel_id=1, source_target_pairs={{0,24},{4,28},{8,16},{12,20},{16,8},{20,12},{24,0},{28,4},{1,25},{... | collective-permute-start | bytes 393224 | tf_op jit(solution)/shard_map/ppermute | solution.py:64
  47.2 2.0 %collective-permute-done.refs_1_ = bf16[128,512]{1,0:T(8,128)(2,1)S(1)} collective-permute-done((bf16[128,512]{1,0:T(8,128)(2,1)S(1)}, bf16[128,512]{1,0:T(8,128)(2,1)S(1)}, u32[]{:S(2)}, u32[]{:S(2)}) %collective-permute-start) | collective-permute-done | bytes 131104 | tf_op jit(solution)/shard_map/ppermute | solution.py:64
  49.2 1.4 %collective-permute-start.2 = (bf16[128,512]{1,0:T(8,128)(2,1)S(1)}, bf16[128,512]{1,0:T(8,128)(2,1)S(1)}, u32[]{:S(2)}, u32[]{:S(2)}) collective-permute-start(bf16[128,512]{1,0:T(8,128)(2,1)S(1)} %get-tuple-element.23.refs_0_), channel_id=1, source_target_pairs={{0,16},{4,20},{8,24},{12,28},{16,0},{20,4},{24,8},{28,12},{1,17},{... | collective-permute-start | bytes 393224 | tf_op jit(solution)/shard_map/ppermute | solution.py:64
  50.6 1.7 %collective-permute-done.1.refs_2_ = bf16[128,512]{1,0:T(8,128)(2,1)S(1)} collective-permute-done((bf16[128,512]{1,0:T(8,128)(2,1)S(1)}, bf16[128,512]{1,0:T(8,128)(2,1)S(1)}, u32[]{:S(2)}, u32[]{:S(2)}) %collective-permute-start.1) | collective-permute-done | bytes 131104 | tf_op jit(solution)/shard_map/ppermute | solution.py:64
  52.3 0.0 collective-permute-start.3
  52.3 4.4 %shard_map.150 = (f32[256,512]{1,0:T(8,128)}, f32[32,512]{1,0:T(8,128)}) custom-call(s32[2]{0:T(128)S(1)} %pad_add_fusion.place, bf16[256,512]{1,0:T(8,128)(2,1)} %get-tuple-element.22.qt_ref, bf16[128,512]{1,0:T(8,128)(2,1)S(1)} %get-tuple-element.23.refs_0_, bf16[128,512]{1,0:T(8,128)(2,1)S(1)} %collective-permute-done.refs_1_), custom_call_target="tpu_custom_call" | custom-call | flops 1400000000 | tf_op jit(solution)/shard_map/pallas_call | solution.py:39
  56.7 1.4 %collective-permute-done.2.refs_3_ = bf16[128,512]{1,0:T(8,128)(2,1)S(1)} collective-permute-done((bf16[128,512]{1,0:T(8,128)(2,1)S(1)}, bf16[128,512]{1,0:T(8,128)(2,1)S(1)}, u32[]{:S(2)}, u32[]{:S(2)}) %collective-permute-start.2) | collective-permute-done | bytes 131104 | tf_op jit(solution)/shard_map/ppermute | solution.py:64
  58.0 4.5 %collective-permute-start.4 = (bf16[128,512]{1,0:T(8,128)(2,1)S(1)}, bf16[128,512]{1,0:T(8,128)(2,1)S(1)}, u32[]{:S(2)}, u32[]{:S(2)}) collective-permute-start(bf16[128,512]{1,0:T(8,128)(2,1)S(1)} %collective-permute-done.1.refs_2_), channel_id=1, source_target_pairs={{0,4},{4,0},{8,12},{12,8},{16,20},{20,16},{24,28},{28,24},{1,5},{5... | collective-permute-start | bytes 393224 | tf_op jit(solution)/shard_map/ppermute | solution.py:64
  62.6 0.0 collective-permute-done.3.refs_4_
  62.6 0.1 collective-permute-start.5
  62.6 0.0 collective-permute-done.13.refs_1_
  62.6 1.9 %collective-permute-start.6 = (bf16[128,512]{1,0:T(8,128)(2,1)S(1)}, bf16[128,512]{1,0:T(8,128)(2,1)S(1)}, u32[]{:S(2)}, u32[]{:S(2)}) collective-permute-start(bf16[128,512]{1,0:T(8,128)(2,1)S(1)} %collective-permute-done.3.refs_4_), channel_id=1, source_target_pairs={{0,4},{4,0},{8,12},{12,8},{16,20},{20,16},{24,28},{28,24},{1,5},{5... | collective-permute-start | bytes 393224 | tf_op jit(solution)/shard_map/ppermute | solution.py:64
  64.6 0.0 collective-permute-done.15.refs_3_
  64.6 8.7 %shard_map.155 = (bf16[256,512]{1,0:T(8,128)(2,1)S(1)}, bf16[256,512]{1,0:T(8,128)(2,1)S(1)}, bf16[256,512]{1,0:T(8,128)(2,1)S(1)}, bf16[256,512]{1,0:T(8,128)(2...) custom-call(s32[2]{0:T(128)S(1)} %pad_add_fusion.place, ...), custom_call_target="tpu_custom_call" | custom-call | flops 4499999744 | tf_op jit(solution)/shard_map/pallas_call | solution.py:39
  73.3 0.0 copy-start
  73.3 0.1 collective-permute-start.24
  73.4 5.4 %shard_map.151 = (f32[256,512]{1,0:T(8,128)}, f32[32,512]{1,0:T(8,128)}) custom-call(s32[2]{0:T(128)S(1)} %pad_add_fusion.place, bf16[256,512]{1,0:T(8,128)(2,1)} %get-tuple-element.22.qt_ref, f32[256,512]{1,0:T(8,128)} %get-tuple-element.24.refs_0_, f32[32,512]{1,0:T(8,128)} %get-tuple-element.25.refs_1_, ...), custom_call_target="tpu_custom_call" | custom-call | flops 2100000000 | tf_op jit(solution)/shard_map/pallas_call | solution.py:39
  78.8 0.0 collective-permute-done.4.refs_2_
  78.8 0.6 collective-permute-start.10
  79.4 0.0 collective-permute-done.11.refs_6_
  79.4 0.1 collective-permute-start.12
  79.4 0.0 collective-permute-done.5.refs_3_
  79.5 0.4 collective-permute-start.17
  79.9 0.0 collective-permute-done.6.refs_4_
  79.9 4.9 %shard_map.152 = (bf16[128,256]{1,0:T(8,128)(2,1)S(1)}, bf16[128,256]{1,0:T(8,128)(2,1)S(1)}, bf16[128,256]{1,0:T(8,128)(2,1)S(1)}, bf16[128,256]{1,0:T(8,128)(2,1)S(1)}) custom-call(s32[2]{0:T(128)S(1)} %pad_add_fusion.place, bf16[256,512]{1,0:T(8,128)(2,1)} %get-tuple-element.22.qt_ref, f32[256,512]{1,0:T(8,128)} %get-tuple-element.26.refs_0_, ...), custom_call_target="tpu_custom_call" | custom-call | flops 2100000000 | tf_op jit(solution)/shard_map/pallas_call | solution.py:39
  84.8 0.1 collective-permute-start.7
  85.0 0.4 collective-permute-start.23
  85.4 0.1 add_convert_fusion
  85.5 0.7 collective-permute-done.7.refs_1_
  86.1 0.2 collective-permute-start.16
  86.3 0.5 collective-permute-start.25
  86.8 0.1 add_convert_fusion.1
  86.9 1.6 %collective-permute-start.18 = (bf16[256,512]{1,0:T(8,128)(2,1)S(1)}, bf16[256,512]{1,0:T(8,128)(2,1)S(1)}, u32[]{:S(2)}, u32[]{:S(2)}) collective-permute-start(bf16[256,512]{1,0:T(8,128)(2,1)S(1)} %add_convert_fusion.1), channel_id=1, source_target_pairs={{0,2},{1,3},{2,0},{3,1},{4,6},{5,7},{6,4},{7,5},{8,10},{9,11},{10,... | collective-permute-start | bytes 786440 | tf_op jit(solution)/shard_map/ppermute | solution.py:64
  88.5 7.0 %collective-permute-done.25 = bf16[256,512]{1,0:T(8,128)(2,1)S(1)} collective-permute-done((bf16[256,512]{1,0:T(8,128)(2,1)S(1)}, bf16[256,512]{1,0:T(8,128)(2,1)S(1)}, u32[]{:S(2)}, u32[]{:S(2)}) %collective-permute-start.25) | collective-permute-done | bytes 262176 | tf_op jit(solution)/shard_map/ppermute | solution.py:64
  95.5 0.5 collective-permute-start.8
  96.0 0.1 add_convert_fusion.2
  96.1 5.8 %collective-permute-done.8.refs_2_ = bf16[128,256]{1,0:T(8,128)(2,1)S(1)} collective-permute-done((bf16[128,256]{1,0:T(8,128)(2,1)S(1)}, bf16[128,256]{1,0:T(8,128)(2,1)S(1)}, u32[]{:S(2)}, u32[]{:S(2)}) %collective-permute-start.8) | collective-permute-done | bytes 65568 | tf_op jit(solution)/shard_map/ppermute | solution.py:64
  101.9 0.0 collective-permute-start.9
  101.9 0.0 collective-permute-done.16
  101.9 0.1 collective-permute-start.26
  102.0 0.5 collective-permute-start.27
  102.5 0.1 add_convert_fusion.6
  102.6 3.3 %collective-permute-done.9.refs_3_ = bf16[128,256]{1,0:T(8,128)(2,1)S(1)} collective-permute-done((bf16[128,256]{1,0:T(8,128)(2,1)S(1)}, bf16[128,256]{1,0:T(8,128)(2,1)S(1)}, u32[]{:S(2)}, u32[]{:S(2)}) %collective-permute-start.9) | collective-permute-done | bytes 65568 | tf_op jit(solution)/shard_map/ppermute | solution.py:64
  105.9 0.0 collective-permute-start.28
  106.0 2.3 %collective-permute-start.19 = (bf16[64,512]{1,0:T(8,128)(2,1)S(1)}, bf16[64,512]{1,0:T(8,128)(2,1)S(1)}, u32[]{:S(2)}, u32[]{:S(2)}) collective-permute-start(bf16[64,512]{1,0:T(8,128)(2,1)S(1)} %get-tuple-element.49), channel_id=1, source_target_pairs={{0,16},{4,20},{8,24},{12,28},{16,0},{20,4},{24,8},{28,12},{1,17},{... | collective-permute-start | bytes 196616 | tf_op jit(solution)/shard_map/ppermute | solution.py:64
  108.3 0.0 collective-permute-done.12.refs_7_
  108.3 1.5 %collective-permute-start.20 = (bf16[64,512]{1,0:T(8,128)(2,1)S(1)}, bf16[64,512]{1,0:T(8,128)(2,1)S(1)}, u32[]{:S(2)}, u32[]{:S(2)}) collective-permute-start(bf16[64,512]{1,0:T(8,128)(2,1)S(1)} %get-tuple-element.48), channel_id=1, source_target_pairs={{0,20},{4,16},{8,28},{12,24},{16,4},{20,0},{24,12},{28,8},{1,21},{... | collective-permute-start | bytes 196616 | tf_op jit(solution)/shard_map/ppermute | solution.py:64
  109.8 0.0 collective-permute-done.26.refs_5_
  109.8 2.3 %collective-permute-start.21 = (bf16[64,512]{1,0:T(8,128)(2,1)S(1)}, bf16[64,512]{1,0:T(8,128)(2,1)S(1)}, u32[]{:S(2)}, u32[]{:S(2)}) collective-permute-start(bf16[64,512]{1,0:T(8,128)(2,1)S(1)} %get-tuple-element.47), channel_id=1, source_target_pairs={{0,24},{4,28},{8,16},{12,20},{16,8},{20,12},{24,0},{28,4},{1,25},{... | collective-permute-start | bytes 196616 | tf_op jit(solution)/shard_map/ppermute | solution.py:64
  112.0 0.0 collective-permute-done.27.refs_6_
  112.1 1.6 %collective-permute-start.22 = (bf16[64,512]{1,0:T(8,128)(2,1)S(1)}, bf16[64,512]{1,0:T(8,128)(2,1)S(1)}, u32[]{:S(2)}, u32[]{:S(2)}) collective-permute-start(bf16[64,512]{1,0:T(8,128)(2,1)S(1)} %get-tuple-element.46), channel_id=1, source_target_pairs={{0,28},{4,24},{8,20},{12,16},{16,12},{20,8},{24,4},{28,0},{1,29},{... | collective-permute-start | bytes 196616 | tf_op jit(solution)/shard_map/ppermute | solution.py:64
  113.7 3.1 %shard_map.153 = bf16[128,2048]{1,0:T(8,128)(2,1)} custom-call(s32[2]{0:T(128)S(1)} %pad_add_fusion.place, bf16[128,256]{1,0:T(8,128)(2,1)S(1)} %get-tuple-element.28.refs_0_, bf16[128,256]{1,0:T(8,128)(2,1)S(1)} %collective-permute-done.7.refs_1_, bf16[128,256]{1,0:T(8,128)(2,1)S(1)} %collective-permute-done.8.refs_2_, ...), custom_call_target="tpu_custom_call" | custom-call | flops 1250000000 | tf_op jit(solution)/shard_map/pallas_call | solution.py:39
  116.7 2.9 %collective-permute-done.20.refs_1_ = bf16[64,512]{1,0:T(8,128)(2,1)S(1)} collective-permute-done((bf16[64,512]{1,0:T(8,128)(2,1)S(1)}, bf16[64,512]{1,0:T(8,128)(2,1)S(1)}, u32[]{:S(2)}, u32[]{:S(2)}) %collective-permute-start.20) | collective-permute-done | bytes 65568 | tf_op jit(solution)/shard_map/ppermute | solution.py:64
  119.6 1.6 %shard_map.156 = bf16[160,512]{1,0:T(8,128)(2,1)} custom-call(s32[2]{0:T(128)S(1)} %pad_add_fusion.place, s32[2,160]{1,0:T(2,128)S(1)} %get-tuple-element.32.slot_ref, f32[2,160]{1,0:T(2,128)S(1)} %bitcast.19, bf16[64,512]{1,0:T(8,128)(2,1)S(1)} %collective-permute-done.19.refs_0_, bf16[64,512]{1,0:T(8,128)(2,1)S(1)} %collective-permute-done.20.refs_1_, ...), custom_call_target="tpu_custom_call" | custom-call | flops 750000000 | tf_op jit(solution)/shard_map/pallas_call | solution.py:39
  (18 shorter events, 0.0 us)
Async XLA Ops:
  0.7 63.9 %copy-start.3 = (bf16[1,1024,2048]{2,1,0:T(8,128)(2,1)S(1)}, bf16[1,1024,2048]{2,1,0:T(8,128)(2,1)}, u32[]{:S(2)}) copy-start(bf16[1,1024,2048]{2,1,0:T(8,128)(2,1)} %param.26) | copy-start | bytes 12582916
  25.0 12.5 %collective-permute-start.14 = (bf16[512,512]{1,0:T(8,128)(2,1)S(1)}, bf16[512,512]{1,0:T(8,128)(2,1)S(1)}, u32[]{:S(2)}, u32[]{:S(2)}) collective-permute-start(bf16[512,512]{1,0:T(8,128)(2,1)S(1)} %bitcast.12), channel_id=1, source_target_pairs={{0,2},{1,3},{2,0},{3,1},{4,6},{5,7},{6,4},{7,5},{8,10},{9,11},{10,... | collective-permute-start | bytes 1572872 | tf_op jit(solution)/shard_map/ppermute | solution.py:64
  26.6 36.1 %collective-permute-start.13 = (bf16[512,512]{1,0:T(8,128)(2,1)S(1)}, bf16[512,512]{1,0:T(8,128)(2,1)S(1)}, u32[]{:S(2)}, u32[]{:S(2)}) collective-permute-start(bf16[512,512]{1,0:T(8,128)(2,1)S(1)} %bitcast.13), channel_id=1, source_target_pairs={{0,1},{1,0},{2,3},{3,2},{4,5},{5,4},{6,7},{7,6},{8,9},{9,8},{10,11... | collective-permute-start | bytes 1572872 | tf_op jit(solution)/shard_map/ppermute | solution.py:64
  37.6 27.0 %collective-permute-start.15 = (bf16[512,512]{1,0:T(8,128)(2,1)S(1)}, bf16[512,512]{1,0:T(8,128)(2,1)S(1)}, u32[]{:S(2)}, u32[]{:S(2)}) collective-permute-start(bf16[512,512]{1,0:T(8,128)(2,1)S(1)} %collective-permute-done.14.refs_2_), channel_id=1, source_target_pairs={{0,1},{1,0},{2,3},{3,2},{4,5},{5,4},{6,7},{7,6},{8,9},{9,8},{10,11... | collective-permute-start | bytes 1572872 | tf_op jit(solution)/shard_map/ppermute | solution.py:64
  37.6 41.8 %collective-permute-start.11 = (bf16[256,2048]{1,0:T(8,128)(2,1)}, bf16[256,2048]{1,0:T(8,128)(2,1)S(1)}, u32[]{:S(2)}, u32[]{:S(2)}) collective-permute-start(bf16[256,2048]{1,0:T(8,128)(2,1)} %refs_4_.1), channel_id=1, source_target_pairs={{0,2},{1,3},{2,0},{3,1},{4,6},{5,7},{6,4},{7,5},{8,10},{9,11},{10,... | collective-permute-start | bytes 3145736 | tf_op jit(solution)/shard_map/ppermute | solution.py:64
  39.1 25.5 %copy-start.1 = (bf16[1,2048,1024]{2,1,0:T(8,128)(2,1)S(1)}, bf16[1,2048,1024]{2,1,0:T(8,128)(2,1)}, u32[]{:S(2)}) copy-start(bf16[1,2048,1024]{2,1,0:T(8,128)(2,1)} %param.24) | copy-start | bytes 12582916
  39.1 25.5 %copy-start.2 = (bf16[1,2048,1024]{2,1,0:T(8,128)(2,1)S(1)}, bf16[1,2048,1024]{2,1,0:T(8,128)(2,1)}, u32[]{:S(2)}) copy-start(bf16[1,2048,1024]{2,1,0:T(8,128)(2,1)} %param.25) | copy-start | bytes 12582916
  43.5 5.7 %collective-permute-start = (bf16[128,512]{1,0:T(8,128)(2,1)S(1)}, bf16[128,512]{1,0:T(8,128)(2,1)S(1)}, u32[]{:S(2)}, u32[]{:S(2)}) collective-permute-start(bf16[128,512]{1,0:T(8,128)(2,1)S(1)} %get-tuple-element.23.refs_0_), channel_id=1, source_target_pairs={{0,4},{4,0},{8,12},{12,8},{16,20},{20,16},{24,28},{28,24},{1,5},{5... | collective-permute-start | bytes 393224 | tf_op jit(solution)/shard_map/ppermute | solution.py:64
  45.0 7.3 %collective-permute-start.1 = (bf16[128,512]{1,0:T(8,128)(2,1)S(1)}, bf16[128,512]{1,0:T(8,128)(2,1)S(1)}, u32[]{:S(2)}, u32[]{:S(2)}) collective-permute-start(bf16[128,512]{1,0:T(8,128)(2,1)S(1)} %get-tuple-element.23.refs_0_), channel_id=1, source_target_pairs={{0,24},{4,28},{8,16},{12,20},{16,8},{20,12},{24,0},{28,4},{1,25},{... | collective-permute-start | bytes 393224 | tf_op jit(solution)/shard_map/ppermute | solution.py:64
  49.2 8.8 %collective-permute-start.2 = (bf16[128,512]{1,0:T(8,128)(2,1)S(1)}, bf16[128,512]{1,0:T(8,128)(2,1)S(1)}, u32[]{:S(2)}, u32[]{:S(2)}) collective-permute-start(bf16[128,512]{1,0:T(8,128)(2,1)S(1)} %get-tuple-element.23.refs_0_), channel_id=1, source_target_pairs={{0,16},{4,20},{8,24},{12,28},{16,0},{20,4},{24,8},{28,12},{1,17},{... | collective-permute-start | bytes 393224 | tf_op jit(solution)/shard_map/ppermute | solution.py:64
  52.3 10.3 %collective-permute-start.3 = (bf16[128,512]{1,0:T(8,128)(2,1)S(1)}, bf16[128,512]{1,0:T(8,128)(2,1)S(1)}, u32[]{:S(2)}, u32[]{:S(2)}) collective-permute-start(bf16[128,512]{1,0:T(8,128)(2,1)S(1)} %get-tuple-element.23.refs_0_), channel_id=1, source_target_pairs={{0,8},{4,12},{8,0},{12,4},{16,24},{20,28},{24,16},{28,20},{1,9},{5... | collective-permute-start | bytes 393224 | tf_op jit(solution)/shard_map/ppermute | solution.py:64
  58.0 20.8 %collective-permute-start.4 = (bf16[128,512]{1,0:T(8,128)(2,1)S(1)}, bf16[128,512]{1,0:T(8,128)(2,1)S(1)}, u32[]{:S(2)}, u32[]{:S(2)}) collective-permute-start(bf16[128,512]{1,0:T(8,128)(2,1)S(1)} %collective-permute-done.1.refs_2_), channel_id=1, source_target_pairs={{0,4},{4,0},{8,12},{12,8},{16,20},{20,16},{24,28},{28,24},{1,5},{5... | collective-permute-start | bytes 393224 | tf_op jit(solution)/shard_map/ppermute | solution.py:64
  62.6 16.9 %collective-permute-start.5 = (bf16[128,512]{1,0:T(8,128)(2,1)S(1)}, bf16[128,512]{1,0:T(8,128)(2,1)S(1)}, u32[]{:S(2)}, u32[]{:S(2)}) collective-permute-start(bf16[128,512]{1,0:T(8,128)(2,1)S(1)} %collective-permute-done.2.refs_3_), channel_id=1, source_target_pairs={{0,4},{4,0},{8,12},{12,8},{16,20},{20,16},{24,28},{28,24},{1,5},{5... | collective-permute-start | bytes 393224 | tf_op jit(solution)/shard_map/ppermute | solution.py:64
  62.6 17.2 %collective-permute-start.6 = (bf16[128,512]{1,0:T(8,128)(2,1)S(1)}, bf16[128,512]{1,0:T(8,128)(2,1)S(1)}, u32[]{:S(2)}, u32[]{:S(2)}) collective-permute-start(bf16[128,512]{1,0:T(8,128)(2,1)S(1)} %collective-permute-done.3.refs_4_), channel_id=1, source_target_pairs={{0,4},{4,0},{8,12},{12,8},{16,20},{20,16},{24,28},{28,24},{1,5},{5... | collective-permute-start | bytes 393224 | tf_op jit(solution)/shard_map/ppermute | solution.py:64
  73.3 5.5 %copy-start = (bf16[256,2048]{1,0:T(8,128)(2,1)S(1)}, bf16[256,2048]{1,0:T(8,128)(2,1)}, u32[]{:S(2)}) copy-start(bf16[256,2048]{1,0:T(8,128)(2,1)} %refs_4_.1) | copy-start | bytes 3145732
  73.3 11.6 %collective-permute-start.24 = (bf16[256,512]{1,0:T(8,128)(2,1)S(1)}, bf16[256,512]{1,0:T(8,128)(2,1)S(1)}, u32[]{:S(2)}, u32[]{:S(2)}) collective-permute-start(bf16[256,512]{1,0:T(8,128)(2,1)S(1)} %get-tuple-element.41), channel_id=1, source_target_pairs={{0,1},{1,0},{2,3},{3,2},{4,5},{5,4},{6,7},{7,6},{8,9},{9,8},{10,11... | collective-permute-start | bytes 786440 | tf_op jit(solution)/shard_map/ppermute | solution.py:64
  78.8 27.2 %collective-permute-start.10 = (bf16[256,2048]{1,0:T(8,128)(2,1)S(1)}, bf16[256,2048]{1,0:T(8,128)(2,1)S(1)}, u32[]{:S(2)}, u32[]{:S(2)}) collective-permute-start(bf16[256,2048]{1,0:T(8,128)(2,1)S(1)} %copy-done), channel_id=1, source_target_pairs={{0,1},{1,0},{2,3},{3,2},{4,5},{5,4},{6,7},{7,6},{8,9},{9,8},{10,11... | collective-permute-start | bytes 3145736 | tf_op jit(solution)/shard_map/ppermute | solution.py:64
  79.4 28.9 %collective-permute-start.12 = (bf16[256,2048]{1,0:T(8,128)(2,1)S(1)}, bf16[256,2048]{1,0:T(8,128)(2,1)S(1)}, u32[]{:S(2)}, u32[]{:S(2)}) collective-permute-start(bf16[256,2048]{1,0:T(8,128)(2,1)S(1)} %collective-permute-done.11.refs_6_), channel_id=1, source_target_pairs={{0,1},{1,0},{2,3},{3,2},{4,5},{5,4},{6,7},{7,6},{8,9},{9,8},{10,11... | collective-permute-start | bytes 3145736 | tf_op jit(solution)/shard_map/ppermute | solution.py:64
  79.5 6.8 %collective-permute-start.17 = (bf16[256,512]{1,0:T(8,128)(2,1)S(1)}, bf16[256,512]{1,0:T(8,128)(2,1)S(1)}, u32[]{:S(2)}, u32[]{:S(2)}) collective-permute-start(bf16[256,512]{1,0:T(8,128)(2,1)S(1)} %get-tuple-element.37), channel_id=1, source_target_pairs={{0,1},{1,0},{2,3},{3,2},{4,5},{5,4},{6,7},{7,6},{8,9},{9,8},{10,11... | collective-permute-start | bytes 786440 | tf_op jit(solution)/shard_map/ppermute | solution.py:64
  84.8 1.3 %collective-permute-start.7 = (bf16[128,256]{1,0:T(8,128)(2,1)S(1)}, bf16[128,256]{1,0:T(8,128)(2,1)S(1)}, u32[]{:S(2)}, u32[]{:S(2)}) collective-permute-start(bf16[128,256]{1,0:T(8,128)(2,1)S(1)} %get-tuple-element.29), channel_id=1, source_target_pairs={{0,1},{1,0},{2,3},{3,2},{4,5},{5,4},{6,7},{7,6},{8,9},{9,8},{10,11... | collective-permute-start | bytes 196616 | tf_op jit(solution)/shard_map/ppermute | solution.py:64
  85.0 1.9 %collective-permute-start.23 = (bf16[256,512]{1,0:T(8,128)(2,1)S(1)}, bf16[256,512]{1,0:T(8,128)(2,1)S(1)}, u32[]{:S(2)}, u32[]{:S(2)}) collective-permute-start(bf16[256,512]{1,0:T(8,128)(2,1)S(1)} %get-tuple-element.39), channel_id=1, source_target_pairs={{0,1},{1,0},{2,3},{3,2},{4,5},{5,4},{6,7},{7,6},{8,9},{9,8},{10,11... | collective-permute-start | bytes 786440 | tf_op jit(solution)/shard_map/ppermute | solution.py:64
  85.4 34.2 %copy-start.4 = (f32[160,2]{0,1:T(2,128)S(1)}, f32[160,2]{0,1:T(2,128)}, u32[]{:S(2)}) copy-start(f32[160,2]{0,1:T(2,128)} %param.23) | copy-start | bytes 3844
  86.1 15.8 %collective-permute-start.16 = (bf16[256,512]{1,0:T(8,128)(2,1)S(1)}, bf16[256,512]{1,0:T(8,128)(2,1)S(1)}, u32[]{:S(2)}, u32[]{:S(2)}) collective-permute-start(bf16[256,512]{1,0:T(8,128)(2,1)S(1)} %get-tuple-element.35), channel_id=1, source_target_pairs={{0,1},{1,0},{2,3},{3,2},{4,5},{5,4},{6,7},{7,6},{8,9},{9,8},{10,11... | collective-permute-start | bytes 786440 | tf_op jit(solution)/shard_map/ppermute | solution.py:64
  86.3 9.2 %collective-permute-start.25 = (bf16[256,512]{1,0:T(8,128)(2,1)S(1)}, bf16[256,512]{1,0:T(8,128)(2,1)S(1)}, u32[]{:S(2)}, u32[]{:S(2)}) collective-permute-start(bf16[256,512]{1,0:T(8,128)(2,1)S(1)} %add_convert_fusion), channel_id=1, source_target_pairs={{0,2},{1,3},{2,0},{3,1},{4,6},{5,7},{6,4},{7,5},{8,10},{9,11},{10,... | collective-permute-start | bytes 786440 | tf_op jit(solution)/shard_map/ppermute | solution.py:64
  86.9 15.1 %collective-permute-start.18 = (bf16[256,512]{1,0:T(8,128)(2,1)S(1)}, bf16[256,512]{1,0:T(8,128)(2,1)S(1)}, u32[]{:S(2)}, u32[]{:S(2)}) collective-permute-start(bf16[256,512]{1,0:T(8,128)(2,1)S(1)} %add_convert_fusion.1), channel_id=1, source_target_pairs={{0,2},{1,3},{2,0},{3,1},{4,6},{5,7},{6,4},{7,5},{8,10},{9,11},{10,... | collective-permute-start | bytes 786440 | tf_op jit(solution)/shard_map/ppermute | solution.py:64
  95.5 6.4 %collective-permute-start.8 = (bf16[128,256]{1,0:T(8,128)(2,1)S(1)}, bf16[128,256]{1,0:T(8,128)(2,1)S(1)}, u32[]{:S(2)}, u32[]{:S(2)}) collective-permute-start(bf16[128,256]{1,0:T(8,128)(2,1)S(1)} %get-tuple-element.30), channel_id=1, source_target_pairs={{0,2},{1,3},{2,0},{3,1},{4,6},{5,7},{6,4},{7,5},{8,10},{9,11},{10,... | collective-permute-start | bytes 196616 | tf_op jit(solution)/shard_map/ppermute | solution.py:64
  101.9 4.1 %collective-permute-start.9 = (bf16[128,256]{1,0:T(8,128)(2,1)S(1)}, bf16[128,256]{1,0:T(8,128)(2,1)S(1)}, u32[]{:S(2)}, u32[]{:S(2)}) collective-permute-start(bf16[128,256]{1,0:T(8,128)(2,1)S(1)} %get-tuple-element.31), channel_id=1, source_target_pairs={{0,3},{1,2},{2,1},{3,0},{4,7},{5,6},{6,5},{7,4},{8,11},{9,10},{10,... | collective-permute-start | bytes 196616 | tf_op jit(solution)/shard_map/ppermute | solution.py:64
  101.9 7.9 %collective-permute-start.26 = (bf16[64,512]{1,0:T(8,128)(2,1)S(1)}, bf16[64,512]{1,0:T(8,128)(2,1)S(1)}, u32[]{:S(2)}, u32[]{:S(2)}) collective-permute-start(bf16[64,512]{1,0:T(8,128)(2,1)S(1)} %get-tuple-element.44), channel_id=1, source_target_pairs={{0,4},{4,0},{8,12},{12,8},{16,20},{20,16},{24,28},{28,24},{1,5},{5... | collective-permute-start | bytes 196616 | tf_op jit(solution)/shard_map/ppermute | solution.py:64
  102.0 10.1 %collective-permute-start.27 = (bf16[64,512]{1,0:T(8,128)(2,1)S(1)}, bf16[64,512]{1,0:T(8,128)(2,1)S(1)}, u32[]{:S(2)}, u32[]{:S(2)}) collective-permute-start(bf16[64,512]{1,0:T(8,128)(2,1)S(1)} %get-tuple-element.43), channel_id=1, source_target_pairs={{0,8},{4,12},{8,0},{12,4},{16,24},{20,28},{24,16},{28,20},{1,9},{5... | collective-permute-start | bytes 196616 | tf_op jit(solution)/shard_map/ppermute | solution.py:64
  105.9 10.8 %collective-permute-start.28 = (bf16[64,512]{1,0:T(8,128)(2,1)S(1)}, bf16[64,512]{1,0:T(8,128)(2,1)S(1)}, u32[]{:S(2)}, u32[]{:S(2)}) collective-permute-start(bf16[64,512]{1,0:T(8,128)(2,1)S(1)} %get-tuple-element.42), channel_id=1, source_target_pairs={{0,12},{4,8},{8,4},{12,0},{16,28},{20,24},{24,20},{28,16},{1,13},{... | collective-permute-start | bytes 196616 | tf_op jit(solution)/shard_map/ppermute | solution.py:64
  106.0 10.7 %collective-permute-start.19 = (bf16[64,512]{1,0:T(8,128)(2,1)S(1)}, bf16[64,512]{1,0:T(8,128)(2,1)S(1)}, u32[]{:S(2)}, u32[]{:S(2)}) collective-permute-start(bf16[64,512]{1,0:T(8,128)(2,1)S(1)} %get-tuple-element.49), channel_id=1, source_target_pairs={{0,16},{4,20},{8,24},{12,28},{16,0},{20,4},{24,8},{28,12},{1,17},{... | collective-permute-start | bytes 196616 | tf_op jit(solution)/shard_map/ppermute | solution.py:64
  108.3 11.3 %collective-permute-start.20 = (bf16[64,512]{1,0:T(8,128)(2,1)S(1)}, bf16[64,512]{1,0:T(8,128)(2,1)S(1)}, u32[]{:S(2)}, u32[]{:S(2)}) collective-permute-start(bf16[64,512]{1,0:T(8,128)(2,1)S(1)} %get-tuple-element.48), channel_id=1, source_target_pairs={{0,20},{4,16},{8,28},{12,24},{16,4},{20,0},{24,12},{28,8},{1,21},{... | collective-permute-start | bytes 196616 | tf_op jit(solution)/shard_map/ppermute | solution.py:64
  109.8 9.8 %collective-permute-start.21 = (bf16[64,512]{1,0:T(8,128)(2,1)S(1)}, bf16[64,512]{1,0:T(8,128)(2,1)S(1)}, u32[]{:S(2)}, u32[]{:S(2)}) collective-permute-start(bf16[64,512]{1,0:T(8,128)(2,1)S(1)} %get-tuple-element.47), channel_id=1, source_target_pairs={{0,24},{4,28},{8,16},{12,20},{16,8},{20,12},{24,0},{28,4},{1,25},{... | collective-permute-start | bytes 196616 | tf_op jit(solution)/shard_map/ppermute | solution.py:64
  112.1 7.6 %collective-permute-start.22 = (bf16[64,512]{1,0:T(8,128)(2,1)S(1)}, bf16[64,512]{1,0:T(8,128)(2,1)S(1)}, u32[]{:S(2)}, u32[]{:S(2)}) collective-permute-start(bf16[64,512]{1,0:T(8,128)(2,1)S(1)} %get-tuple-element.46), channel_id=1, source_target_pairs={{0,28},{4,24},{8,20},{12,16},{16,12},{20,8},{24,4},{28,0},{1,29},{... | collective-permute-start | bytes 196616 | tf_op jit(solution)/shard_map/ppermute | solution.py:64

commit v5 on v4

--- a/solution.py
+++ b/solution.py
@@ -20,7 +20,7 @@
 BF16 = jnp.bfloat16
 VMEM_LIMIT = 24 * 1024 * 1024
 FLOPS_PER_MICRO = 500_000_000
-SPAN = 4
+SPAN = 6
 
 
 def full(shape):
@@ -226,11 +226,14 @@
     num_ref[...] = sums[0][...] if sums else jnp.zeros_like(num_ref)
     den_ref[...] = sums[1][...] if sums else jnp.zeros_like(den_ref)
     keys = kv_refs[0].shape[1]
-    for b in range(count):
-        k_ref[b * keys : (b + 1) * keys, :] = kv_refs[b][:HD, :].astype(F32).T.astype(BF16)
-        v_ref[:, b * keys : (b + 1) * keys] = kv_refs[b][HD:, :]
-    for b in range(0, count, SPAN):
-        at = slice(b * keys, min(b + SPAN, count) * keys)
+    per = kv_refs[0].shape[0] // (2 * HD)
+    blocks = count * per
+    for b in range(blocks):
+        base = (b % per) * 2 * HD
+        k_ref[b * keys : (b + 1) * keys, :] = kv_refs[b // per][base : base + HD, :].astype(F32).T.astype(BF16)
+        v_ref[:, b * keys : (b + 1) * keys] = kv_refs[b // per][base + HD : base + 2 * HD, :]
+    for b in range(0, blocks, SPAN):
+        at = slice(b * keys, min(b + SPAN, blocks) * keys)
         for h in range(heads):
             q = qt_ref[h * HD : (h + 1) * HD, :]
             p = jnp.exp2(mm(k_ref[at, :], q) * (LOG2E * HD**-0.5))
@@ -251,8 +254,9 @@
     rows = qt.shape[1]
     keys = kv_blocks[0].shape[1]
     count = len(kv_blocks)
+    total = sum(b.shape[0] for b in kv_blocks) // (2 * HD) * keys
     held = [pltpu.HBM(qt.shape, F32), pltpu.HBM((heads * 8, rows), F32)]
-    scratch = [pltpu.VMEM((count * keys, HD), BF16), pltpu.VMEM((HD, count * keys), BF16)]
+    scratch = [pltpu.VMEM((total, HD), BF16), pltpu.VMEM((HD, total), BF16)]
     if groups:
         outs = [jax.ShapeDtypeStruct((rows // groups, qt.shape[0]), BF16)] * groups
         scratch = [pltpu.VMEM((rows, qt.shape[0]), F32)] + scratch + [pltpu.VMEM(h.shape, F32) for h in held]
@@ -265,7 +269,7 @@
         [full(qt.shape)] + [full(x.shape) for x in sums] + [full(b.shape) for b in kv_blocks],
         outs,
         scratch=scratch,
-        micros=1.4 * count,
+        micros=16.0,
     )
 
 
@@ -415,9 +419,8 @@
         *map(far_memory, (queries, key_input, value_input, query_gain[None], key_gain[None], table)),
         heads,
     )
-    along = [send(kvt, "ep", k) for k in range(n_ep - 2, 0, -2)]
-    beside = send(kvt, "ep", 1)
-    across = [send(b, "ep", 1) for b in along]
+    pair = jnp.concatenate([kvt, send(kvt, "ep", 1)], axis=0)
+    along = [send(pair, "ep", k) for k in range(n_ep - 2, 0, -2)]
 
     outbound, slot = dispatch(place, far_memory(routes.T), far_memory(expert_input), n_ep, cap, feat)
     arrived = lax.all_to_all(outbound, "ep", split_axis=0, concat_axis=0, tiled=True)
@@ -428,9 +431,8 @@
         xs[k + 1] = send(xs[k], "tp", 1)
 
     qt = far_memory(qt)
-    sums = attend(place, qt, (), [kvt, beside], heads, 0)
-    sums = attend(place, qt, [far_memory(x) for x in sums], along, heads, 0)
-    atts = attend(place, qt, [far_memory(x) for x in sums], across, heads, n_tp)
+    sums = attend(place, qt, (), [pair], heads, 0)
+    atts = attend(place, qt, [far_memory(x) for x in sums], along, heads, n_tp)
     atts = [atts[0]] + [send(atts[k], "tp", k) for k in range(1, n_tp)]
 
     parts = expert(

time: 121 us -> 118 us (0.975)
  starting transfers between devices: 27.6 us -> 21.5 us
  waiting for transfers between devices: 35.7 us -> 41.6 us
  Pallas kernels: 35.1 us -> 31.5 us
    ppermute x29 -> x26, starting transfers between devices: 27.6 us -> 21.5 us  [send(): return lax.ppermute(x, axis, [(i, i ^ flip) for i in range(n)])]
    ppermute x29 -> x26, waiting for transfers between devices: 35.7 us -> 41.6 us  [send(): return lax.ppermute(x, axis, [(i, i ^ flip) for i in range(n)])]
    pallas_call x8 -> x7, Pallas kernels: 35.1 us -> 31.5 us  [call(): pl.pallas_call(body, grid_spec=pltpu.PrefetchScalarGridSpec(num_scalar_pr...]
  transfers between devices with their start and end apart: 29 -> 26, of which waited for: 9 -> 10; matrix products, arithmetic and copies ran while one was open for 0% -> 0% of each run, Pallas kernels for 25% -> 23%
where the time goes in v5:
time: 118 us
  waiting for transfers between devices  41.6 us (35%)
  Pallas kernels  31.5 us (27%)
  blocking collectives  21.6 us (18%)
  starting transfers between devices  21.5 us (18%)
    ppermute x26, waiting for transfers between devices, send(): return lax.ppermute(x, axis, [(i, i ^ flip) for i in range(n)])  41.6 us
    pallas_call x7, Pallas kernels, call(): pl.pallas_call(body, grid_spec=pltpu.PrefetchScalarGridSpec(num_scalar_pr...  31.5 us
    all_to_all x1, blocking collectives, local(): lax.all_to_all(outbound, 'ep', split_axis=0, concat_axis=0, tiled=True)  21.6 us
    ppermute x26, starting transfers between devices, send(): return lax.ppermute(x, axis, [(i, i ^ flip) for i in range(n)])  21.5 us
  transfers between devices with their start and end apart: 26, of which 10 were waited for; matrix products, arithmetic and copies ran while one was open for 0% of the time, Pallas kernels for 23%

profile of v5, /device:TPU:0, one launch (start us, length us, event | category | flops | bytes accessed | tf_op | source)
XLA Modules:
  0.0 117.5 jit_solution(14843315074380365333)
XLA Ops:
  0.6 0.0 copy-start
  0.6 0.1 pad_add_fusion.place
  0.7 2.4 %shard_map.153 = (bf16[512,512]{1,0:T(8,128)(2,1)S(1)}, s32[2,160]{1,0:T(2,128)S(1)}) custom-call(s32[2]{0:T(128)S(1)} %pad_add_fusion.place, s32[2,160]{1,0:T(2,128)} %bitcast.21, bf16[160,2048]{1,0:T(8,128)(2,1)} %x_hbm.1), custom_call_target="tpu_custom_call" | custom-call | flops 750000000 | tf_op jit(solution)/shard_map/pallas_call | solution.py:39
  3.2 21.6 %all_to_all.11 = bf16[8,64,512]{2,1,0:T(8,128)(2,1)S(1)} all-to-all(bf16[8,64,512]{2,1,0:T(8,128)(2,1)S(1)} %bitcast.15), channel_id=1, replica_groups=mesh['ep'=8,'tp'=4] {'ep'}, dimensions={0} | all-to-all | bytes 1048576 | tf_op jit(solution)/shard_map/all_to_all | solution.py:426
  24.8 1.5 %collective-permute-start.11 = (bf16[512,512]{1,0:T(8,128)(2,1)S(1)}, bf16[512,512]{1,0:T(8,128)(2,1)S(1)}, u32[]{:S(2)}, u32[]{:S(2)}) collective-permute-start(bf16[512,512]{1,0:T(8,128)(2,1)S(1)} %bitcast.12), channel_id=1, source_target_pairs={{0,2},{1,3},{2,0},{3,1},{4,6},{5,7},{6,4},{7,5},{8,10},{9,11},{10,... | collective-permute-start | bytes 1572872 | tf_op jit(solution)/shard_map/ppermute | solution.py:64
  26.3 0.5 collective-permute-start.8
  26.8 3.4 %shard_map.149 = (bf16[256,512]{1,0:T(8,128)(2,1)}, bf16[128,512]{1,0:T(8,128)(2,1)S(1)}) custom-call(s32[2]{0:T(128)S(1)} %pad_add_fusion.place, bf16[512,256]{1,0:T(8,128)(2,1)} %q_hbm.1, bf16[512,256]{1,0:T(8,128)(2,1)} %k_hbm.1, bf16[512,256]{1,0:T(8,128)(2,1)} %v_hbm.1, f32[1,64]{1,0:T(1,128)} %bitcast.22, f32[1,64]{1,0:T(1,128)} %bitcast.23, ...), custom_call_target="tpu_custom_call" | custom-call | flops 1000000000 | tf_op jit(solution)/shard_map/pallas_call | solution.py:39
  30.2 1.5 %collective-permute-start = (bf16[128,512]{1,0:T(8,128)(2,1)S(1)}, bf16[128,512]{1,0:T(8,128)(2,1)S(1)}, u32[]{:S(2)}, u32[]{:S(2)}) collective-permute-start(bf16[128,512]{1,0:T(8,128)(2,1)S(1)} %get-tuple-element.21), channel_id=1, source_target_pairs={{0,4},{4,0},{8,12},{12,8},{16,20},{20,16},{24,28},{28,24},{1,5},{5... | collective-permute-start | bytes 393224 | tf_op jit(solution)/shard_map/ppermute | solution.py:64
  31.7 0.0 collective-permute-start.7
  31.7 3.5 %collective-permute-done = bf16[128,512]{1,0:T(8,128)(2,1)S(1)} collective-permute-done((bf16[128,512]{1,0:T(8,128)(2,1)S(1)}, bf16[128,512]{1,0:T(8,128)(2,1)S(1)}, u32[]{:S(2)}, u32[]{:S(2)}) %collective-permute-start) | collective-permute-done | bytes 131104 | tf_op jit(solution)/shard_map/ppermute | solution.py:64
  35.3 1.2 %collective-permute-start.1 = (bf16[256,512]{1,0:T(8,128)(2,1)S(1)}, bf16[256,512]{1,0:T(8,128)(2,1)S(1)}, u32[]{:S(2)}, u32[]{:S(2)}) collective-permute-start(bf16[256,512]{1,0:T(8,128)(2,1)S(1)} %constant_dynamic-update-slice_fusion.refs_0_), channel_id=1, source_target_pairs={{0,24},{4,28},{8,16},{12,20},{16,8},{20,12},{24,0},{28,4},{1,25},{... | collective-permute-start | bytes 786440 | tf_op jit(solution)/shard_map/ppermute | solution.py:64
  36.5 0.0 collective-permute-start.10
  36.5 3.1 %collective-permute-done.11.refs_2_ = bf16[512,512]{1,0:T(8,128)(2,1)S(1)} collective-permute-done((bf16[512,512]{1,0:T(8,128)(2,1)S(1)}, bf16[512,512]{1,0:T(8,128)(2,1)S(1)}, u32[]{:S(2)}, u32[]{:S(2)}) %collective-permute-start.11) | collective-permute-done | bytes 524320 | tf_op jit(solution)/shard_map/ppermute | solution.py:64
  39.6 0.0 collective-permute-start.12
  39.6 4.6 %shard_map.150 = (f32[256,512]{1,0:T(8,128)}, f32[32,512]{1,0:T(8,128)}) custom-call(s32[2]{0:T(128)S(1)} %pad_add_fusion.place, bf16[256,512]{1,0:T(8,128)(2,1)} %get-tuple-element.20.qt_ref, bf16[256,512]{1,0:T(8,128)(2,1)S(1)} %constant_dynamic-update-slice_fusion.refs_0_), custom_call_target="tpu_custom_call" | custom-call | flops 8000000000 | tf_op jit(solution)/shard_map/pallas_call | solution.py:39
  44.2 15.6 %collective-permute-done.8.refs_6_ = bf16[256,2048]{1,0:T(8,128)(2,1)S(1)} collective-permute-done((bf16[256,2048]{1,0:T(8,128)(2,1)}, bf16[256,2048]{1,0:T(8,128)(2,1)S(1)}, u32[]{:S(2)}, u32[]{:S(2)}) %collective-permute-start.8) | collective-permute-done | bytes 1048608 | tf_op jit(solution)/shard_map/ppermute | solution.py:64
  59.8 1.4 %collective-permute-start.2 = (bf16[256,512]{1,0:T(8,128)(2,1)S(1)}, bf16[256,512]{1,0:T(8,128)(2,1)S(1)}, u32[]{:S(2)}, u32[]{:S(2)}) collective-permute-start(bf16[256,512]{1,0:T(8,128)(2,1)S(1)} %constant_dynamic-update-slice_fusion.refs_0_), channel_id=1, source_target_pairs={{0,16},{4,20},{8,24},{12,28},{16,0},{20,4},{24,8},{28,12},{1,17},{... | collective-permute-start | bytes 786440 | tf_op jit(solution)/shard_map/ppermute | solution.py:64
  61.2 0.0 collective-permute-done.10.refs_1_
  61.2 1.0 collective-permute-start.3
  62.2 0.0 collective-permute-done.12.refs_3_
  62.2 0.0 collective-permute-start.9
  62.2 8.7 %shard_map.154 = (bf16[256,512]{1,0:T(8,128)(2,1)S(1)}, bf16[256,512]{1,0:T(8,128)(2,1)S(1)}, bf16[256,512]{1,0:T(8,128)(2,1)S(1)}, bf16[256,512]{1,0:T(8,128)(2...) custom-call(s32[2]{0:T(128)S(1)} %pad_add_fusion.place, ...), custom_call_target="tpu_custom_call" | custom-call | flops 4499999744 | tf_op jit(solution)/shard_map/pallas_call | solution.py:39
  70.9 0.0 collective-permute-done.1.refs_2_
  70.9 0.6 collective-permute-start.21
  71.5 0.9 collective-permute-done.2.refs_3_
  72.4 0.0 collective-permute-start.14
  72.4 0.5 collective-permute-done.3.refs_4_
  72.9 7.7 %shard_map.151 = (bf16[128,256]{1,0:T(8,128)(2,1)S(1)}, bf16[128,256]{1,0:T(8,128)(2,1)S(1)}, bf16[128,256]{1,0:T(8,128)(2,1)S(1)}, bf16[128,256]{1,0:T(8,128)(2,1)S(1)}) custom-call(s32[2]{0:T(128)S(1)} %pad_add_fusion.place, bf16[256,512]{1,0:T(8,128)(2,1)} %get-tuple-element.20.qt_ref, f32[256,512]{1,0:T(8,128)} %get-tuple-element.22.refs_0_, ...), custom_call_target="tpu_custom_call" | custom-call | flops 8000000000 | tf_op jit(solution)/shard_map/pallas_call | solution.py:39
  80.6 0.1 collective-permute-start.4
  80.7 0.0 collective-permute-done.21
  80.7 0.5 collective-permute-start.20
  81.2 0.1 add_convert_fusion
  81.3 0.7 collective-permute-done.4.refs_1_
  81.9 0.2 collective-permute-start.13
  82.1 0.0 collective-permute-done.14
  82.1 1.5 %collective-permute-start.22 = (bf16[256,512]{1,0:T(8,128)(2,1)S(1)}, bf16[256,512]{1,0:T(8,128)(2,1)S(1)}, u32[]{:S(2)}, u32[]{:S(2)}) collective-permute-start(bf16[256,512]{1,0:T(8,128)(2,1)S(1)} %add_convert_fusion), channel_id=1, source_target_pairs={{0,2},{1,3},{2,0},{3,1},{4,6},{5,7},{6,4},{7,5},{8,10},{9,11},{10,... | collective-permute-start | bytes 786440 | tf_op jit(solution)/shard_map/ppermute | solution.py:64
  83.6 0.1 add_convert_fusion.1
  83.7 0.0 collective-permute-done.20
  83.7 0.6 collective-permute-start.15
  84.3 7.0 %collective-permute-done.22 = bf16[256,512]{1,0:T(8,128)(2,1)S(1)} collective-permute-done((bf16[256,512]{1,0:T(8,128)(2,1)S(1)}, bf16[256,512]{1,0:T(8,128)(2,1)S(1)}, u32[]{:S(2)}, u32[]{:S(2)}) %collective-permute-start.22) | collective-permute-done | bytes 262176 | tf_op jit(solution)/shard_map/ppermute | solution.py:64
  91.3 1.5 %collective-permute-start.5 = (bf16[128,256]{1,0:T(8,128)(2,1)S(1)}, bf16[128,256]{1,0:T(8,128)(2,1)S(1)}, u32[]{:S(2)}, u32[]{:S(2)}) collective-permute-start(bf16[128,256]{1,0:T(8,128)(2,1)S(1)} %get-tuple-element.26), channel_id=1, source_target_pairs={{0,2},{1,3},{2,0},{3,1},{4,6},{5,7},{6,4},{7,5},{8,10},{9,11},{10,... | collective-permute-start | bytes 196616 | tf_op jit(solution)/shard_map/ppermute | solution.py:64
  92.8 0.1 add_convert_fusion.2
  92.9 4.8 %collective-permute-done.5.refs_2_ = bf16[128,256]{1,0:T(8,128)(2,1)S(1)} collective-permute-done((bf16[128,256]{1,0:T(8,128)(2,1)S(1)}, bf16[128,256]{1,0:T(8,128)(2,1)S(1)}, u32[]{:S(2)}, u32[]{:S(2)}) %collective-permute-start.5) | collective-permute-done | bytes 65568 | tf_op jit(solution)/shard_map/ppermute | solution.py:64
  97.7 0.6 collective-permute-start.6
  98.3 0.0 collective-permute-done.13
  98.3 1.0 collective-permute-start.23
  99.3 0.0 collective-permute-done.15
  99.3 0.0 collective-permute-start.24
  99.3 0.1 add_convert_fusion.6
  99.5 2.6 %collective-permute-done.6.refs_3_ = bf16[128,256]{1,0:T(8,128)(2,1)S(1)} collective-permute-done((bf16[128,256]{1,0:T(8,128)(2,1)S(1)}, bf16[128,256]{1,0:T(8,128)(2,1)S(1)}, u32[]{:S(2)}, u32[]{:S(2)}) %collective-permute-start.6) | collective-permute-done | bytes 65568 | tf_op jit(solution)/shard_map/ppermute | solution.py:64
  102.0 0.2 collective-permute-start.25
  102.2 0.0 collective-permute-done.7.refs_5_
  102.2 2.8 %collective-permute-start.16 = (bf16[64,512]{1,0:T(8,128)(2,1)S(1)}, bf16[64,512]{1,0:T(8,128)(2,1)S(1)}, u32[]{:S(2)}, u32[]{:S(2)}) collective-permute-start(bf16[64,512]{1,0:T(8,128)(2,1)S(1)} %get-tuple-element.45), channel_id=1, source_target_pairs={{0,16},{4,20},{8,24},{12,28},{16,0},{20,4},{24,8},{28,12},{1,17},{... | collective-permute-start | bytes 196616 | tf_op jit(solution)/shard_map/ppermute | solution.py:64
  105.0 0.0 collective-permute-done.9.refs_7_
  105.0 1.3 %collective-permute-start.17 = (bf16[64,512]{1,0:T(8,128)(2,1)S(1)}, bf16[64,512]{1,0:T(8,128)(2,1)S(1)}, u32[]{:S(2)}, u32[]{:S(2)}) collective-permute-start(bf16[64,512]{1,0:T(8,128)(2,1)S(1)} %get-tuple-element.44), channel_id=1, source_target_pairs={{0,20},{4,16},{8,28},{12,24},{16,4},{20,0},{24,12},{28,8},{1,21},{... | collective-permute-start | bytes 196616 | tf_op jit(solution)/shard_map/ppermute | solution.py:64
  106.3 0.0 collective-permute-done.23.refs_5_
  106.3 1.1 collective-permute-start.18
  107.4 0.0 collective-permute-done.24.refs_6_
  107.4 2.5 %collective-permute-start.19 = (bf16[64,512]{1,0:T(8,128)(2,1)S(1)}, bf16[64,512]{1,0:T(8,128)(2,1)S(1)}, u32[]{:S(2)}, u32[]{:S(2)}) collective-permute-start(bf16[64,512]{1,0:T(8,128)(2,1)S(1)} %get-tuple-element.42), channel_id=1, source_target_pairs={{0,28},{4,24},{8,20},{12,16},{16,12},{20,8},{24,4},{28,0},{1,29},{... | collective-permute-start | bytes 196616 | tf_op jit(solution)/shard_map/ppermute | solution.py:64
  109.9 3.1 %shard_map.152 = bf16[128,2048]{1,0:T(8,128)(2,1)} custom-call(s32[2]{0:T(128)S(1)} %pad_add_fusion.place, bf16[128,256]{1,0:T(8,128)(2,1)S(1)} %get-tuple-element.24.refs_0_, bf16[128,256]{1,0:T(8,128)(2,1)S(1)} %collective-permute-done.4.refs_1_, bf16[128,256]{1,0:T(8,128)(2,1)S(1)} %collective-permute-done.5.refs_2_, ...), custom_call_target="tpu_custom_call" | custom-call | flops 1250000000 | tf_op jit(solution)/shard_map/pallas_call | solution.py:39
  112.9 0.0 collective-permute-done.25.refs_7_
  112.9 0.0 collective-permute-done.16.refs_0_
  112.9 3.0 %collective-permute-done.17.refs_1_ = bf16[64,512]{1,0:T(8,128)(2,1)S(1)} collective-permute-done((bf16[64,512]{1,0:T(8,128)(2,1)S(1)}, bf16[64,512]{1,0:T(8,128)(2,1)S(1)}, u32[]{:S(2)}, u32[]{:S(2)}) %collective-permute-start.17) | collective-permute-done | bytes 65568 | tf_op jit(solution)/shard_map/ppermute | solution.py:64
  115.9 1.6 %shard_map.155 = bf16[160,512]{1,0:T(8,128)(2,1)} custom-call(s32[2]{0:T(128)S(1)} %pad_add_fusion.place, s32[2,160]{1,0:T(2,128)S(1)} %get-tuple-element.28.slot_ref, f32[2,160]{1,0:T(2,128)S(1)} %bitcast.19, bf16[64,512]{1,0:T(8,128)(2,1)S(1)} %collective-permute-done.16.refs_0_, bf16[64,512]{1,0:T(8,128)(2,1)S(1)} %collective-permute-done.17.refs_1_, ...), custom_call_target="tpu_custom_call" | custom-call | flops 750000000 | tf_op jit(solution)/shard_map/pallas_call | solution.py:39
  (13 shorter events, 0.0 us)
Async XLA Ops:
  0.6 31.1 %copy-start = (bf16[256,2048]{1,0:T(8,128)(2,1)S(1)}, bf16[256,2048]{1,0:T(8,128)(2,1)}, u32[]{:S(2)}) copy-start(bf16[256,2048]{1,0:T(8,128)(2,1)} %refs_4_.1) | copy-start | bytes 3145732
  24.8 14.8 %collective-permute-start.11 = (bf16[512,512]{1,0:T(8,128)(2,1)S(1)}, bf16[512,512]{1,0:T(8,128)(2,1)S(1)}, u32[]{:S(2)}, u32[]{:S(2)}) collective-permute-start(bf16[512,512]{1,0:T(8,128)(2,1)S(1)} %bitcast.12), channel_id=1, source_target_pairs={{0,2},{1,3},{2,0},{3,1},{4,6},{5,7},{6,4},{7,5},{8,10},{9,11},{10,... | collective-permute-start | bytes 1572872 | tf_op jit(solution)/shard_map/ppermute | solution.py:64
  26.3 33.5 %collective-permute-start.8 = (bf16[256,2048]{1,0:T(8,128)(2,1)}, bf16[256,2048]{1,0:T(8,128)(2,1)S(1)}, u32[]{:S(2)}, u32[]{:S(2)}) collective-permute-start(bf16[256,2048]{1,0:T(8,128)(2,1)} %refs_4_.1), channel_id=1, source_target_pairs={{0,2},{1,3},{2,0},{3,1},{4,6},{5,7},{6,4},{7,5},{8,10},{9,11},{10,... | collective-permute-start | bytes 3145736 | tf_op jit(solution)/shard_map/ppermute | solution.py:64
  30.2 5.0 %collective-permute-start = (bf16[128,512]{1,0:T(8,128)(2,1)S(1)}, bf16[128,512]{1,0:T(8,128)(2,1)S(1)}, u32[]{:S(2)}, u32[]{:S(2)}) collective-permute-start(bf16[128,512]{1,0:T(8,128)(2,1)S(1)} %get-tuple-element.21), channel_id=1, source_target_pairs={{0,4},{4,0},{8,12},{12,8},{16,20},{20,16},{24,28},{28,24},{1,5},{5... | collective-permute-start | bytes 393224 | tf_op jit(solution)/shard_map/ppermute | solution.py:64
  31.7 70.5 %collective-permute-start.7 = (bf16[256,2048]{1,0:T(8,128)(2,1)S(1)}, bf16[256,2048]{1,0:T(8,128)(2,1)S(1)}, u32[]{:S(2)}, u32[]{:S(2)}) collective-permute-start(bf16[256,2048]{1,0:T(8,128)(2,1)S(1)} %copy-done), channel_id=1, source_target_pairs={{0,1},{1,0},{2,3},{3,2},{4,5},{5,4},{6,7},{7,6},{8,9},{9,8},{10,11... | collective-permute-start | bytes 3145736 | tf_op jit(solution)/shard_map/ppermute | solution.py:64
  35.3 35.6 %collective-permute-start.1 = (bf16[256,512]{1,0:T(8,128)(2,1)S(1)}, bf16[256,512]{1,0:T(8,128)(2,1)S(1)}, u32[]{:S(2)}, u32[]{:S(2)}) collective-permute-start(bf16[256,512]{1,0:T(8,128)(2,1)S(1)} %constant_dynamic-update-slice_fusion.refs_0_), channel_id=1, source_target_pairs={{0,24},{4,28},{8,16},{12,20},{16,8},{20,12},{24,0},{28,4},{1,25},{... | collective-permute-start | bytes 786440 | tf_op jit(solution)/shard_map/ppermute | solution.py:64
  36.5 24.7 %collective-permute-start.10 = (bf16[512,512]{1,0:T(8,128)(2,1)S(1)}, bf16[512,512]{1,0:T(8,128)(2,1)S(1)}, u32[]{:S(2)}, u32[]{:S(2)}) collective-permute-start(bf16[512,512]{1,0:T(8,128)(2,1)S(1)} %bitcast.13), channel_id=1, source_target_pairs={{0,1},{1,0},{2,3},{3,2},{4,5},{5,4},{6,7},{7,6},{8,9},{9,8},{10,11... | collective-permute-start | bytes 1572872 | tf_op jit(solution)/shard_map/ppermute | solution.py:64
  39.6 22.6 %collective-permute-start.12 = (bf16[512,512]{1,0:T(8,128)(2,1)S(1)}, bf16[512,512]{1,0:T(8,128)(2,1)S(1)}, u32[]{:S(2)}, u32[]{:S(2)}) collective-permute-start(bf16[512,512]{1,0:T(8,128)(2,1)S(1)} %collective-permute-done.11.refs_2_), channel_id=1, source_target_pairs={{0,1},{1,0},{2,3},{3,2},{4,5},{5,4},{6,7},{7,6},{8,9},{9,8},{10,11... | collective-permute-start | bytes 1572872 | tf_op jit(solution)/shard_map/ppermute | solution.py:64
  39.6 22.6 %copy-start.1 = (bf16[1,2048,1024]{2,1,0:T(8,128)(2,1)S(1)}, bf16[1,2048,1024]{2,1,0:T(8,128)(2,1)}, u32[]{:S(2)}) copy-start(bf16[1,2048,1024]{2,1,0:T(8,128)(2,1)} %param.24) | copy-start | bytes 12582916
  39.6 22.6 %copy-start.2 = (bf16[1,2048,1024]{2,1,0:T(8,128)(2,1)S(1)}, bf16[1,2048,1024]{2,1,0:T(8,128)(2,1)}, u32[]{:S(2)}) copy-start(bf16[1,2048,1024]{2,1,0:T(8,128)(2,1)} %param.25) | copy-start | bytes 12582916
  39.6 22.6 %copy-start.3 = (bf16[1,1024,2048]{2,1,0:T(8,128)(2,1)S(1)}, bf16[1,1024,2048]{2,1,0:T(8,128)(2,1)}, u32[]{:S(2)}) copy-start(bf16[1,1024,2048]{2,1,0:T(8,128)(2,1)} %param.26) | copy-start | bytes 12582916
  59.8 12.6 %collective-permute-start.2 = (bf16[256,512]{1,0:T(8,128)(2,1)S(1)}, bf16[256,512]{1,0:T(8,128)(2,1)S(1)}, u32[]{:S(2)}, u32[]{:S(2)}) collective-permute-start(bf16[256,512]{1,0:T(8,128)(2,1)S(1)} %constant_dynamic-update-slice_fusion.refs_0_), channel_id=1, source_target_pairs={{0,16},{4,20},{8,24},{12,28},{16,0},{20,4},{24,8},{28,12},{1,17},{... | collective-permute-start | bytes 786440 | tf_op jit(solution)/shard_map/ppermute | solution.py:64
  61.2 11.7 %collective-permute-start.3 = (bf16[256,512]{1,0:T(8,128)(2,1)S(1)}, bf16[256,512]{1,0:T(8,128)(2,1)S(1)}, u32[]{:S(2)}, u32[]{:S(2)}) collective-permute-start(bf16[256,512]{1,0:T(8,128)(2,1)S(1)} %constant_dynamic-update-slice_fusion.refs_0_), channel_id=1, source_target_pairs={{0,8},{4,12},{8,0},{12,4},{16,24},{20,28},{24,16},{28,20},{1,9},{5... | collective-permute-start | bytes 786440 | tf_op jit(solution)/shard_map/ppermute | solution.py:64
  62.2 42.8 %collective-permute-start.9 = (bf16[256,2048]{1,0:T(8,128)(2,1)S(1)}, bf16[256,2048]{1,0:T(8,128)(2,1)S(1)}, u32[]{:S(2)}, u32[]{:S(2)}) collective-permute-start(bf16[256,2048]{1,0:T(8,128)(2,1)S(1)} %collective-permute-done.8.refs_6_), channel_id=1, source_target_pairs={{0,1},{1,0},{2,3},{3,2},{4,5},{5,4},{6,7},{7,6},{8,9},{9,8},{10,11... | collective-permute-start | bytes 3145736 | tf_op jit(solution)/shard_map/ppermute | solution.py:64
  70.9 9.8 %collective-permute-start.21 = (bf16[256,512]{1,0:T(8,128)(2,1)S(1)}, bf16[256,512]{1,0:T(8,128)(2,1)S(1)}, u32[]{:S(2)}, u32[]{:S(2)}) collective-permute-start(bf16[256,512]{1,0:T(8,128)(2,1)S(1)} %get-tuple-element.37), channel_id=1, source_target_pairs={{0,1},{1,0},{2,3},{3,2},{4,5},{5,4},{6,7},{7,6},{8,9},{9,8},{10,11... | collective-permute-start | bytes 786440 | tf_op jit(solution)/shard_map/ppermute | solution.py:64
  72.4 9.7 %collective-permute-start.14 = (bf16[256,512]{1,0:T(8,128)(2,1)S(1)}, bf16[256,512]{1,0:T(8,128)(2,1)S(1)}, u32[]{:S(2)}, u32[]{:S(2)}) collective-permute-start(bf16[256,512]{1,0:T(8,128)(2,1)S(1)} %get-tuple-element.33), channel_id=1, source_target_pairs={{0,1},{1,0},{2,3},{3,2},{4,5},{5,4},{6,7},{7,6},{8,9},{9,8},{10,11... | collective-permute-start | bytes 786440 | tf_op jit(solution)/shard_map/ppermute | solution.py:64
  80.6 1.3 %collective-permute-start.4 = (bf16[128,256]{1,0:T(8,128)(2,1)S(1)}, bf16[128,256]{1,0:T(8,128)(2,1)S(1)}, u32[]{:S(2)}, u32[]{:S(2)}) collective-permute-start(bf16[128,256]{1,0:T(8,128)(2,1)S(1)} %get-tuple-element.25), channel_id=1, source_target_pairs={{0,1},{1,0},{2,3},{3,2},{4,5},{5,4},{6,7},{7,6},{8,9},{9,8},{10,11... | collective-permute-start | bytes 196616 | tf_op jit(solution)/shard_map/ppermute | solution.py:64
  80.7 3.0 %collective-permute-start.20 = (bf16[256,512]{1,0:T(8,128)(2,1)S(1)}, bf16[256,512]{1,0:T(8,128)(2,1)S(1)}, u32[]{:S(2)}, u32[]{:S(2)}) collective-permute-start(bf16[256,512]{1,0:T(8,128)(2,1)S(1)} %get-tuple-element.35), channel_id=1, source_target_pairs={{0,1},{1,0},{2,3},{3,2},{4,5},{5,4},{6,7},{7,6},{8,9},{9,8},{10,11... | collective-permute-start | bytes 786440 | tf_op jit(solution)/shard_map/ppermute | solution.py:64
  81.2 34.7 %copy-start.4 = (f32[160,2]{0,1:T(2,128)S(1)}, f32[160,2]{0,1:T(2,128)}, u32[]{:S(2)}) copy-start(f32[160,2]{0,1:T(2,128)} %param.23) | copy-start | bytes 3844
  81.9 16.4 %collective-permute-start.13 = (bf16[256,512]{1,0:T(8,128)(2,1)S(1)}, bf16[256,512]{1,0:T(8,128)(2,1)S(1)}, u32[]{:S(2)}, u32[]{:S(2)}) collective-permute-start(bf16[256,512]{1,0:T(8,128)(2,1)S(1)} %get-tuple-element.31), channel_id=1, source_target_pairs={{0,1},{1,0},{2,3},{3,2},{4,5},{5,4},{6,7},{7,6},{8,9},{9,8},{10,11... | collective-permute-start | bytes 786440 | tf_op jit(solution)/shard_map/ppermute | solution.py:64
  82.1 9.2 %collective-permute-start.22 = (bf16[256,512]{1,0:T(8,128)(2,1)S(1)}, bf16[256,512]{1,0:T(8,128)(2,1)S(1)}, u32[]{:S(2)}, u32[]{:S(2)}) collective-permute-start(bf16[256,512]{1,0:T(8,128)(2,1)S(1)} %add_convert_fusion), channel_id=1, source_target_pairs={{0,2},{1,3},{2,0},{3,1},{4,6},{5,7},{6,4},{7,5},{8,10},{9,11},{10,... | collective-permute-start | bytes 786440 | tf_op jit(solution)/shard_map/ppermute | solution.py:64
  83.7 15.6 %collective-permute-start.15 = (bf16[256,512]{1,0:T(8,128)(2,1)S(1)}, bf16[256,512]{1,0:T(8,128)(2,1)S(1)}, u32[]{:S(2)}, u32[]{:S(2)}) collective-permute-start(bf16[256,512]{1,0:T(8,128)(2,1)S(1)} %add_convert_fusion.1), channel_id=1, source_target_pairs={{0,2},{1,3},{2,0},{3,1},{4,6},{5,7},{6,4},{7,5},{8,10},{9,11},{10,... | collective-permute-start | bytes 786440 | tf_op jit(solution)/shard_map/ppermute | solution.py:64
  91.3 6.4 %collective-permute-start.5 = (bf16[128,256]{1,0:T(8,128)(2,1)S(1)}, bf16[128,256]{1,0:T(8,128)(2,1)S(1)}, u32[]{:S(2)}, u32[]{:S(2)}) collective-permute-start(bf16[128,256]{1,0:T(8,128)(2,1)S(1)} %get-tuple-element.26), channel_id=1, source_target_pairs={{0,2},{1,3},{2,0},{3,1},{4,6},{5,7},{6,4},{7,5},{8,10},{9,11},{10,... | collective-permute-start | bytes 196616 | tf_op jit(solution)/shard_map/ppermute | solution.py:64
  97.7 4.3 %collective-permute-start.6 = (bf16[128,256]{1,0:T(8,128)(2,1)S(1)}, bf16[128,256]{1,0:T(8,128)(2,1)S(1)}, u32[]{:S(2)}, u32[]{:S(2)}) collective-permute-start(bf16[128,256]{1,0:T(8,128)(2,1)S(1)} %get-tuple-element.27), channel_id=1, source_target_pairs={{0,3},{1,2},{2,1},{3,0},{4,7},{5,6},{6,5},{7,4},{8,11},{9,10},{10,... | collective-permute-start | bytes 196616 | tf_op jit(solution)/shard_map/ppermute | solution.py:64
  98.3 8.0 %collective-permute-start.23 = (bf16[64,512]{1,0:T(8,128)(2,1)S(1)}, bf16[64,512]{1,0:T(8,128)(2,1)S(1)}, u32[]{:S(2)}, u32[]{:S(2)}) collective-permute-start(bf16[64,512]{1,0:T(8,128)(2,1)S(1)} %get-tuple-element.40), channel_id=1, source_target_pairs={{0,4},{4,0},{8,12},{12,8},{16,20},{20,16},{24,28},{28,24},{1,5},{5... | collective-permute-start | bytes 196616 | tf_op jit(solution)/shard_map/ppermute | solution.py:64
  99.3 8.1 %collective-permute-start.24 = (bf16[64,512]{1,0:T(8,128)(2,1)S(1)}, bf16[64,512]{1,0:T(8,128)(2,1)S(1)}, u32[]{:S(2)}, u32[]{:S(2)}) collective-permute-start(bf16[64,512]{1,0:T(8,128)(2,1)S(1)} %get-tuple-element.39), channel_id=1, source_target_pairs={{0,8},{4,12},{8,0},{12,4},{16,24},{20,28},{24,16},{28,20},{1,9},{5... | collective-permute-start | bytes 196616 | tf_op jit(solution)/shard_map/ppermute | solution.py:64
  102.0 10.9 %collective-permute-start.25 = (bf16[64,512]{1,0:T(8,128)(2,1)S(1)}, bf16[64,512]{1,0:T(8,128)(2,1)S(1)}, u32[]{:S(2)}, u32[]{:S(2)}) collective-permute-start(bf16[64,512]{1,0:T(8,128)(2,1)S(1)} %get-tuple-element.38), channel_id=1, source_target_pairs={{0,12},{4,8},{8,4},{12,0},{16,28},{20,24},{24,20},{28,16},{1,13},{... | collective-permute-start | bytes 196616 | tf_op jit(solution)/shard_map/ppermute | solution.py:64
  102.2 10.7 %collective-permute-start.16 = (bf16[64,512]{1,0:T(8,128)(2,1)S(1)}, bf16[64,512]{1,0:T(8,128)(2,1)S(1)}, u32[]{:S(2)}, u32[]{:S(2)}) collective-permute-start(bf16[64,512]{1,0:T(8,128)(2,1)S(1)} %get-tuple-element.45), channel_id=1, source_target_pairs={{0,16},{4,20},{8,24},{12,28},{16,0},{20,4},{24,8},{28,12},{1,17},{... | collective-permute-start | bytes 196616 | tf_op jit(solution)/shard_map/ppermute | solution.py:64
  105.0 10.9 %collective-permute-start.17 = (bf16[64,512]{1,0:T(8,128)(2,1)S(1)}, bf16[64,512]{1,0:T(8,128)(2,1)S(1)}, u32[]{:S(2)}, u32[]{:S(2)}) collective-permute-start(bf16[64,512]{1,0:T(8,128)(2,1)S(1)} %get-tuple-element.44), channel_id=1, source_target_pairs={{0,20},{4,16},{8,28},{12,24},{16,4},{20,0},{24,12},{28,8},{1,21},{... | collective-permute-start | bytes 196616 | tf_op jit(solution)/shard_map/ppermute | solution.py:64
  106.3 9.6 %collective-permute-start.18 = (bf16[64,512]{1,0:T(8,128)(2,1)S(1)}, bf16[64,512]{1,0:T(8,128)(2,1)S(1)}, u32[]{:S(2)}, u32[]{:S(2)}) collective-permute-start(bf16[64,512]{1,0:T(8,128)(2,1)S(1)} %get-tuple-element.43), channel_id=1, source_target_pairs={{0,24},{4,28},{8,16},{12,20},{16,8},{20,12},{24,0},{28,4},{1,25},{... | collective-permute-start | bytes 196616 | tf_op jit(solution)/shard_map/ppermute | solution.py:64
  107.4 8.5 %collective-permute-start.19 = (bf16[64,512]{1,0:T(8,128)(2,1)S(1)}, bf16[64,512]{1,0:T(8,128)(2,1)S(1)}, u32[]{:S(2)}, u32[]{:S(2)}) collective-permute-start(bf16[64,512]{1,0:T(8,128)(2,1)S(1)} %get-tuple-element.42), channel_id=1, source_target_pairs={{0,28},{4,24},{8,20},{12,16},{16,12},{20,8},{24,4},{28,0},{1,29},{... | collective-permute-start | bytes 196616 | tf_op jit(solution)/shard_map/ppermute | solution.py:64

commit v6 on v5

--- a/solution.py
+++ b/solution.py
@@ -64,12 +64,14 @@
     return lax.ppermute(x, axis, [(i, i ^ flip) for i in range(n)])
 
 
-def dispatch_body(place, routes_ref, x_hbm, *outs, experts, cap):
-    out_ref, slot_ref, x_ref, sem = outs
+def dispatch_body(place, routes_hbm, x_hbm, out_ref, slot_ref, x_ref, routes_ref, sem, routes_sem, *, experts, cap):
     tokens, feat = x_ref.shape
     cols = pl.ds(pl.multiple_of(place[0] * feat, feat), feat)
     fetch = pltpu.make_async_copy(x_hbm.at[:, cols], x_ref, sem)
+    fetch_routes = pltpu.make_async_copy(routes_hbm, routes_ref, routes_sem)
+    fetch_routes.start()
     fetch.start()
+    fetch_routes.wait()
     routes = routes_ref[...]
     rows = lax.broadcasted_iota(jnp.int32, (experts, tokens), 0)
     first = (rows == routes[0:1, :]).astype(F32)
@@ -101,9 +103,14 @@
         functools.partial(dispatch_body, experts=experts, cap=cap),
         place,
         (routes, expert_input),
-        [full(routes.shape), hbm()],
+        [hbm(), hbm()],
         outs,
-        scratch=[pltpu.VMEM((tokens, feat), BF16), pltpu.SemaphoreType.DMA],
+        scratch=[
+            pltpu.VMEM((tokens, feat), BF16),
+            pltpu.VMEM(routes.shape, jnp.int32),
+            pltpu.SemaphoreType.DMA,
+            pltpu.SemaphoreType.DMA,
+        ],
         micros=1.5,
     )
 
@@ -275,25 +282,24 @@
 
 def mix_body(place, *refs, groups):
     att_refs, w_refs, out_ref = refs[:groups], refs[groups : 2 * groups], refs[2 * groups]
-    total = jnp.zeros(out_ref.shape, F32)
-    for k in range(groups):
-        total += mm(att_refs[k][...], w_refs[k][...]).astype(BF16).astype(F32)
-    out_ref[...] = total.astype(BF16)
+    width = out_ref.shape[1]
+    tile = min(width, 1024)
+    for j in range(0, width, tile):
+        total = 0.0
+        for k in range(groups):
+            total += mm(att_refs[k][...], w_refs[k][:, j : j + tile]).astype(BF16).astype(F32)
+        out_ref[:, j : j + tile] = total.astype(BF16)
 
 
 def mix(place, atts, weights):
     groups = len(weights)
     rows = atts[0].shape[0]
-    depth, width = weights[0].shape
-    tile = min(width, 512)
     return call(
         functools.partial(mix_body, groups=groups),
         place,
         (*atts, *weights),
-        [full(a.shape) for a in atts] + [pl.BlockSpec((depth, tile), lambda j, place: (0, j))] * groups,
-        [jax.ShapeDtypeStruct((rows, width), BF16)],
-        grid=(width // tile,),
-        out_specs=[pl.BlockSpec((rows, tile), lambda j, place: (0, j))],
+        [full(a.shape) for a in atts] + [full(w.shape) for w in weights],
+        [jax.ShapeDtypeStruct((rows, weights[0].shape[1]), BF16)],
         micros=2.5,
     )[0]
 

time: 118 us -> 117 us (level)
  Pallas kernels: 31.5 us -> 29.9 us
    pallas_call x7, Pallas kernels: 31.5 us -> 29.9 us  [call(): pl.pallas_call(body, grid_spec=pltpu.PrefetchScalarGridSpec(num_scalar_pr...]
where the time goes in v6:
time: 117 us
  waiting for transfers between devices  42.4 us (36%)
  Pallas kernels  29.9 us (26%)
  blocking collectives  21.6 us (18%)
  starting transfers between devices  21.5 us (18%)
    ppermute x26, waiting for transfers between devices, send(): return lax.ppermute(x, axis, [(i, i ^ flip) for i in range(n)])  42.4 us
    pallas_call x7, Pallas kernels, call(): pl.pallas_call(body, grid_spec=pltpu.PrefetchScalarGridSpec(num_scalar_pr...  29.9 us
    all_to_all x1, blocking collectives, local(): lax.all_to_all(outbound, 'ep', split_axis=0, concat_axis=0, tiled=True)  21.6 us
    ppermute x26, starting transfers between devices, send(): return lax.ppermute(x, axis, [(i, i ^ flip) for i in range(n)])  21.5 us
  transfers between devices with their start and end apart: 26, of which 10 were waited for; matrix products, arithmetic and copies ran while one was open for 0% of the time, Pallas kernels for 23%

profile of v6, /device:TPU:0, one launch (start us, length us, event | category | flops | bytes accessed | tf_op | source)
XLA Modules:
  0.0 116.8 jit_solution(8419025147345132853)
XLA Ops:
  0.6 0.0 copy-start
  0.6 0.1 pad_add_fusion.place
  0.7 1.8 %shard_map.153 = (bf16[512,512]{1,0:T(8,128)(2,1)S(1)}, s32[2,160]{1,0:T(2,128)S(1)}) custom-call(s32[2]{0:T(128)S(1)} %pad_add_fusion.place, s32[2,160]{1,0:T(2,128)} %bitcast.21, bf16[160,2048]{1,0:T(8,128)(2,1)} %x_hbm.1), custom_call_target="tpu_custom_call" | custom-call | flops 750000000 | tf_op jit(solution)/shard_map/pallas_call | solution.py:39
  2.5 21.6 %all_to_all.11 = bf16[8,64,512]{2,1,0:T(8,128)(2,1)S(1)} all-to-all(bf16[8,64,512]{2,1,0:T(8,128)(2,1)S(1)} %bitcast.15), channel_id=1, replica_groups=mesh['ep'=8,'tp'=4] {'ep'}, dimensions={0} | all-to-all | bytes 1048576 | tf_op jit(solution)/shard_map/all_to_all | solution.py:432
  24.1 1.5 %collective-permute-start.11 = (bf16[512,512]{1,0:T(8,128)(2,1)S(1)}, bf16[512,512]{1,0:T(8,128)(2,1)S(1)}, u32[]{:S(2)}, u32[]{:S(2)}) collective-permute-start(bf16[512,512]{1,0:T(8,128)(2,1)S(1)} %bitcast.12), channel_id=1, source_target_pairs={{0,2},{1,3},{2,0},{3,1},{4,6},{5,7},{6,4},{7,5},{8,10},{9,11},{10,... | collective-permute-start | bytes 1572872 | tf_op jit(solution)/shard_map/ppermute | solution.py:64
  25.6 0.5 collective-permute-start.8
  26.1 3.4 %shard_map.149 = (bf16[256,512]{1,0:T(8,128)(2,1)}, bf16[128,512]{1,0:T(8,128)(2,1)S(1)}) custom-call(s32[2]{0:T(128)S(1)} %pad_add_fusion.place, bf16[512,256]{1,0:T(8,128)(2,1)} %q_hbm.1, bf16[512,256]{1,0:T(8,128)(2,1)} %k_hbm.1, bf16[512,256]{1,0:T(8,128)(2,1)} %v_hbm.1, f32[1,64]{1,0:T(1,128)} %bitcast.22, f32[1,64]{1,0:T(1,128)} %bitcast.23, ...), custom_call_target="tpu_custom_call" | custom-call | flops 1000000000 | tf_op jit(solution)/shard_map/pallas_call | solution.py:39
  29.6 1.5 %collective-permute-start = (bf16[128,512]{1,0:T(8,128)(2,1)S(1)}, bf16[128,512]{1,0:T(8,128)(2,1)S(1)}, u32[]{:S(2)}, u32[]{:S(2)}) collective-permute-start(bf16[128,512]{1,0:T(8,128)(2,1)S(1)} %get-tuple-element.21), channel_id=1, source_target_pairs={{0,4},{4,0},{8,12},{12,8},{16,20},{20,16},{24,28},{28,24},{1,5},{5... | collective-permute-start | bytes 393224 | tf_op jit(solution)/shard_map/ppermute | solution.py:64
  31.1 0.0 collective-permute-start.7
  31.1 3.5 %collective-permute-done = bf16[128,512]{1,0:T(8,128)(2,1)S(1)} collective-permute-done((bf16[128,512]{1,0:T(8,128)(2,1)S(1)}, bf16[128,512]{1,0:T(8,128)(2,1)S(1)}, u32[]{:S(2)}, u32[]{:S(2)}) %collective-permute-start) | collective-permute-done | bytes 131104 | tf_op jit(solution)/shard_map/ppermute | solution.py:64
  34.6 1.2 %collective-permute-start.1 = (bf16[256,512]{1,0:T(8,128)(2,1)S(1)}, bf16[256,512]{1,0:T(8,128)(2,1)S(1)}, u32[]{:S(2)}, u32[]{:S(2)}) collective-permute-start(bf16[256,512]{1,0:T(8,128)(2,1)S(1)} %constant_dynamic-update-slice_fusion.refs_0_), channel_id=1, source_target_pairs={{0,24},{4,28},{8,16},{12,20},{16,8},{20,12},{24,0},{28,4},{1,25},{... | collective-permute-start | bytes 786440 | tf_op jit(solution)/shard_map/ppermute | solution.py:64
  35.8 0.0 collective-permute-start.10
  35.8 3.1 %collective-permute-done.11.refs_2_ = bf16[512,512]{1,0:T(8,128)(2,1)S(1)} collective-permute-done((bf16[512,512]{1,0:T(8,128)(2,1)S(1)}, bf16[512,512]{1,0:T(8,128)(2,1)S(1)}, u32[]{:S(2)}, u32[]{:S(2)}) %collective-permute-start.11) | collective-permute-done | bytes 524320 | tf_op jit(solution)/shard_map/ppermute | solution.py:64
  38.9 0.0 collective-permute-start.12
  38.9 4.6 %shard_map.150 = (f32[256,512]{1,0:T(8,128)}, f32[32,512]{1,0:T(8,128)}) custom-call(s32[2]{0:T(128)S(1)} %pad_add_fusion.place, bf16[256,512]{1,0:T(8,128)(2,1)} %get-tuple-element.20.qt_ref, bf16[256,512]{1,0:T(8,128)(2,1)S(1)} %constant_dynamic-update-slice_fusion.refs_0_), custom_call_target="tpu_custom_call" | custom-call | flops 8000000000 | tf_op jit(solution)/shard_map/pallas_call | solution.py:39
  43.5 15.6 %collective-permute-done.8.refs_6_ = bf16[256,2048]{1,0:T(8,128)(2,1)S(1)} collective-permute-done((bf16[256,2048]{1,0:T(8,128)(2,1)}, bf16[256,2048]{1,0:T(8,128)(2,1)S(1)}, u32[]{:S(2)}, u32[]{:S(2)}) %collective-permute-start.8) | collective-permute-done | bytes 1048608 | tf_op jit(solution)/shard_map/ppermute | solution.py:64
  59.1 1.4 %collective-permute-start.2 = (bf16[256,512]{1,0:T(8,128)(2,1)S(1)}, bf16[256,512]{1,0:T(8,128)(2,1)S(1)}, u32[]{:S(2)}, u32[]{:S(2)}) collective-permute-start(bf16[256,512]{1,0:T(8,128)(2,1)S(1)} %constant_dynamic-update-slice_fusion.refs_0_), channel_id=1, source_target_pairs={{0,16},{4,20},{8,24},{12,28},{16,0},{20,4},{24,8},{28,12},{1,17},{... | collective-permute-start | bytes 786440 | tf_op jit(solution)/shard_map/ppermute | solution.py:64
  60.6 0.0 collective-permute-done.10.refs_1_
  60.6 1.0 collective-permute-start.3
  61.5 0.0 collective-permute-done.12.refs_3_
  61.5 0.0 collective-permute-start.9
  61.6 8.7 %shard_map.154 = (bf16[256,512]{1,0:T(8,128)(2,1)S(1)}, bf16[256,512]{1,0:T(8,128)(2,1)S(1)}, bf16[256,512]{1,0:T(8,128)(2,1)S(1)}, bf16[256,512]{1,0:T(8,128)(2...) custom-call(s32[2]{0:T(128)S(1)} %pad_add_fusion.place, ...), custom_call_target="tpu_custom_call" | custom-call | flops 4499999744 | tf_op jit(solution)/shard_map/pallas_call | solution.py:39
  70.3 0.0 collective-permute-done.1.refs_2_
  70.3 0.6 collective-permute-start.21
  70.8 0.9 collective-permute-done.2.refs_3_
  71.7 0.0 collective-permute-start.14
  71.7 0.5 collective-permute-done.3.refs_4_
  72.3 7.7 %shard_map.151 = (bf16[128,256]{1,0:T(8,128)(2,1)S(1)}, bf16[128,256]{1,0:T(8,128)(2,1)S(1)}, bf16[128,256]{1,0:T(8,128)(2,1)S(1)}, bf16[128,256]{1,0:T(8,128)(2,1)S(1)}) custom-call(s32[2]{0:T(128)S(1)} %pad_add_fusion.place, bf16[256,512]{1,0:T(8,128)(2,1)} %get-tuple-element.20.qt_ref, f32[256,512]{1,0:T(8,128)} %get-tuple-element.22.refs_0_, ...), custom_call_target="tpu_custom_call" | custom-call | flops 8000000000 | tf_op jit(solution)/shard_map/pallas_call | solution.py:39
  80.0 0.1 collective-permute-start.4
  80.0 0.0 collective-permute-done.21
  80.1 0.5 collective-permute-start.20
  80.5 0.1 add_convert_fusion
  80.6 0.7 collective-permute-done.4.refs_1_
  81.3 0.2 collective-permute-start.13
  81.4 0.0 collective-permute-done.14
  81.4 1.5 %collective-permute-start.22 = (bf16[256,512]{1,0:T(8,128)(2,1)S(1)}, bf16[256,512]{1,0:T(8,128)(2,1)S(1)}, u32[]{:S(2)}, u32[]{:S(2)}) collective-permute-start(bf16[256,512]{1,0:T(8,128)(2,1)S(1)} %add_convert_fusion), channel_id=1, source_target_pairs={{0,2},{1,3},{2,0},{3,1},{4,6},{5,7},{6,4},{7,5},{8,10},{9,11},{10,... | collective-permute-start | bytes 786440 | tf_op jit(solution)/shard_map/ppermute | solution.py:64
  83.0 0.1 add_convert_fusion.1
  83.0 0.0 collective-permute-done.20
  83.0 0.6 collective-permute-start.15
  83.6 7.0 %collective-permute-done.22 = bf16[256,512]{1,0:T(8,128)(2,1)S(1)} collective-permute-done((bf16[256,512]{1,0:T(8,128)(2,1)S(1)}, bf16[256,512]{1,0:T(8,128)(2,1)S(1)}, u32[]{:S(2)}, u32[]{:S(2)}) %collective-permute-start.22) | collective-permute-done | bytes 262176 | tf_op jit(solution)/shard_map/ppermute | solution.py:64
  90.6 1.5 %collective-permute-start.5 = (bf16[128,256]{1,0:T(8,128)(2,1)S(1)}, bf16[128,256]{1,0:T(8,128)(2,1)S(1)}, u32[]{:S(2)}, u32[]{:S(2)}) collective-permute-start(bf16[128,256]{1,0:T(8,128)(2,1)S(1)} %get-tuple-element.26), channel_id=1, source_target_pairs={{0,2},{1,3},{2,0},{3,1},{4,6},{5,7},{6,4},{7,5},{8,10},{9,11},{10,... | collective-permute-start | bytes 196616 | tf_op jit(solution)/shard_map/ppermute | solution.py:64
  92.1 0.1 add_convert_fusion.2
  92.3 4.8 %collective-permute-done.5.refs_2_ = bf16[128,256]{1,0:T(8,128)(2,1)S(1)} collective-permute-done((bf16[128,256]{1,0:T(8,128)(2,1)S(1)}, bf16[128,256]{1,0:T(8,128)(2,1)S(1)}, u32[]{:S(2)}, u32[]{:S(2)}) %collective-permute-start.5) | collective-permute-done | bytes 65568 | tf_op jit(solution)/shard_map/ppermute | solution.py:64
  97.0 0.6 collective-permute-start.6
  97.6 0.0 collective-permute-done.13
  97.7 1.0 collective-permute-start.23
  98.7 0.0 collective-permute-done.15
  98.7 0.1 add_convert_fusion.6
  98.8 2.5 %collective-permute-done.6.refs_3_ = bf16[128,256]{1,0:T(8,128)(2,1)S(1)} collective-permute-done((bf16[128,256]{1,0:T(8,128)(2,1)S(1)}, bf16[128,256]{1,0:T(8,128)(2,1)S(1)}, u32[]{:S(2)}, u32[]{:S(2)}) %collective-permute-start.6) | collective-permute-done | bytes 65568 | tf_op jit(solution)/shard_map/ppermute | solution.py:64
  101.3 0.2 collective-permute-start.25
  101.6 0.0 collective-permute-done.7.refs_5_
  101.6 2.8 %collective-permute-start.16 = (bf16[64,512]{1,0:T(8,128)(2,1)S(1)}, bf16[64,512]{1,0:T(8,128)(2,1)S(1)}, u32[]{:S(2)}, u32[]{:S(2)}) collective-permute-start(bf16[64,512]{1,0:T(8,128)(2,1)S(1)} %get-tuple-element.45), channel_id=1, source_target_pairs={{0,16},{4,20},{8,24},{12,28},{16,0},{20,4},{24,8},{28,12},{1,17},{... | collective-permute-start | bytes 196616 | tf_op jit(solution)/shard_map/ppermute | solution.py:64
  104.4 0.0 collective-permute-done.9.refs_7_
  104.4 1.2 %collective-permute-start.17 = (bf16[64,512]{1,0:T(8,128)(2,1)S(1)}, bf16[64,512]{1,0:T(8,128)(2,1)S(1)}, u32[]{:S(2)}, u32[]{:S(2)}) collective-permute-start(bf16[64,512]{1,0:T(8,128)(2,1)S(1)} %get-tuple-element.44), channel_id=1, source_target_pairs={{0,20},{4,16},{8,28},{12,24},{16,4},{20,0},{24,12},{28,8},{1,21},{... | collective-permute-start | bytes 196616 | tf_op jit(solution)/shard_map/ppermute | solution.py:64
  105.6 0.0 collective-permute-done.23.refs_5_
  105.6 1.2 %collective-permute-start.18 = (bf16[64,512]{1,0:T(8,128)(2,1)S(1)}, bf16[64,512]{1,0:T(8,128)(2,1)S(1)}, u32[]{:S(2)}, u32[]{:S(2)}) collective-permute-start(bf16[64,512]{1,0:T(8,128)(2,1)S(1)} %get-tuple-element.43), channel_id=1, source_target_pairs={{0,24},{4,28},{8,16},{12,20},{16,8},{20,12},{24,0},{28,4},{1,25},{... | collective-permute-start | bytes 196616 | tf_op jit(solution)/shard_map/ppermute | solution.py:64
  106.8 0.0 collective-permute-done.24.refs_6_
  106.8 2.5 %collective-permute-start.19 = (bf16[64,512]{1,0:T(8,128)(2,1)S(1)}, bf16[64,512]{1,0:T(8,128)(2,1)S(1)}, u32[]{:S(2)}, u32[]{:S(2)}) collective-permute-start(bf16[64,512]{1,0:T(8,128)(2,1)S(1)} %get-tuple-element.42), channel_id=1, source_target_pairs={{0,28},{4,24},{8,20},{12,16},{16,12},{20,8},{24,4},{28,0},{1,29},{... | collective-permute-start | bytes 196616 | tf_op jit(solution)/shard_map/ppermute | solution.py:64
  109.2 2.2 %shard_map.152 = bf16[128,2048]{1,0:T(8,128)(2,1)} custom-call(s32[2]{0:T(128)S(1)} %pad_add_fusion.place, bf16[128,256]{1,0:T(8,128)(2,1)S(1)} %get-tuple-element.24.refs_0_, bf16[128,256]{1,0:T(8,128)(2,1)S(1)} %collective-permute-done.4.refs_1_, bf16[128,256]{1,0:T(8,128)(2,1)S(1)} %collective-permute-done.5.refs_2_, ...), custom_call_target="tpu_custom_call" | custom-call | flops 1250000000 | tf_op jit(solution)/shard_map/pallas_call | solution.py:39
  111.4 0.0 collective-permute-done.25.refs_7_
  111.4 3.8 %collective-permute-done.17.refs_1_ = bf16[64,512]{1,0:T(8,128)(2,1)S(1)} collective-permute-done((bf16[64,512]{1,0:T(8,128)(2,1)S(1)}, bf16[64,512]{1,0:T(8,128)(2,1)S(1)}, u32[]{:S(2)}, u32[]{:S(2)}) %collective-permute-start.17) | collective-permute-done | bytes 65568 | tf_op jit(solution)/shard_map/ppermute | solution.py:64
  115.2 0.0 collective-permute-done.18.refs_2_
  115.2 0.0 collective-permute-done.19.refs_3_
  115.2 1.6 %shard_map.155 = bf16[160,512]{1,0:T(8,128)(2,1)} custom-call(s32[2]{0:T(128)S(1)} %pad_add_fusion.place, s32[2,160]{1,0:T(2,128)S(1)} %get-tuple-element.28.slot_ref, f32[2,160]{1,0:T(2,128)S(1)} %bitcast.19, bf16[64,512]{1,0:T(8,128)(2,1)S(1)} %collective-permute-done.16.refs_0_, bf16[64,512]{1,0:T(8,128)(2,1)S(1)} %collective-permute-done.17.refs_1_, ...), custom_call_target="tpu_custom_call" | custom-call | flops 750000000 | tf_op jit(solution)/shard_map/pallas_call | solution.py:39
  (13 shorter events, 0.0 us)
Async XLA Ops:
  0.6 30.4 %copy-start = (bf16[256,2048]{1,0:T(8,128)(2,1)S(1)}, bf16[256,2048]{1,0:T(8,128)(2,1)}, u32[]{:S(2)}) copy-start(bf16[256,2048]{1,0:T(8,128)(2,1)} %refs_4_.1) | copy-start | bytes 3145732
  24.1 14.8 %collective-permute-start.11 = (bf16[512,512]{1,0:T(8,128)(2,1)S(1)}, bf16[512,512]{1,0:T(8,128)(2,1)S(1)}, u32[]{:S(2)}, u32[]{:S(2)}) collective-permute-start(bf16[512,512]{1,0:T(8,128)(2,1)S(1)} %bitcast.12), channel_id=1, source_target_pairs={{0,2},{1,3},{2,0},{3,1},{4,6},{5,7},{6,4},{7,5},{8,10},{9,11},{10,... | collective-permute-start | bytes 1572872 | tf_op jit(solution)/shard_map/ppermute | solution.py:64
  25.6 33.5 %collective-permute-start.8 = (bf16[256,2048]{1,0:T(8,128)(2,1)}, bf16[256,2048]{1,0:T(8,128)(2,1)S(1)}, u32[]{:S(2)}, u32[]{:S(2)}) collective-permute-start(bf16[256,2048]{1,0:T(8,128)(2,1)} %refs_4_.1), channel_id=1, source_target_pairs={{0,2},{1,3},{2,0},{3,1},{4,6},{5,7},{6,4},{7,5},{8,10},{9,11},{10,... | collective-permute-start | bytes 3145736 | tf_op jit(solution)/shard_map/ppermute | solution.py:64
  29.6 5.0 %collective-permute-start = (bf16[128,512]{1,0:T(8,128)(2,1)S(1)}, bf16[128,512]{1,0:T(8,128)(2,1)S(1)}, u32[]{:S(2)}, u32[]{:S(2)}) collective-permute-start(bf16[128,512]{1,0:T(8,128)(2,1)S(1)} %get-tuple-element.21), channel_id=1, source_target_pairs={{0,4},{4,0},{8,12},{12,8},{16,20},{20,16},{24,28},{28,24},{1,5},{5... | collective-permute-start | bytes 393224 | tf_op jit(solution)/shard_map/ppermute | solution.py:64
  31.1 70.5 %collective-permute-start.7 = (bf16[256,2048]{1,0:T(8,128)(2,1)S(1)}, bf16[256,2048]{1,0:T(8,128)(2,1)S(1)}, u32[]{:S(2)}, u32[]{:S(2)}) collective-permute-start(bf16[256,2048]{1,0:T(8,128)(2,1)S(1)} %copy-done), channel_id=1, source_target_pairs={{0,1},{1,0},{2,3},{3,2},{4,5},{5,4},{6,7},{7,6},{8,9},{9,8},{10,11... | collective-permute-start | bytes 3145736 | tf_op jit(solution)/shard_map/ppermute | solution.py:64
  34.6 35.6 %collective-permute-start.1 = (bf16[256,512]{1,0:T(8,128)(2,1)S(1)}, bf16[256,512]{1,0:T(8,128)(2,1)S(1)}, u32[]{:S(2)}, u32[]{:S(2)}) collective-permute-start(bf16[256,512]{1,0:T(8,128)(2,1)S(1)} %constant_dynamic-update-slice_fusion.refs_0_), channel_id=1, source_target_pairs={{0,24},{4,28},{8,16},{12,20},{16,8},{20,12},{24,0},{28,4},{1,25},{... | collective-permute-start | bytes 786440 | tf_op jit(solution)/shard_map/ppermute | solution.py:64
  35.8 24.7 %collective-permute-start.10 = (bf16[512,512]{1,0:T(8,128)(2,1)S(1)}, bf16[512,512]{1,0:T(8,128)(2,1)S(1)}, u32[]{:S(2)}, u32[]{:S(2)}) collective-permute-start(bf16[512,512]{1,0:T(8,128)(2,1)S(1)} %bitcast.13), channel_id=1, source_target_pairs={{0,1},{1,0},{2,3},{3,2},{4,5},{5,4},{6,7},{7,6},{8,9},{9,8},{10,11... | collective-permute-start | bytes 1572872 | tf_op jit(solution)/shard_map/ppermute | solution.py:64
  38.9 22.6 %collective-permute-start.12 = (bf16[512,512]{1,0:T(8,128)(2,1)S(1)}, bf16[512,512]{1,0:T(8,128)(2,1)S(1)}, u32[]{:S(2)}, u32[]{:S(2)}) collective-permute-start(bf16[512,512]{1,0:T(8,128)(2,1)S(1)} %collective-permute-done.11.refs_2_), channel_id=1, source_target_pairs={{0,1},{1,0},{2,3},{3,2},{4,5},{5,4},{6,7},{7,6},{8,9},{9,8},{10,11... | collective-permute-start | bytes 1572872 | tf_op jit(solution)/shard_map/ppermute | solution.py:64
  38.9 22.6 %copy-start.1 = (bf16[1,2048,1024]{2,1,0:T(8,128)(2,1)S(1)}, bf16[1,2048,1024]{2,1,0:T(8,128)(2,1)}, u32[]{:S(2)}) copy-start(bf16[1,2048,1024]{2,1,0:T(8,128)(2,1)} %param.24) | copy-start | bytes 12582916
  38.9 22.6 %copy-start.2 = (bf16[1,2048,1024]{2,1,0:T(8,128)(2,1)S(1)}, bf16[1,2048,1024]{2,1,0:T(8,128)(2,1)}, u32[]{:S(2)}) copy-start(bf16[1,2048,1024]{2,1,0:T(8,128)(2,1)} %param.25) | copy-start | bytes 12582916
  38.9 22.6 %copy-start.3 = (bf16[1,1024,2048]{2,1,0:T(8,128)(2,1)S(1)}, bf16[1,1024,2048]{2,1,0:T(8,128)(2,1)}, u32[]{:S(2)}) copy-start(bf16[1,1024,2048]{2,1,0:T(8,128)(2,1)} %param.26) | copy-start | bytes 12582916
  59.1 12.6 %collective-permute-start.2 = (bf16[256,512]{1,0:T(8,128)(2,1)S(1)}, bf16[256,512]{1,0:T(8,128)(2,1)S(1)}, u32[]{:S(2)}, u32[]{:S(2)}) collective-permute-start(bf16[256,512]{1,0:T(8,128)(2,1)S(1)} %constant_dynamic-update-slice_fusion.refs_0_), channel_id=1, source_target_pairs={{0,16},{4,20},{8,24},{12,28},{16,0},{20,4},{24,8},{28,12},{1,17},{... | collective-permute-start | bytes 786440 | tf_op jit(solution)/shard_map/ppermute | solution.py:64
  60.6 11.7 %collective-permute-start.3 = (bf16[256,512]{1,0:T(8,128)(2,1)S(1)}, bf16[256,512]{1,0:T(8,128)(2,1)S(1)}, u32[]{:S(2)}, u32[]{:S(2)}) collective-permute-start(bf16[256,512]{1,0:T(8,128)(2,1)S(1)} %constant_dynamic-update-slice_fusion.refs_0_), channel_id=1, source_target_pairs={{0,8},{4,12},{8,0},{12,4},{16,24},{20,28},{24,16},{28,20},{1,9},{5... | collective-permute-start | bytes 786440 | tf_op jit(solution)/shard_map/ppermute | solution.py:64
  61.5 42.8 %collective-permute-start.9 = (bf16[256,2048]{1,0:T(8,128)(2,1)S(1)}, bf16[256,2048]{1,0:T(8,128)(2,1)S(1)}, u32[]{:S(2)}, u32[]{:S(2)}) collective-permute-start(bf16[256,2048]{1,0:T(8,128)(2,1)S(1)} %collective-permute-done.8.refs_6_), channel_id=1, source_target_pairs={{0,1},{1,0},{2,3},{3,2},{4,5},{5,4},{6,7},{7,6},{8,9},{9,8},{10,11... | collective-permute-start | bytes 3145736 | tf_op jit(solution)/shard_map/ppermute | solution.py:64
  70.3 9.8 %collective-permute-start.21 = (bf16[256,512]{1,0:T(8,128)(2,1)S(1)}, bf16[256,512]{1,0:T(8,128)(2,1)S(1)}, u32[]{:S(2)}, u32[]{:S(2)}) collective-permute-start(bf16[256,512]{1,0:T(8,128)(2,1)S(1)} %get-tuple-element.37), channel_id=1, source_target_pairs={{0,1},{1,0},{2,3},{3,2},{4,5},{5,4},{6,7},{7,6},{8,9},{9,8},{10,11... | collective-permute-start | bytes 786440 | tf_op jit(solution)/shard_map/ppermute | solution.py:64
  71.7 9.7 %collective-permute-start.14 = (bf16[256,512]{1,0:T(8,128)(2,1)S(1)}, bf16[256,512]{1,0:T(8,128)(2,1)S(1)}, u32[]{:S(2)}, u32[]{:S(2)}) collective-permute-start(bf16[256,512]{1,0:T(8,128)(2,1)S(1)} %get-tuple-element.33), channel_id=1, source_target_pairs={{0,1},{1,0},{2,3},{3,2},{4,5},{5,4},{6,7},{7,6},{8,9},{9,8},{10,11... | collective-permute-start | bytes 786440 | tf_op jit(solution)/shard_map/ppermute | solution.py:64
  80.0 1.3 %collective-permute-start.4 = (bf16[128,256]{1,0:T(8,128)(2,1)S(1)}, bf16[128,256]{1,0:T(8,128)(2,1)S(1)}, u32[]{:S(2)}, u32[]{:S(2)}) collective-permute-start(bf16[128,256]{1,0:T(8,128)(2,1)S(1)} %get-tuple-element.25), channel_id=1, source_target_pairs={{0,1},{1,0},{2,3},{3,2},{4,5},{5,4},{6,7},{7,6},{8,9},{9,8},{10,11... | collective-permute-start | bytes 196616 | tf_op jit(solution)/shard_map/ppermute | solution.py:64
  80.1 3.0 %collective-permute-start.20 = (bf16[256,512]{1,0:T(8,128)(2,1)S(1)}, bf16[256,512]{1,0:T(8,128)(2,1)S(1)}, u32[]{:S(2)}, u32[]{:S(2)}) collective-permute-start(bf16[256,512]{1,0:T(8,128)(2,1)S(1)} %get-tuple-element.35), channel_id=1, source_target_pairs={{0,1},{1,0},{2,3},{3,2},{4,5},{5,4},{6,7},{7,6},{8,9},{9,8},{10,11... | collective-permute-start | bytes 786440 | tf_op jit(solution)/shard_map/ppermute | solution.py:64
  80.5 34.6 %copy-start.4 = (f32[160,2]{0,1:T(2,128)S(1)}, f32[160,2]{0,1:T(2,128)}, u32[]{:S(2)}) copy-start(f32[160,2]{0,1:T(2,128)} %param.23) | copy-start | bytes 3844
  81.3 16.4 %collective-permute-start.13 = (bf16[256,512]{1,0:T(8,128)(2,1)S(1)}, bf16[256,512]{1,0:T(8,128)(2,1)S(1)}, u32[]{:S(2)}, u32[]{:S(2)}) collective-permute-start(bf16[256,512]{1,0:T(8,128)(2,1)S(1)} %get-tuple-element.31), channel_id=1, source_target_pairs={{0,1},{1,0},{2,3},{3,2},{4,5},{5,4},{6,7},{7,6},{8,9},{9,8},{10,11... | collective-permute-start | bytes 786440 | tf_op jit(solution)/shard_map/ppermute | solution.py:64
  81.4 9.2 %collective-permute-start.22 = (bf16[256,512]{1,0:T(8,128)(2,1)S(1)}, bf16[256,512]{1,0:T(8,128)(2,1)S(1)}, u32[]{:S(2)}, u32[]{:S(2)}) collective-permute-start(bf16[256,512]{1,0:T(8,128)(2,1)S(1)} %add_convert_fusion), channel_id=1, source_target_pairs={{0,2},{1,3},{2,0},{3,1},{4,6},{5,7},{6,4},{7,5},{8,10},{9,11},{10,... | collective-permute-start | bytes 786440 | tf_op jit(solution)/shard_map/ppermute | solution.py:64
  83.0 15.6 %collective-permute-start.15 = (bf16[256,512]{1,0:T(8,128)(2,1)S(1)}, bf16[256,512]{1,0:T(8,128)(2,1)S(1)}, u32[]{:S(2)}, u32[]{:S(2)}) collective-permute-start(bf16[256,512]{1,0:T(8,128)(2,1)S(1)} %add_convert_fusion.1), channel_id=1, source_target_pairs={{0,2},{1,3},{2,0},{3,1},{4,6},{5,7},{6,4},{7,5},{8,10},{9,11},{10,... | collective-permute-start | bytes 786440 | tf_op jit(solution)/shard_map/ppermute | solution.py:64
  90.6 6.4 %collective-permute-start.5 = (bf16[128,256]{1,0:T(8,128)(2,1)S(1)}, bf16[128,256]{1,0:T(8,128)(2,1)S(1)}, u32[]{:S(2)}, u32[]{:S(2)}) collective-permute-start(bf16[128,256]{1,0:T(8,128)(2,1)S(1)} %get-tuple-element.26), channel_id=1, source_target_pairs={{0,2},{1,3},{2,0},{3,1},{4,6},{5,7},{6,4},{7,5},{8,10},{9,11},{10,... | collective-permute-start | bytes 196616 | tf_op jit(solution)/shard_map/ppermute | solution.py:64
  97.0 4.3 %collective-permute-start.6 = (bf16[128,256]{1,0:T(8,128)(2,1)S(1)}, bf16[128,256]{1,0:T(8,128)(2,1)S(1)}, u32[]{:S(2)}, u32[]{:S(2)}) collective-permute-start(bf16[128,256]{1,0:T(8,128)(2,1)S(1)} %get-tuple-element.27), channel_id=1, source_target_pairs={{0,3},{1,2},{2,1},{3,0},{4,7},{5,6},{6,5},{7,4},{8,11},{9,10},{10,... | collective-permute-start | bytes 196616 | tf_op jit(solution)/shard_map/ppermute | solution.py:64
  97.7 7.9 %collective-permute-start.23 = (bf16[64,512]{1,0:T(8,128)(2,1)S(1)}, bf16[64,512]{1,0:T(8,128)(2,1)S(1)}, u32[]{:S(2)}, u32[]{:S(2)}) collective-permute-start(bf16[64,512]{1,0:T(8,128)(2,1)S(1)} %get-tuple-element.40), channel_id=1, source_target_pairs={{0,4},{4,0},{8,12},{12,8},{16,20},{20,16},{24,28},{28,24},{1,5},{5... | collective-permute-start | bytes 196616 | tf_op jit(solution)/shard_map/ppermute | solution.py:64
  98.7 8.1 %collective-permute-start.24 = (bf16[64,512]{1,0:T(8,128)(2,1)S(1)}, bf16[64,512]{1,0:T(8,128)(2,1)S(1)}, u32[]{:S(2)}, u32[]{:S(2)}) collective-permute-start(bf16[64,512]{1,0:T(8,128)(2,1)S(1)} %get-tuple-element.39), channel_id=1, source_target_pairs={{0,8},{4,12},{8,0},{12,4},{16,24},{20,28},{24,16},{28,20},{1,9},{5... | collective-permute-start | bytes 196616 | tf_op jit(solution)/shard_map/ppermute | solution.py:64
  101.3 10.0 %collective-permute-start.25 = (bf16[64,512]{1,0:T(8,128)(2,1)S(1)}, bf16[64,512]{1,0:T(8,128)(2,1)S(1)}, u32[]{:S(2)}, u32[]{:S(2)}) collective-permute-start(bf16[64,512]{1,0:T(8,128)(2,1)S(1)} %get-tuple-element.38), channel_id=1, source_target_pairs={{0,12},{4,8},{8,4},{12,0},{16,28},{20,24},{24,20},{28,16},{1,13},{... | collective-permute-start | bytes 196616 | tf_op jit(solution)/shard_map/ppermute | solution.py:64
  101.6 9.8 %collective-permute-start.16 = (bf16[64,512]{1,0:T(8,128)(2,1)S(1)}, bf16[64,512]{1,0:T(8,128)(2,1)S(1)}, u32[]{:S(2)}, u32[]{:S(2)}) collective-permute-start(bf16[64,512]{1,0:T(8,128)(2,1)S(1)} %get-tuple-element.45), channel_id=1, source_target_pairs={{0,16},{4,20},{8,24},{12,28},{16,0},{20,4},{24,8},{28,12},{1,17},{... | collective-permute-start | bytes 196616 | tf_op jit(solution)/shard_map/ppermute | solution.py:64
  104.4 10.8 %collective-permute-start.17 = (bf16[64,512]{1,0:T(8,128)(2,1)S(1)}, bf16[64,512]{1,0:T(8,128)(2,1)S(1)}, u32[]{:S(2)}, u32[]{:S(2)}) collective-permute-start(bf16[64,512]{1,0:T(8,128)(2,1)S(1)} %get-tuple-element.44), channel_id=1, source_target_pairs={{0,20},{4,16},{8,28},{12,24},{16,4},{20,0},{24,12},{28,8},{1,21},{... | collective-permute-start | bytes 196616 | tf_op jit(solution)/shard_map/ppermute | solution.py:64
  105.6 9.6 %collective-permute-start.18 = (bf16[64,512]{1,0:T(8,128)(2,1)S(1)}, bf16[64,512]{1,0:T(8,128)(2,1)S(1)}, u32[]{:S(2)}, u32[]{:S(2)}) collective-permute-start(bf16[64,512]{1,0:T(8,128)(2,1)S(1)} %get-tuple-element.43), channel_id=1, source_target_pairs={{0,24},{4,28},{8,16},{12,20},{16,8},{20,12},{24,0},{28,4},{1,25},{... | collective-permute-start | bytes 196616 | tf_op jit(solution)/shard_map/ppermute | solution.py:64
  106.8 8.4 %collective-permute-start.19 = (bf16[64,512]{1,0:T(8,128)(2,1)S(1)}, bf16[64,512]{1,0:T(8,128)(2,1)S(1)}, u32[]{:S(2)}, u32[]{:S(2)}) collective-permute-start(bf16[64,512]{1,0:T(8,128)(2,1)S(1)} %get-tuple-element.42), channel_id=1, source_target_pairs={{0,28},{4,24},{8,20},{12,16},{16,12},{20,8},{24,4},{28,0},{1,29},{... | collective-permute-start | bytes 196616 | tf_op jit(solution)/shard_map/ppermute | solution.py:64
